TPU v7x, 512 devices: a 8x2x16 block of a 8x8x16 slice. The times are simulated.
512 devices in a mesh: grp: 2 (over y), ep: 32 (over z, core), tp: 8 (over x).
Axes of the slice: x: 8, y: 2, z: 16, core: 2. Of those that a mesh axis runs over, the one named last changes fastest.
The devices are a block of a 8x8x16 slice.
Arguments:
- value_in: bfloat16 [32768, 1024], P(('grp', 'ep'), 'tp'), parts along dimension 0, may hold values from -6 to 6
- gate_in: bfloat16 [32768, 1024], P(('grp', 'ep'), 'tp'), parts along dimension 0, may hold values from -6 to 6
- conv_taps: float32 [31, 1024], P(None, 'tp'), may hold values from -12 to 12
- chan_gain: float32 [1024], replicated, may hold values from 0.1 to 1.9
- out_weight: bfloat16 [1024, 2048], P(None, 'tp'), may hold values from -0.1875 to 0.1875
- second_rows: bfloat16 [8192, 2048], P(('grp', 'ep')), parts along dimension 0, may hold values from -6 to 6
- expert_gain: float32 [2048], replicated, may hold values from 0.1 to 1.9
- routes: int32 [8192, 2], P(('grp', 'ep')), parts along dimension 0, may hold values from 0 to 15, all different within a row; in each aligned block of 128 rows (0 to 127, 128 to 255, ...) at most 24 rows name the same one
- route_weights: float32 [8192, 2], P(('grp', 'ep')), parts along dimension 0, may hold values from 0.1 to 0.9
- gate_w: bfloat16 [32, 2048, 2048], P('ep', None, 'tp'), may hold values from -0.125 to 0.125
- up_w: bfloat16 [32, 2048, 2048], P('ep', None, 'tp'), may hold values from -0.125 to 0.125
- down_w: bfloat16 [32, 2048, 2048], P('ep', 'tp'), may hold values from -0.125 to 0.125
Outputs:
- mixer_rows: bfloat16 [32768, 2048], P(('grp', 'ep'), 'tp'), parts along dimension 0
- routed_rows: bfloat16 [8192, 2048], P(('grp', 'ep'), 'tp'), parts along dimension 0
There are 2 independent parts, one for each index of `grp`. A program takes and returns all parts, laid end to end along the dimension named above; an argument that names none is the same for every part. Nothing has to cross between parts.
Inputs may be any that keep to these rules, and one draw needn't show every extreme that they name: `routes`: in each aligned block of 128 rows (the rows of one index of ep) no expert is named by more than 24 rows, a bound that some block reaches; each row names 2 different experts.
All inputs are finite; a program needn't handle non-finite values.
Results may differ from a plain program's by a relative error of at most 0.017.
Values may be sent and summed in bfloat16 or wider, within the bound.
No kernel may reach another device: no remote copies, remote signals or barrier semaphores. Data moves between devices by JAX's collectives and lax.ppermute only.
A program may use at most 64 MiB of HBM per device.

v0:
```python
import jax
import jax.numpy as jnp
from jax import lax
from jax.sharding import PartitionSpec as P

eps = 1e-06


def partner_2(value, axis, bit):
    return lax.ppermute(value, axis, [(i, i ^ 1 << bit) for i in range(lax.axis_size(axis))])


def shifted(value, axis, by):
    devices = lax.axis_size(axis)
    pairs = [(i, i + by) for i in range(devices) if 0 <= i + by < devices]
    return lax.ppermute(value, axis, pairs)


def copy_for_each(value, axis):
    copies = jnp.broadcast_to(value, (lax.axis_size(axis), *value.shape))
    return lax.all_to_all(copies, axis, split_axis=0, concat_axis=0, tiled=True)


def laid_out(tiles, dim):
    lengths = list(tiles.shape[1:])
    lengths[dim] *= tiles.shape[0]
    return jnp.moveaxis(tiles, 0, dim).reshape(lengths)


def gather_directly(value, axis, dim):
    tiles = copy_for_each(value, axis)
    return laid_out(tiles, dim)


def partner(block):
    return partner_2(block, "ep", 0)


def across(block):
    return lax.all_to_all(block, "ep", split_axis=0, concat_axis=0, tiled=True)


def on_device(
    value_in,
    gate_in,
    conv_taps,
    chan_gain,
    out_weight,
    second_rows,
    expert_gain,
    routes,
    route_weights,
    gate_w,
    up_w,
    down_w,
):
    taps = conv_taps.shape[0]
    glu = (value_in.astype(jnp.float32) * jax.nn.sigmoid(gate_in.astype(jnp.float32))).astype(
        jnp.bfloat16
    )
    length = glu.shape[0]
    before = shifted(glu[length - taps + 1 :], "ep", 1)
    padded = jnp.concatenate([before, glu], axis=0).astype(jnp.float32)
    total = jnp.zeros(glu.shape, jnp.float32)
    for offset in range(taps):
        total = total + conv_taps[offset][None, :] * padded[offset : offset + length]
    convolved = total.astype(jnp.bfloat16)
    channels = gather_directly(convolved, "tp", 1)
    values = channels.astype(jnp.float32)
    centered = values - jnp.mean(values, axis=-1, keepdims=True)
    scaled = (
        centered
        * lax.rsqrt(jnp.mean(centered * centered, axis=-1, keepdims=True) + eps)
        * chan_gain
    )
    activated = jax.nn.silu(scaled).astype(jnp.bfloat16)
    mixer_rows = jnp.dot(activated, out_weight, preferred_element_type=jnp.float32).astype(
        jnp.bfloat16
    )
    n_ep = lax.axis_size("ep")
    experts = n_ep // 2
    tokens = second_rows.shape[0]
    top = routes.shape[1]
    width = second_rows.shape[1]
    capacity = 2 * max(1, min(tokens // 2, 3 * tokens * top // (4 * experts)))
    half_slots = capacity // 2
    rows = second_rows.astype(jnp.float32)
    normed = (
        rows * lax.rsqrt(jnp.mean(rows * rows, axis=-1, keepdims=True) + eps) * expert_gain
    ).astype(jnp.bfloat16)
    chosen = routes.reshape(-1)
    hits = (chosen[:, None] == jnp.arange(experts, dtype=jnp.int32)[None, :]).astype(jnp.int32)
    place = jnp.sum((jnp.cumsum(hits, axis=0) - 1) * hits, axis=1)
    target = (chosen * capacity + place).reshape(tokens, top)
    slots = jnp.arange(experts * capacity, dtype=jnp.int32)
    matches = target[:, :, None] == slots[None, None, :]
    picker = jnp.any(matches, axis=1).astype(jnp.bfloat16)
    outgoing = jnp.dot(picker.T, normed, preferred_element_type=jnp.float32).astype(jnp.bfloat16)
    combiner = jnp.sum(jnp.where(matches, route_weights[:, :, None], 0.0), axis=1)
    upper = lax.axis_index("ep") % 2
    arrived = across(outgoing.reshape(n_ep, half_slots, width))
    other = partner(arrived)
    first = jnp.where(upper == 0, arrived, other)
    second = jnp.where(upper == 0, other, arrived)
    incoming = jnp.concatenate([first, second], axis=1)
    block_rows = incoming.reshape(n_ep * capacity, width)
    gate = jnp.dot(block_rows, gate_w[0], preferred_element_type=jnp.float32)
    lifted = jnp.dot(block_rows, up_w[0], preferred_element_type=jnp.float32)
    hidden = (jax.nn.silu(gate) * lifted).astype(jnp.bfloat16)
    partial_value = jnp.dot(hidden, down_w[0], preferred_element_type=jnp.float32)
    half_sums = lax.psum_scatter(
        partial_value.astype(jnp.bfloat16), "tp", scatter_dimension=1, tiled=True
    )
    columns = half_sums.shape[1]
    half_sums = half_sums.reshape(n_ep, capacity, columns)
    other_sums = partner(half_sums)
    joined = (half_sums.astype(jnp.float32) + other_sums.astype(jnp.float32)).astype(jnp.bfloat16)
    own = lax.dynamic_slice_in_dim(joined, upper * half_slots, half_slots, 1)
    results = across(own).reshape(experts * capacity, columns)
    routed_rows = jnp.dot(
        combiner,
        results.astype(jnp.float32),
        precision=lax.Precision.HIGHEST,
        preferred_element_type=jnp.float32,
    ).astype(jnp.bfloat16)
    return (mixer_rows, routed_rows)


def solution(mesh):
    placed = (
        P(("grp", "ep"), "tp"),
        P(("grp", "ep"), "tp"),
        P(None, "tp"),
        P(),
        P(None, "tp"),
        P(("grp", "ep"), None),
        P(),
        P(("grp", "ep"), None),
        P(("grp", "ep"), None),
        P("ep", None, "tp"),
        P("ep", None, "tp"),
        P("ep", "tp", None),
    )
    return jax.shard_map(
        on_device,
        mesh=mesh,
        in_specs=placed,
        out_specs=(P(("grp", "ep"), "tp"), P(("grp", "ep"), "tp")),
        check_vma=False,
    )
```

profile of v0, /device:TPU:65, one launch (start us, length us, event | category | flops | bytes accessed | tf_op | source)
XLA Modules:
  0.0 291.8 jit_solution(6401108884725112407)
XLA Ops:
  10.4 1.2 fusion.2
  11.6 1.7 convolution_convert_fusion.1
  13.3 1.5 reshape.74
  14.9 145.9 %all_to_all.15 = bf16[32,12,2048]{2,1,0:T(8,128)(2,1)S(1)} all-to-all(bf16[32,12,2048]{2,1,0:T(8,128)(2,1)} %reshape.74), channel_id=1, replica_groups=mesh['grp'=2,'ep'=32,'tp'=8] {'ep'}, dimensions={0} | all-to-all | bytes 3145728 | tf_op jit(solution)/shard_map/all_to_all | solution.py:40
  160.7 2.0 copy.48
  162.7 3.1 %collective-permute-start.1 = (bf16[32,12,2048]{2,0,1:T(8,128)(2,1)}, bf16[32,12,2048]{2,0,1:T(8,128)(2,1)}, u32[]{:S(2)}, u32[]{:S(2)}) collective-permute-start(bf16[32,12,2048]{2,0,1:T(8,128)(2,1)} %copy.48), channel_id=1, source_target_pairs={{0,8},{8,0},{16,24},{24,16},{32,40},{40,32},{48,56},{56,48},{64,72... | collective-permute-start | bytes 4718600 | tf_op jit(solution)/shard_map/ppermute | solution.py:10
  165.8 3.3 %collective-permute-done.1 = bf16[32,12,2048]{2,0,1:T(8,128)(2,1)} collective-permute-done((bf16[32,12,2048]{2,0,1:T(8,128)(2,1)}, bf16[32,12,2048]{2,0,1:T(8,128)(2,1)}, u32[]{:S(2)}, u32[]{:S(2)}) %collective-permute-start.1) | collective-permute-done | bytes 1572896 | tf_op jit(solution)/shard_map/ppermute | solution.py:10
  169.2 2.4 copy_select_fusion.1
  171.6 1.0 pad_maximum_fusion
  172.6 1.7 copy-done.1
  174.3 1.0 fusion.6
  175.5 6.9 %convolution_convert_fusion = bf16[768,2048]{1,0:T(8,128)(2,1)} fusion(bf16[1,256,2048]{2,1,0:T(8,128)(2,1)S(1)} %copy-done, f32[768,256]{1,0:T(8,128)S(1)} %fusion.6, bf16[768,2048]{1,0:T(8,128)(2,1)} %bitcast.110, bf16[1,2048,256]{2,1,0:T(8,128)(2,1)S(1)} %copy-done.8), kind=kOutput, calls=%fused_computation | convolution fusion | flops 1613365248 | bytes 9175040 | tf_op jit(solution)/shard_map/dot_general | solution.py:110
  183.5 2.0 collective-permute-start
  185.5 1.1 collective-permute-done
  187.5 1.1 broadcast_in_dim.10
  188.5 6.2 %all-to-all-start = ((bf16[8,512,128]{1,2,0:T(8,128)(2,1)}), bf16[8,512,128]{1,2,0:T(8,128)(2,1)S(1)}, u32[]{:S(2)}, u32[]{:S(2)}) async-start(bf16[8,512,128]{1,2,0:T(8,128)(2,1)} %broadcast_in_dim.10), calls=%async_computation | async-start | bytes 2097152 | tf_op jit(solution)/shard_map/all_to_all | solution.py:21
  194.9 40.3 %all-to-all-done = bf16[8,512,128]{1,2,0:T(8,128)(2,1)S(1)} async-done(((bf16[8,512,128]{1,2,0:T(8,128)(2,1)}), bf16[8,512,128]{1,2,0:T(8,128)(2,1)S(1)}, u32[]{:S(2)}, u32[]{:S(2)}) %all-to-all-start) | async-done | bytes 1048608 | tf_op jit(solution)/shard_map/all_to_all | solution.py:21
  235.3 12.2 %reduce-scatter.2.cloned.1.call-done = bf16[768,256]{1,0:T(8,128)(2,1)} async-done(((bf16[768,2048]{1,0:T(8,128)(2,1)}), bf16[768,256]{1,0:T(8,128)(2,1)}) %reduce-scatter.2.cloned.1.call-update) | async-done | bytes 393232 | tf_op jit(solution)/shard_map/reduce_scatter | solution.py:111
  247.5 4.2 %collective-permute-start.2 = (bf16[32,24,256]{2,1,0:T(8,128)(2,1)}, bf16[32,24,256]{2,1,0:T(8,128)(2,1)S(1)}, u32[]{:S(2)}, u32[]{:S(2)}) collective-permute-start(bf16[32,24,256]{2,1,0:T(8,128)(2,1)} %bitcast.111), channel_id=1, source_target_pairs={{0,8},{8,0},{16,24},{24,16},{32,40},{40,32},{48,56},{56,48},{64,72... | collective-permute-start | bytes 1179656 | tf_op jit(solution)/shard_map/ppermute | solution.py:10
  252.1 1.2 collective-permute-done.2
  253.3 1.8 add_convert_fusion
  255.1 6.8 %all-to-all-start.2 = ((bf16[32,12,256]{2,1,0:T(8,128)(2,1)}), bf16[32,12,256]{2,1,0:T(8,128)(2,1)S(1)}, u32[]{:S(2)}, u32[]{:S(2)}) async-start(bf16[32,12,256]{2,1,0:T(8,128)(2,1)} %add_convert_fusion), calls=%async_computation.3 | async-start | bytes 524288 | tf_op jit(solution)/shard_map/all_to_all | solution.py:40
  262.7 1.2 convolution_convert_fusion.2
  263.9 20.2 %all-to-all-done.2 = bf16[32,12,256]{2,1,0:T(8,128)(2,1)S(1)} async-done(((bf16[32,12,256]{2,1,0:T(8,128)(2,1)}), bf16[32,12,256]{2,1,0:T(8,128)(2,1)S(1)}, u32[]{:S(2)}, u32[]{:S(2)}) %all-to-all-start.2) | async-done | bytes 196640 | tf_op jit(solution)/shard_map/all_to_all | solution.py:40
  (50 shorter events, 7.6 us)
Async XLA Ops:
  7.2 168.1 %copy-start = (bf16[1,256,2048]{2,1,0:T(8,128)(2,1)S(1)}, bf16[1,256,2048]{2,1,0:T(8,128)(2,1)}, u32[]{:S(2)}) copy-start(bf16[1,256,2048]{2,1,0:T(8,128)(2,1)} %param.23) | copy-start | bytes 3145732
  7.2 240.3 %reduce-scatter.2.cloned.1.call-start = ((), (), s32[]{:S(2)}) async-start(), calls=%async_computation.4 | async-start | bytes 3538944 | tf_op jit(solution)/shard_map/reduce_scatter | solution.py:111
  162.7 6.4 %collective-permute-start.1 = (bf16[32,12,2048]{2,0,1:T(8,128)(2,1)}, bf16[32,12,2048]{2,0,1:T(8,128)(2,1)}, u32[]{:S(2)}, u32[]{:S(2)}) collective-permute-start(bf16[32,12,2048]{2,0,1:T(8,128)(2,1)} %copy.48), channel_id=1, source_target_pairs={{0,8},{8,0},{16,24},{24,16},{32,40},{40,32},{48,56},{56,48},{64,72... | collective-permute-start | bytes 4718600 | tf_op jit(solution)/shard_map/ppermute | solution.py:10
  171.5 2.8 copy-start.7
  172.6 1.7 copy-start.1
  174.3 1.2 copy-start.8
  182.4 0.9 copy-start.2
  182.4 1.0 copy-start.3
  182.4 3.0 %copy-start.4 = (f32[31,128]{1,0:T(8,128)S(1)}, f32[31,128]{1,0:T(8,128)}, u32[]{:S(2)}) copy-start(f32[31,128]{1,0:T(8,128)} %param.14) | copy-start | bytes 47620
  183.5 3.1 %collective-permute-start = (bf16[30,128]{1,0:T(8,128)(2,1)S(1)}, bf16[30,128]{1,0:T(8,128)(2,1)S(1)}, u32[]{:S(2)}, u32[]{:S(2)}) collective-permute-start(bf16[30,128]{1,0:T(8,128)(2,1)S(1)} %slice.260), channel_id=1, source_target_pairs={{0,8},{8,16},{16,24},{24,32},{32,40},{40,48},{48,56},{56,64},{64,7... | collective-permute-start | bytes 23048 | tf_op jit(solution)/shard_map/ppermute | solution.py:16
  187.3 7.4 %copy-start.6 = (f32[128,2]{0,1:T(2,128)S(1)}, f32[128,2]{0,1:T(2,128)}, u32[]{:S(2)}) copy-start(f32[128,2]{0,1:T(2,128)} %param.20) | copy-start | bytes 3076
  188.5 46.6 %all-to-all-start = ((bf16[8,512,128]{1,2,0:T(8,128)(2,1)}), bf16[8,512,128]{1,2,0:T(8,128)(2,1)S(1)}, u32[]{:S(2)}, u32[]{:S(2)}) async-start(bf16[8,512,128]{1,2,0:T(8,128)(2,1)} %broadcast_in_dim.10), calls=%async_computation | async-start | bytes 2097152 | tf_op jit(solution)/shard_map/all_to_all | solution.py:21
  194.7 67.2 %copy-start.5 = (f32[1024]{0:T(1024)S(1)}, f32[1024]{0:T(1024)}, u32[]{:S(2)}) copy-start(f32[1024]{0:T(1024)} %param.15) | copy-start | bytes 12292
  247.5 5.8 %collective-permute-start.2 = (bf16[32,24,256]{2,1,0:T(8,128)(2,1)}, bf16[32,24,256]{2,1,0:T(8,128)(2,1)S(1)}, u32[]{:S(2)}, u32[]{:S(2)}) collective-permute-start(bf16[32,24,256]{2,1,0:T(8,128)(2,1)} %bitcast.111), channel_id=1, source_target_pairs={{0,8},{8,0},{16,24},{24,16},{32,40},{40,32},{48,56},{56,48},{64,72... | collective-permute-start | bytes 1179656 | tf_op jit(solution)/shard_map/ppermute | solution.py:10
  251.8 10.9 %copy-start.9 = (bf16[1024,256]{1,0:T(8,128)(2,1)S(1)}, bf16[1024,256]{1,0:T(8,128)(2,1)}, u32[]{:S(2)}) copy-start(bf16[1024,256]{1,0:T(8,128)(2,1)} %param.16) | copy-start | bytes 1572868
  255.1 28.9 %all-to-all-start.2 = ((bf16[32,12,256]{2,1,0:T(8,128)(2,1)}), bf16[32,12,256]{2,1,0:T(8,128)(2,1)S(1)}, u32[]{:S(2)}, u32[]{:S(2)}) async-start(bf16[32,12,256]{2,1,0:T(8,128)(2,1)} %add_convert_fusion), calls=%async_computation.3 | async-start | bytes 524288 | tf_op jit(solution)/shard_map/all_to_all | solution.py:40
Sparse Core Ops, SparseCore 0:
  182.6 64.8 reduce-scatter.1
where the time goes:
time: 292 us
  blocking collectives  146 us (50%)
  waiting for transfers between devices  78.3 us (27%)
  starting transfers between devices  22.2 us (8%)
  between operations  14.3 us (5%)
  matrix products  11.7 us (4%)
  other arithmetic  10.2 us (3%)
  local copies, waits for them, and re-layouts  9.22 us (3%)
    all_to_all x1, blocking collectives, across(): return lax.all_to_all(block, 'ep', split_axis=0, concat_axis=0, tiled=True)  146 us
    all_to_all x1, waiting for transfers between devices, copy_for_each(): return lax.all_to_all(copies, axis, split_axis=0, concat_axis=0, tiled=True)  40.3 us
    all_to_all x1, waiting for transfers between devices, across(): return lax.all_to_all(block, 'ep', split_axis=0, concat_axis=0, tiled=True)  20.2 us
    reduce_scatter x1, waiting for transfers between devices, on_device(): lax.psum_scatter(partial_value.astype(jnp.bfloat16), 'tp', scatter_dimens...  12.2 us
    ppermute x2, starting transfers between devices, partner_2(): lax.ppermute(value, axis, [(i, i ^ 1 << bit) for i in range(lax.axis_size...  7.26 us
    dot_general x1, matrix products, on_device(): jnp.dot(hidden, down_w[0], preferred_element_type=jnp.float32)  6.9 us
    all_to_all x1, starting transfers between devices, across(): return lax.all_to_all(block, 'ep', split_axis=0, concat_axis=0, tiled=True)  6.8 us
    all_to_all x1, starting transfers between devices, copy_for_each(): return lax.all_to_all(copies, axis, split_axis=0, concat_axis=0, tiled=True)  6.16 us
  transfers between devices with their start and end apart: 6, of which 6 were waited for; matrix products, arithmetic and copies ran while one was open for 2% of the time, Pallas kernels for 0%

commit v1 on v0

v1 whole, which is shorter than its diff:
```python
import functools

import jax
import jax.numpy as jnp
from jax import lax
from jax.experimental import pallas as pl
from jax.experimental.pallas import tpu as pltpu
from jax.sharding import Mesh
from jax.sharding import PartitionSpec as P

eps = 1e-06
f32 = jnp.float32
bf16 = jnp.bfloat16


def dot(a, b):
    return jnp.dot(a, b, preferred_element_type=f32)


def slot_hits(routes, experts, capacity):
    top, tokens = routes.shape
    expert = lax.broadcasted_iota(jnp.int32, (experts, tokens), 0)
    hits = [(routes[j : j + 1, :] == expert).astype(f32) for j in range(top)]
    named = functools.reduce(jnp.add, hits).astype(bf16)
    before = lax.broadcasted_iota(jnp.int32, (tokens, tokens), 0)
    after = lax.broadcasted_iota(jnp.int32, (tokens, tokens), 1)
    places = dot(named, (before < after).astype(f32).astype(bf16)).astype(bf16)
    slots = experts * capacity
    first = lax.broadcasted_iota(jnp.int32, (slots, experts), 1) * capacity
    slot = lax.broadcasted_iota(jnp.int32, (slots, experts), 0)
    own = (slot >= first) & (slot < first + capacity)
    spread = own.astype(f32).astype(bf16)
    first_of = jnp.sum(jnp.where(own, first, 0), axis=1, keepdims=True)
    offset = (lax.broadcasted_iota(jnp.int32, (slots, 1), 0) - first_of).astype(f32)
    at_place = dot(spread, places) == offset
    return [(dot(spread, hit.astype(bf16)) > 0.5) & at_place for hit in hits]


def dispatch_kernel(experts, capacity, index, routes, rows, gain, out):
    values = rows[...].astype(f32)
    scale = lax.rsqrt(jnp.mean(values * values, axis=-1, keepdims=True) + eps)
    width = out.shape[1]
    start = pl.multiple_of(index[0] * width, width)
    own = rows[:, pl.ds(start, width)].astype(f32)
    normed = (own * scale * gain[:, pl.ds(start, width)]).astype(bf16)
    matches = slot_hits(routes[...], experts, capacity)
    picker = functools.reduce(jnp.logical_or, matches).astype(f32).astype(bf16)
    out[...] = dot(picker, normed).astype(bf16)


def combiner_kernel(experts, capacity, routes, weights, high, low):
    matches = slot_hits(routes[...], experts, capacity)
    terms = [jnp.where(m, weights[j : j + 1, :], 0.0) for j, m in enumerate(matches)]
    total = functools.reduce(jnp.add, terms).T
    rounded = total.astype(bf16)
    high[...] = rounded
    low[...] = (total - rounded.astype(f32)).astype(bf16)


def combine_kernel(high, low, results, out):
    out[...] = (dot(high[...], results[...]) + dot(low[...], results[...])).astype(bf16)


def experts_kernel(x, gate_w, up_w, down_w, out):
    blocks, width = x.shape[1], x.shape[3]
    gate = up = None
    for b in range(blocks):
        part = x[0, b]
        g = dot(part, gate_w[0, b * width : (b + 1) * width, :])
        u = dot(part, up_w[0, b * width : (b + 1) * width, :])
        gate = g if gate is None else gate + g
        up = u if up is None else up + u
    hidden = (jax.nn.silu(gate) * up).astype(bf16)
    for b in range(blocks):
        piece = dot(hidden, down_w[0, :, b * width : (b + 1) * width])
        out[0, b] = piece.astype(bf16)


def mixer_kernel(x, gain, weight, out):
    values = jnp.concatenate([x[b] for b in range(x.shape[0])], axis=1).astype(f32)
    centered = values - jnp.mean(values, axis=-1, keepdims=True)
    scale = lax.rsqrt(jnp.mean(centered * centered, axis=-1, keepdims=True) + eps)
    activated = jax.nn.silu(centered * scale * gain[...]).astype(bf16)
    out[...] = dot(activated, weight[...]).astype(bf16)


def params(mib):
    return pltpu.CompilerParams(vmem_limit_bytes=mib << 20)


def cost(flops, moved):
    return pl.CostEstimate(flops=flops, bytes_accessed=moved, transcendentals=0)


def on_device(
    value_in,
    gate_in,
    conv_taps,
    chan_gain,
    out_weight,
    second_rows,
    expert_gain,
    routes,
    route_weights,
    gate_w,
    up_w,
    down_w,
):
    n_z, n_core, n_tp = lax.axis_size("z"), lax.axis_size("core"), lax.axis_size("tp")
    experts = n_z
    tokens, width = second_rows.shape
    top = routes.shape[1]
    capacity = 2 * max(1, min(tokens // 2, 3 * tokens * top // (4 * experts)))
    columns = width // n_tp
    slots = experts * capacity
    vmem = pl.BlockSpec(memory_space=pltpu.VMEM)
    smem = pl.BlockSpec(memory_space=pltpu.SMEM)

    routes_t = routes.T
    outgoing = pl.pallas_call(
        functools.partial(dispatch_kernel, experts, capacity),
        out_shape=jax.ShapeDtypeStruct((slots, columns), bf16),
        in_specs=[smem, vmem, vmem, vmem],
        out_specs=vmem,
        compiler_params=params(16),
        cost_estimate=cost(10**8, 10**6),
    )(lax.axis_index("tp").reshape(1), routes_t, second_rows, expert_gain.reshape(1, -1))
    arrived = lax.all_to_all(
        outgoing.reshape(experts, capacity, columns), "z", split_axis=0, concat_axis=0, tiled=True
    )
    rows = n_z * capacity
    incoming = lax.all_gather(arrived.reshape(1, rows, columns), ("core", "tp"), axis=0, tiled=True)

    taps = conv_taps.shape[0]
    halo = -(-(taps - 1) // 16) * 16
    glu = (value_in.astype(f32) * jax.nn.sigmoid(gate_in.astype(f32))).astype(bf16)
    length, channels = glu.shape
    n_ep = n_z * n_core
    before = lax.ppermute(
        glu[length - halo :], ("z", "core"), [(i, i + 1) for i in range(n_ep - 1)]
    )
    padded = jnp.concatenate([before, glu], axis=0).astype(f32)
    total = jnp.zeros(glu.shape, f32)
    for offset in range(taps):
        start = halo - taps + 1 + offset
        total = total + conv_taps[offset][None, :] * padded[start : start + length]
    convolved = total.astype(bf16)
    gathered = lax.all_gather(convolved, "tp", axis=0, tiled=False)
    step = length // 2
    mixer_rows = pl.pallas_call(
        mixer_kernel,
        grid=(length // step,),
        out_shape=jax.ShapeDtypeStruct((length, out_weight.shape[1]), bf16),
        in_specs=[
            pl.BlockSpec((n_tp, step, channels), lambda i: (0, i, 0)),
            pl.BlockSpec((1, n_tp * channels), lambda i: (0, 0)),
            pl.BlockSpec(out_weight.shape, lambda i: (0, 0)),
        ],
        out_specs=pl.BlockSpec((step, out_weight.shape[1]), lambda i: (i, 0)),
        compiler_params=params(16),
        cost_estimate=cost(10**9, 2 * 10**6),
    )(gathered, chan_gain.reshape(1, -1), out_weight)

    step = rows // 2
    block = (1, n_tp, step, columns)
    whole = lambda i: (0, 0, 0)
    pieces = pl.pallas_call(
        experts_kernel,
        grid=(n_core * 2,),
        out_shape=jax.ShapeDtypeStruct((n_core, n_tp, rows, columns), bf16),
        in_specs=[
            pl.BlockSpec(block, lambda i: (i // 2, 0, i % 2, 0)),
            pl.BlockSpec(gate_w.shape, whole),
            pl.BlockSpec(up_w.shape, whole),
            pl.BlockSpec(down_w.shape, whole),
        ],
        out_specs=pl.BlockSpec(block, lambda i: (i // 2, 0, i % 2, 0)),
        compiler_params=params(24),
        cost_estimate=cost(3 * 10**9, 10**7),
    )(incoming.reshape(n_core, n_tp, rows, columns), gate_w, up_w, down_w)
    sums = lax.psum_scatter(
        pieces.reshape(n_core * n_tp, rows, columns), ("core", "tp"), scatter_dimension=0, tiled=True
    )
    results = lax.all_to_all(
        sums.reshape(n_z, capacity, columns), "z", split_axis=0, concat_axis=0, tiled=True
    ).reshape(slots, columns)

    high, low = pl.pallas_call(
        functools.partial(combiner_kernel, experts, capacity),
        out_shape=[jax.ShapeDtypeStruct((tokens, slots), bf16)] * 2,
        in_specs=[vmem] * 2,
        out_specs=[vmem] * 2,
        compiler_params=params(16),
        cost_estimate=cost(10**8, 10**6),
    )(routes_t, route_weights.T)
    routed_rows = pl.pallas_call(
        combine_kernel,
        out_shape=jax.ShapeDtypeStruct((tokens, columns), bf16),
        in_specs=[vmem] * 3,
        out_specs=vmem,
        compiler_params=params(16),
        cost_estimate=cost(10**8, 10**6),
    )(high, low, results)
    return (mixer_rows, routed_rows)


def solution(mesh):
    n_grp, n_ep, n_tp = (mesh.shape[name] for name in ("grp", "ep", "tp"))
    finer = Mesh(mesh.devices.reshape(n_grp, n_ep // 2, 2, n_tp), ("grp", "z", "core", "tp"))
    tok = ("grp", "z", "core")
    placed = (
        P(tok, "tp"),
        P(tok, "tp"),
        P(None, "tp"),
        P(),
        P(None, "tp"),
        P(tok, None),
        P(),
        P(tok, None),
        P(tok, None),
        P(("z", "core"), None, "tp"),
        P(("z", "core"), None, "tp"),
        P(("z", "core"), "tp", None),
    )
    return jax.shard_map(
        on_device,
        mesh=finer,
        in_specs=placed,
        out_specs=(P(tok, "tp"), P(tok, "tp")),
        check_vma=False,
    )
```

time: 292 us -> 238 us (0.82); the launches traced: 292 us -> 235 us
  blocking collectives: 146 us -> 56.4 us
  waiting for transfers between devices: 78.3 us -> 126 us
  matrix products: 11.7 us -> 0 us
  other arithmetic: 10.2 us -> 1.46 us
  Pallas kernels: 0 us -> 8.55 us
  starting transfers between devices: 22.2 us -> 16.3 us
    all_to_all x1, blocking collectives: 146 us -> 56.4 us  [on_device(): lax.all_to_all(outgoing.reshape(experts, capacity, columns), 'z', split_a...]
    reduce_scatter x1, waiting for transfers between devices: 12.2 us -> 70 us  [on_device(): lax.psum_scatter(pieces.reshape(n_core * n_tp, rows, columns), ('core', '...]
    all_to_all x2 -> x1, waiting for transfers between devices: 60.4 us -> 8.63 us  [on_device(): lax.all_to_all(sums.reshape(n_z, capacity, columns), 'z', split_axis=0, c...]
    all_gather x0 -> x2, waiting for transfers between devices: none -> 46.8 us  [the longest x1 46.7 us: on_device(): lax.all_gather(arrived.reshape(1, rows, columns), ('core', 'tp'), axis=0,...]
    dot_general x5 -> x0, matrix products: 11.7 us -> none  [the longest x1 6.9 us: on_device(): jnp.dot(hidden, down_w[0], preferred_element_type=jnp.float32)]
    pallas_call x0 -> x5, Pallas kernels: none -> 8.55 us  [the longest x1 4.77 us: on_device(): pl.pallas_call(experts_kernel, grid=(n_core * 2,), out_shape=jax.ShapeDty...]
    unnamed x21 -> x30, local copies, waits for them, and re-layouts: 3.72 us -> 10 us
    ppermute x3 -> x1, starting transfers between devices: 9.21 us -> 3.48 us  [on_device(): lax.ppermute(glu[length - halo:], ('z', 'core'), [(i, i + 1) for i in ran...]
  transfers between devices with their start and end apart: 6 -> 5, of which waited for: 6 -> 4; matrix products, arithmetic and copies ran while one was open for 2% -> 1% of each run, Pallas kernels for 0% -> 1%
where the time goes in v1:
time: 238 us; the launch traced here: 235 us
  waiting for transfers between devices  126 us (53%)
  blocking collectives  56.4 us (24%)
  starting transfers between devices  16.3 us (7%)
  between operations  15.7 us (7%)
  local copies, waits for them, and re-layouts  10.1 us (4%)
  Pallas kernels  8.55 us (4%)
    reduce_scatter x1, waiting for transfers between devices, on_device(): lax.psum_scatter(pieces.reshape(n_core * n_tp, rows, columns), ('core', '...  70 us
    all_to_all x1, blocking collectives, on_device(): lax.all_to_all(outgoing.reshape(experts, capacity, columns), 'z', split_a...  56.4 us
    all_gather x1, waiting for transfers between devices, on_device(): lax.all_gather(arrived.reshape(1, rows, columns), ('core', 'tp'), axis=0,...  46.7 us
    all_to_all x1, starting transfers between devices, on_device(): lax.all_to_all(sums.reshape(n_z, capacity, columns), 'z', split_axis=0, c...  12.6 us
    unnamed x30, local copies, waits for them, and re-layouts  10 us
    all_to_all x1, waiting for transfers between devices, on_device(): lax.all_to_all(sums.reshape(n_z, capacity, columns), 'z', split_axis=0, c...  8.63 us
    pallas_call x1, Pallas kernels, on_device(): pl.pallas_call(experts_kernel, grid=(n_core * 2,), out_shape=jax.ShapeDty...  4.77 us
  transfers between devices with their start and end apart: 5, of which 4 were waited for; matrix products, arithmetic and copies ran while one was open for 1% of the time, Pallas kernels for 1%

profile of v1, /device:TPU:65, one launch (start us, length us, event | category | flops | bytes accessed | tf_op | source)
XLA Modules:
  0.0 234.8 jit_solution(1009179352156533516)
XLA Ops:
  8.1 1.0 copy-done
  9.2 0.7 copy-done.1
  9.8 0.7 copy-done.2
  10.5 0.6 shard_map.133
  11.1 56.4 %all_to_all.10 = bf16[16,24,256]{2,1,0:T(8,128)(2,1)} all-to-all(bf16[16,24,256]{2,1,0:T(8,128)(2,1)S(1)} %bitcast.75), channel_id=1, replica_groups=mesh['grp'=2,'z'=16,'core'=2,'tp'=8] {'z'}, dimensions={0} | all-to-all | bytes 393216 | tf_op jit(solution)/shard_map/all_to_all | solution.py:128
  67.7 46.7 %all-gather.4.cloned.1.call-done = bf16[16,384,256]{2,1,0:T(8,128)(2,1)} async-done(((bf16[1,384,256]{2,1,0:T(8,128)(2,1)}), bf16[16,384,256]{2,1,0:T(8,128)(2,1)}) %all-gather.4.cloned.1.call-update) | async-done | bytes 3145744 | tf_op jit(solution)/shard_map/all_gather | solution.py:132
  114.4 1.9 copy-done.4
  116.3 1.2 copy-done.5
  117.5 1.2 copy-done.6
  118.7 1.2 copy-done.7
  120.0 4.8 %shard_map.134 = bf16[2,8,384,256]{3,2,1,0:T(8,128)(2,1)} custom-call(bf16[2,8,384,256]{3,2,1,0:T(8,128)(2,1)S(1)} %bitcast.79, bf16[1,2048,256]{2,1,0:T(8,128)(2,1)S(1)} %copy-done.5, bf16[1,2048,256]{2,1,0:T(8,128)(2,1)S(1)} %copy-done.6, bf16[1,256,2048]{2,1,0:T(8,128)(2,1)S(1)} %copy-done.7), custom_call_target="tpu_custom_call" | custom-call | flops 3000000000 | bytes 10000000 | tf_op jit(solution)/shard_map/pallas_call | solution.py:167
  124.8 0.1 all-gather.6.cloned.1.call-start
  124.9 0.8 copy-done.12
  125.7 0.1 multiply_convert_fusion
  125.8 3.5 %collective-permute-start = (bf16[32,128]{1,0:T(8,128)(2,1)S(1)}, bf16[32,128]{1,0:T(8,128)(2,1)S(1)}, u32[]{:S(2)}, u32[]{:S(2)}) collective-permute-start(bf16[32,128]{1,0:T(8,128)(2,1)S(1)} %slice.252), channel_id=1, source_target_pairs={{0,8},{8,16},{16,24},{24,32},{32,40},{40,48},{48,56},{56,64},{64,7... | collective-permute-start | bytes 24584 | tf_op jit(solution)/shard_map/ppermute | solution.py:139
  129.3 0.7 collective-permute-done
  130.1 1.4 fusion.1
  131.5 70.0 %reduce-scatter.2.cloned.1.call-done = bf16[1,384,256]{2,1,0:T(8,128)(2,1)} async-done(((bf16[16,384,256]{2,1,0:T(8,128)(2,1)}), bf16[1,384,256]{2,1,0:T(8,128)(2,1)}) %reduce-scatter.2.cloned.1.call-update) | async-done | bytes 196624 | tf_op jit(solution)/shard_map/reduce_scatter | solution.py:181
  201.5 12.6 %all-to-all-start.1 = ((bf16[16,24,256]{2,1,0:T(8,128)(2,1)}), bf16[16,24,256]{2,1,0:T(8,128)(2,1)S(1)}, u32[]{:S(2)}, u32[]{:S(2)}) async-start(bf16[16,24,256]{2,1,0:T(8,128)(2,1)} %bitcast.84), calls=%async_computation.2 | async-start | bytes 393216 | tf_op jit(solution)/shard_map/all_to_all | solution.py:184
  214.2 0.4 shard_map.132
  214.7 1.2 copy-done.8
  215.9 1.9 shard_map.131
  217.8 8.6 %all-to-all-done.1 = bf16[16,24,256]{2,1,0:T(8,128)(2,1)S(1)} async-done(((bf16[16,24,256]{2,1,0:T(8,128)(2,1)}), bf16[16,24,256]{2,1,0:T(8,128)(2,1)S(1)}, u32[]{:S(2)}, u32[]{:S(2)}) %all-to-all-start.1) | async-done | bytes 196640 | tf_op jit(solution)/shard_map/all_to_all | solution.py:184
  226.4 0.9 shard_map.135
  (31 shorter events, 0.5 us)
Async XLA Ops:
  8.0 106.4 %all-gather.4.cloned.1.call-start = ((), (), s32[]{:S(2)}) async-start(), calls=%async_computation.3 | async-start | bytes 3342336 | tf_op jit(solution)/shard_map/all_gather | solution.py:132
  8.1 1.0 copy-start
  9.2 0.7 copy-start.1
  9.8 0.7 copy-start.2
  67.6 134.0 %reduce-scatter.2.cloned.1.call-start = ((), (), s32[]{:S(2)}) async-start(), calls=%async_computation.4 | async-start | bytes 3342336 | tf_op jit(solution)/shard_map/reduce_scatter | solution.py:181
  114.4 1.9 copy-start.4
  116.3 1.2 copy-start.5
  117.5 1.2 copy-start.6
  118.7 1.2 copy-start.7
  124.7 0.9 copy-start.12
  124.7 1.0 copy-start.13
  124.7 4.5 %copy-start.14 = (f32[31,128]{1,0:T(8,128)S(1)}, f32[31,128]{1,0:T(8,128)}, u32[]{:S(2)}) copy-start(f32[31,128]{1,0:T(8,128)} %param.14) | copy-start | bytes 47620
  124.8 89.8 %all-gather.6.cloned.1.call-start = ((), (), s32[]{:S(2)}) async-start(), calls=%async_computation.5 | async-start | bytes 1179648 | tf_op jit(solution)/shard_map/all_gather | solution.py:148
  125.8 4.3 %collective-permute-start = (bf16[32,128]{1,0:T(8,128)(2,1)S(1)}, bf16[32,128]{1,0:T(8,128)(2,1)S(1)}, u32[]{:S(2)}, u32[]{:S(2)}) collective-permute-start(bf16[32,128]{1,0:T(8,128)(2,1)S(1)} %slice.252), channel_id=1, source_target_pairs={{0,8},{8,16},{16,24},{24,32},{32,40},{40,48},{48,56},{56,64},{64,7... | collective-permute-start | bytes 24584 | tf_op jit(solution)/shard_map/ppermute | solution.py:139
  130.1 84.1 %copy-start.3 = (s32[128,2]{0,1:T(2,128)S(1)}, s32[128,2]{0,1:T(2,128)}, u32[]{:S(2)}) copy-start(s32[128,2]{0,1:T(2,128)} %param.19) | copy-start | bytes 3076
  130.1 84.1 %copy-start.11 = (f32[128,2]{0,1:T(2,128)S(1)}, f32[128,2]{0,1:T(2,128)}, u32[]{:S(2)}) copy-start(f32[128,2]{0,1:T(2,128)} %param.20) | copy-start | bytes 3076
  130.1 84.6 %copy-start.9 = (bf16[1024,256]{1,0:T(8,128)(2,1)S(1)}, bf16[1024,256]{1,0:T(8,128)(2,1)}, u32[]{:S(2)}) copy-start(bf16[1024,256]{1,0:T(8,128)(2,1)} %weight.1) | copy-start | bytes 1572868
  130.1 84.6 %copy-start.10 = (f32[1024]{0:T(1024)S(1)}, f32[1024]{0:T(1024)}, u32[]{:S(2)}) copy-start(f32[1024]{0:T(1024)} %param.15) | copy-start | bytes 12292
  201.5 24.9 %all-to-all-start.1 = ((bf16[16,24,256]{2,1,0:T(8,128)(2,1)}), bf16[16,24,256]{2,1,0:T(8,128)(2,1)S(1)}, u32[]{:S(2)}, u32[]{:S(2)}) async-start(bf16[16,24,256]{2,1,0:T(8,128)(2,1)} %bitcast.84), calls=%async_computation.2 | async-start | bytes 393216 | tf_op jit(solution)/shard_map/all_to_all | solution.py:184
  214.7 1.2 copy-start.8
Sparse Core Ops, SparseCore 0:
  67.7 46.6 all-gather.3
  124.9 76.5 reduce-scatter.1
Sparse Core Ops, SparseCore 1:
  131.6 43.8 all-gather.5

commit v2 on v1

--- a/solution.py
+++ b/solution.py
@@ -61,19 +61,37 @@
     out[...] = (dot(high[...], results[...]) + dot(low[...], results[...])).astype(bf16)
 
 
-def experts_kernel(x, gate_w, up_w, down_w, out):
-    blocks, width = x.shape[1], x.shape[3]
-    gate = up = None
+def experts_kernel(x, gate_0, up_0, gate_1, up_1, down_0, down_1, out, wide, tall, sems):
+    blocks, width = x.shape[0], x.shape[2]
+    span = lambda b: slice(b * width, (b + 1) * width)
+    held = [wide.at[i] for i in range(4)] + [tall.at[i] for i in range(2)]
+    weights = (gate_0, up_0, gate_1, up_1, down_0, down_1)
+    copies = [
+        pltpu.make_async_copy(w.at[0], h, sems.at[i]) for i, (w, h) in enumerate(zip(weights, held))
+    ]
+    for copy in copies:
+        copy.start()
+
+    def projected(i):
+        copies[i].wait()
+        return functools.reduce(jnp.add, [dot(x[b], held[i][span(b), :]) for b in range(blocks)])
+
+    hidden = []
+    for half in range(2):
+        gate = projected(2 * half)
+        hidden.append((jax.nn.silu(gate) * projected(2 * half + 1)).astype(bf16))
+    copies[4].wait()
+    copies[5].wait()
     for b in range(blocks):
-        part = x[0, b]
-        g = dot(part, gate_w[0, b * width : (b + 1) * width, :])
-        u = dot(part, up_w[0, b * width : (b + 1) * width, :])
-        gate = g if gate is None else gate + g
-        up = u if up is None else up + u
-    hidden = (jax.nn.silu(gate) * up).astype(bf16)
-    for b in range(blocks):
-        piece = dot(hidden, down_w[0, :, b * width : (b + 1) * width])
-        out[0, b] = piece.astype(bf16)
+        piece = dot(hidden[0], held[4][:, span(b)]) + dot(hidden[1], held[5][:, span(b)])
+        out[b] = piece.astype(bf16)
+
+
+def sum_kernel(pieces, out):
+    total = pieces[0].astype(f32)
+    for b in range(1, pieces.shape[0]):
+        total = total + pieces[b].astype(f32)
+    out[...] = total.astype(bf16)
 
 
 def mixer_kernel(x, gain, weight, out):
@@ -82,6 +100,15 @@
     scale = lax.rsqrt(jnp.mean(centered * centered, axis=-1, keepdims=True) + eps)
     activated = jax.nn.silu(centered * scale * gain[...]).astype(bf16)
     out[...] = dot(activated, weight[...]).astype(bf16)
+
+
+def from_each(value, axis):
+    copies = jnp.broadcast_to(value, (lax.axis_size(axis), *value.shape))
+    return lax.all_to_all(copies, axis, split_axis=0, concat_axis=0, tiled=True)
+
+
+def partner(value):
+    return lax.ppermute(value, "core", [(0, 1), (1, 0)])
 
 
 def params(mib):
@@ -129,7 +156,7 @@
         outgoing.reshape(experts, capacity, columns), "z", split_axis=0, concat_axis=0, tiled=True
     )
     rows = n_z * capacity
-    incoming = lax.all_gather(arrived.reshape(1, rows, columns), ("core", "tp"), axis=0, tiled=True)
+    gate_b, up_b, down_b = (partner(w) for w in (gate_w, up_w, down_w))
 
     taps = conv_taps.shape[0]
     halo = -(-(taps - 1) // 16) * 16
@@ -145,7 +172,11 @@
         start = halo - taps + 1 + offset
         total = total + conv_taps[offset][None, :] * padded[start : start + length]
     convolved = total.astype(bf16)
-    gathered = lax.all_gather(convolved, "tp", axis=0, tiled=False)
+    gathered = from_each(convolved, "tp")
+    arrived, gathered, gate_b, up_b, down_b = lax.optimization_barrier(
+        (arrived, gathered, gate_b, up_b, down_b)
+    )
+    incoming = from_each(arrived.reshape(rows, columns), "tp")
     step = length // 2
     mixer_rows = pl.pallas_call(
         mixer_kernel,
@@ -161,26 +192,32 @@
         cost_estimate=cost(10**9, 2 * 10**6),
     )(gathered, chan_gain.reshape(1, -1), out_weight)
 
-    step = rows // 2
-    block = (1, n_tp, step, columns)
-    whole = lambda i: (0, 0, 0)
+    hbm = pl.BlockSpec(memory_space=pl.ANY)
+    units = gate_w.shape[2]
     pieces = pl.pallas_call(
         experts_kernel,
-        grid=(n_core * 2,),
-        out_shape=jax.ShapeDtypeStruct((n_core, n_tp, rows, columns), bf16),
-        in_specs=[
-            pl.BlockSpec(block, lambda i: (i // 2, 0, i % 2, 0)),
-            pl.BlockSpec(gate_w.shape, whole),
-            pl.BlockSpec(up_w.shape, whole),
-            pl.BlockSpec(down_w.shape, whole),
+        out_shape=jax.ShapeDtypeStruct((n_tp, rows, columns), bf16),
+        in_specs=[vmem] + [hbm] * 6,
+        out_specs=vmem,
+        scratch_shapes=[
+            pltpu.VMEM((4, width, units), bf16),
+            pltpu.VMEM((2, units, width), bf16),
+            pltpu.SemaphoreType.DMA((6,)),
         ],
-        out_specs=pl.BlockSpec(block, lambda i: (i // 2, 0, i % 2, 0)),
-        compiler_params=params(24),
+        compiler_params=params(56),
         cost_estimate=cost(3 * 10**9, 10**7),
-    )(incoming.reshape(n_core, n_tp, rows, columns), gate_w, up_w, down_w)
-    sums = lax.psum_scatter(
-        pieces.reshape(n_core * n_tp, rows, columns), ("core", "tp"), scatter_dimension=0, tiled=True
-    )
+    )(incoming, gate_w, up_w, gate_b, up_b, down_w, down_b)
+    pieces = lax.all_to_all(pieces, "tp", split_axis=0, concat_axis=0, tiled=True)
+    step = rows // 2
+    sums = pl.pallas_call(
+        sum_kernel,
+        grid=(rows // step,),
+        out_shape=jax.ShapeDtypeStruct((rows, columns), bf16),
+        in_specs=[pl.BlockSpec((n_tp, step, columns), lambda i: (0, i, 0))],
+        out_specs=pl.BlockSpec((step, columns), lambda i: (i, 0)),
+        compiler_params=params(16),
+        cost_estimate=cost(10**8, 2 * 10**6),
+    )(pieces)
     results = lax.all_to_all(
         sums.reshape(n_z, capacity, columns), "z", split_axis=0, concat_axis=0, tiled=True
     ).reshape(slots, columns)

time: 238 us -> 225 us (0.945)
  waiting for transfers between devices: 126 us -> 42.8 us
  starting transfers between devices: 16.3 us -> 67 us
  blocking collectives: 56.4 us -> 87.1 us
  between operations: 15.7 us -> 0.81 us
  Pallas kernels: 8.55 us -> 14.2 us
  local copies, waits for them, and re-layouts: 10.1 us -> 7.1 us
    reduce_scatter x1 -> x0, waiting for transfers between devices: 70 us -> none  [on_device(): lax.psum_scatter(pieces.reshape(n_core * n_tp, rows, columns), ('core', '...]
    all_to_all x0 -> x2, starting transfers between devices: none -> 47.8 us  [the longest x1 40.8 us: on_device(): lax.all_to_all(outgoing.reshape(experts, capacity, columns), 'z', split_a...]
    all_gather x2 -> x0, waiting for transfers between devices: 46.8 us -> none  [the longest x1 46.7 us: on_device(): lax.all_gather(arrived.reshape(1, rows, columns), ('core', 'tp'), axis=0,...]
    all_to_all x0 -> x2, waiting for transfers between devices: none -> 31.7 us  [the longest x1 19.4 us: from_each(): return lax.all_to_all(copies, axis, split_axis=0, concat_axis=0, tiled=True)]
    all_to_all x1 -> x2, blocking collectives: 56.4 us -> 87.1 us  [the longest x1 43.6 us: from_each(): return lax.all_to_all(copies, axis, split_axis=0, concat_axis=0, tiled=True)]
    all_to_all x1, starting transfers between devices: 12.6 us -> 5.76 us  [on_device(): lax.all_to_all(sums.reshape(n_z, capacity, columns), 'z', split_axis=0, c...]
    ppermute x0 -> x3, starting transfers between devices: none -> 6.34 us  [partner(): return lax.ppermute(value, 'core', [(0, 1), (1, 0)])]
    unnamed x30 -> x20, local copies, waits for them, and re-layouts: 10 us -> 3.89 us
  transfers between devices with their start and end apart: 5 -> 7, of which waited for: 4 -> 5; matrix products, arithmetic and copies ran while one was open for 1% -> 1% of each run, Pallas kernels for 1% -> 2%
where the time goes in v2:
time: 225 us; the launch traced here: 221 us
  blocking collectives  87.1 us (39%)
  starting transfers between devices  67 us (30%)
  waiting for transfers between devices  42.8 us (19%)
  Pallas kernels  14.2 us (6%)
  local copies, waits for them, and re-layouts  7.1 us (3%)
    all_to_all x1, blocking collectives, from_each(): return lax.all_to_all(copies, axis, split_axis=0, concat_axis=0, tiled=True)  43.6 us
    all_to_all x1, blocking collectives, on_device(): lax.all_to_all(pieces, 'tp', split_axis=0, concat_axis=0, tiled=True)  43.5 us
    all_to_all x1, starting transfers between devices, on_device(): lax.all_to_all(outgoing.reshape(experts, capacity, columns), 'z', split_a...  40.8 us
    all_to_all x1, waiting for transfers between devices, from_each(): return lax.all_to_all(copies, axis, split_axis=0, concat_axis=0, tiled=True)  19.4 us
    all_to_all x1, waiting for transfers between devices, on_device(): lax.all_to_all(outgoing.reshape(experts, capacity, columns), 'z', split_a...  12.3 us
    all_to_all x1, waiting for transfers between devices, on_device(): lax.all_to_all(sums.reshape(n_z, capacity, columns), 'z', split_axis=0, c...  9.66 us
    pallas_call x1, Pallas kernels, on_device(): pl.pallas_call(experts_kernel, out_shape=jax.ShapeDtypeStruct((n_tp, rows...  8.66 us
    ppermute x1, starting transfers between devices, on_device(): lax.ppermute(glu[length - halo:], ('z', 'core'), [(i, i + 1) for i in ran...  7.06 us
  transfers between devices with their start and end apart: 7, of which 5 were waited for; matrix products, arithmetic and copies ran while one was open for 1% of the time, Pallas kernels for 2%

profile of v2, /device:TPU:65, one launch (start us, length us, event | category | flops | bytes accessed | tf_op | source)
XLA Modules:
  0.0 220.7 jit_solution(9204346764599740018)
XLA Ops:
  0.6 1.0 multiply_convert_fusion
  1.7 7.1 %collective-permute-start = (bf16[32,128]{1,0:T(8,128)(2,1)S(1)}, bf16[32,128]{1,0:T(8,128)(2,1)S(1)}, u32[]{:S(2)}, u32[]{:S(2)}) collective-permute-start(bf16[32,128]{1,0:T(8,128)(2,1)S(1)} %slice.252), channel_id=1, source_target_pairs={{0,8},{8,16},{16,24},{24,32},{32,40},{40,48},{48,56},{56,64},{64,7... | collective-permute-start | bytes 24584 | tf_op jit(solution)/shard_map/ppermute | solution.py:166
  8.8 1.0 copy-done
  11.2 1.2 shard_map.131
  12.4 40.8 %all-to-all-start = ((bf16[16,24,256]{2,1,0:T(8,128)(2,1)}), bf16[16,24,256]{2,1,0:T(8,128)(2,1)S(1)}, u32[]{:S(2)}, u32[]{:S(2)}) async-start(bf16[16,24,256]{2,1,0:T(8,128)(2,1)} %bitcast.3), calls=%async_computation | async-start | bytes 393216 | tf_op jit(solution)/shard_map/all_to_all | solution.py:155
  53.2 1.0 slice_bitcast_fusion.30
  54.2 1.0 slice_bitcast_fusion.29
  55.9 12.3 %all-to-all-done = bf16[16,24,256]{2,1,0:T(8,128)(2,1)S(1)} async-done(((bf16[16,24,256]{2,1,0:T(8,128)(2,1)}), bf16[16,24,256]{2,1,0:T(8,128)(2,1)S(1)}, u32[]{:S(2)}, u32[]{:S(2)}) %all-to-all-start) | async-done | bytes 196640 | tf_op jit(solution)/shard_map/all_to_all | solution.py:155
  68.2 1.1 broadcast_in_dim.6
  69.4 7.0 %all-to-all-start.1 = ((bf16[8,512,128]{2,1,0:T(8,128)(2,1)}), bf16[8,512,128]{2,1,0:T(8,128)(2,1)S(1)}, u32[]{:S(2)}, u32[]{:S(2)}) async-start(bf16[8,512,128]{2,1,0:T(8,128)(2,1)} %broadcast_in_dim.6), calls=%async_computation.1 | async-start | bytes 2097152 | tf_op jit(solution)/shard_map/all_to_all | solution.py:107
  76.4 2.0 collective-permute-start.1
  78.4 2.4 %collective-permute-start.2 = (bf16[1,2048,256]{2,1,0:T(8,128)(2,1)}, bf16[1,2048,256]{2,1,0:T(8,128)(2,1)S(1)}, u32[]{:S(2)}, u32[]{:S(2)}) collective-permute-start(bf16[1,2048,256]{2,1,0:T(8,128)(2,1)} %up_0.1), channel_id=1, source_target_pairs={{0,8},{8,0},{1,9},{9,1},{2,10},{10,2},{3,11},{11,3},{4,12},{12,4},... | collective-permute-start | bytes 3145736 | tf_op jit(solution)/shard_map/ppermute | solution.py:111
  80.8 2.0 collective-permute-start.3
  83.8 1.0 copy-done.9
  84.7 1.0 collective-permute-done.3.down_1
  85.7 19.4 %all-to-all-done.1.x = bf16[8,512,128]{2,1,0:T(8,128)(2,1)S(1)} async-done(((bf16[8,512,128]{2,1,0:T(8,128)(2,1)}), bf16[8,512,128]{2,1,0:T(8,128)(2,1)S(1)}, u32[]{:S(2)}, u32[]{:S(2)}) %all-to-all-start.1) | async-done | bytes 1048608 | tf_op jit(solution)/shard_map/all_to_all | solution.py:107
  105.2 43.6 %all_to_all.25.x = bf16[8,384,256]{2,1,0:T(8,128)(2,1)} all-to-all(bf16[8,384,256]{2,1,0:T(8,128)(2,1)S(1)} %broadcast_in_dim.7), channel_id=1, replica_groups=mesh['grp'=2,'z'=16,'core'=2,'tp'=8] {'tp'}, dimensions={0} | all-to-all | bytes 3145728 | tf_op jit(solution)/shard_map/all_to_all | solution.py:107
  148.8 8.7 %shard_map.134 = bf16[8,384,256]{2,1,0:T(8,128)(2,1)} custom-call(bf16[8,384,256]{2,1,0:T(8,128)(2,1)} %all_to_all.25.x, bf16[1,2048,256]{2,1,0:T(8,128)(2,1)} %gate_0.1, bf16[1,2048,256]{2,1,0:T(8,128)(2,1)} %up_0.1, bf16[1,2048,256]{2,1,0:T(8,128)(2,1)} %copy-done.8, bf16[1,2048,256]{2,1,0:T(8,128)(2,1)} %copy-done.9, bf16[1,256,2048]{2,1,0:T(8,128)(2,1)} %down_0.1, ...), custom_call_target="tpu_custom_call" | custom-call | flops 3000000000 | bytes 10000000 | tf_op jit(solution)/shard_map/pallas_call | solution.py:197
  157.5 43.5 %all_to_all.26.pieces = bf16[8,384,256]{2,1,0:T(8,128)(2,1)S(1)} all-to-all(bf16[8,384,256]{2,1,0:T(8,128)(2,1)} %shard_map.134), channel_id=1, replica_groups=mesh['grp'=2,'z'=16,'core'=2,'tp'=8] {'tp'}, dimensions={0} | all-to-all | bytes 3145728 | tf_op jit(solution)/shard_map/all_to_all | solution.py:210
  201.0 1.0 shard_map.135
  202.0 5.8 %all-to-all-start.4 = ((bf16[16,24,256]{2,1,0:T(8,128)(2,1)}), bf16[16,24,256]{2,1,0:T(8,128)(2,1)S(1)}, u32[]{:S(2)}, u32[]{:S(2)}) async-start(bf16[16,24,256]{2,1,0:T(8,128)(2,1)} %bitcast.38), calls=%async_computation.4 | async-start | bytes 393216 | tf_op jit(solution)/shard_map/all_to_all | solution.py:221
  208.2 1.9 shard_map.132
  210.2 9.7 %all-to-all-done.4 = bf16[16,24,256]{2,1,0:T(8,128)(2,1)S(1)} async-done(((bf16[16,24,256]{2,1,0:T(8,128)(2,1)}), bf16[16,24,256]{2,1,0:T(8,128)(2,1)S(1)}, u32[]{:S(2)}, u32[]{:S(2)}) %all-to-all-start.4) | async-done | bytes 196640 | tf_op jit(solution)/shard_map/all_to_all | solution.py:221
  219.8 0.9 shard_map.136
  (26 shorter events, 3.6 us)
Async XLA Ops:
  1.7 53.5 %collective-permute-start = (bf16[32,128]{1,0:T(8,128)(2,1)S(1)}, bf16[32,128]{1,0:T(8,128)(2,1)S(1)}, u32[]{:S(2)}, u32[]{:S(2)}) collective-permute-start(bf16[32,128]{1,0:T(8,128)(2,1)S(1)} %slice.252), channel_id=1, source_target_pairs={{0,8},{8,16},{16,24},{24,32},{32,40},{40,48},{48,56},{56,64},{64,7... | collective-permute-start | bytes 24584 | tf_op jit(solution)/shard_map/ppermute | solution.py:166
  8.8 1.0 copy-start
  9.8 0.7 copy-start.1
  10.5 0.7 copy-start.2
  12.4 55.8 %all-to-all-start = ((bf16[16,24,256]{2,1,0:T(8,128)(2,1)}), bf16[16,24,256]{2,1,0:T(8,128)(2,1)S(1)}, u32[]{:S(2)}, u32[]{:S(2)}) async-start(bf16[16,24,256]{2,1,0:T(8,128)(2,1)} %bitcast.3), calls=%async_computation | async-start | bytes 393216 | tf_op jit(solution)/shard_map/all_to_all | solution.py:155
  55.9 20.5 %copy-start.7 = (bf16[1,2048,256]{2,1,0:T(8,128)(2,1)S(1)}, bf16[1,2048,256]{2,1,0:T(8,128)(2,1)}, u32[]{:S(2)}) copy-start(bf16[1,2048,256]{2,1,0:T(8,128)(2,1)} %gate_0.1) | copy-start | bytes 3145732
  69.4 35.8 %all-to-all-start.1 = ((bf16[8,512,128]{2,1,0:T(8,128)(2,1)}), bf16[8,512,128]{2,1,0:T(8,128)(2,1)S(1)}, u32[]{:S(2)}, u32[]{:S(2)}) async-start(bf16[8,512,128]{2,1,0:T(8,128)(2,1)} %broadcast_in_dim.6), calls=%async_computation.1 | async-start | bytes 2097152 | tf_op jit(solution)/shard_map/all_to_all | solution.py:107
  76.4 6.4 %collective-permute-start.1 = (bf16[1,2048,256]{2,1,0:T(8,128)(2,1)S(1)}, bf16[1,2048,256]{2,1,0:T(8,128)(2,1)S(1)}, u32[]{:S(2)}, u32[]{:S(2)}) collective-permute-start(bf16[1,2048,256]{2,1,0:T(8,128)(2,1)S(1)} %copy-done.7), channel_id=1, source_target_pairs={{0,8},{8,0},{1,9},{9,1},{2,10},{10,2},{3,11},{11,3},{4,12},{12,4},... | collective-permute-start | bytes 3145736 | tf_op jit(solution)/shard_map/ppermute | solution.py:111
  78.4 4.9 %collective-permute-start.2 = (bf16[1,2048,256]{2,1,0:T(8,128)(2,1)}, bf16[1,2048,256]{2,1,0:T(8,128)(2,1)S(1)}, u32[]{:S(2)}, u32[]{:S(2)}) collective-permute-start(bf16[1,2048,256]{2,1,0:T(8,128)(2,1)} %up_0.1), channel_id=1, source_target_pairs={{0,8},{8,0},{1,9},{9,1},{2,10},{10,2},{3,11},{11,3},{4,12},{12,4},... | collective-permute-start | bytes 3145736 | tf_op jit(solution)/shard_map/ppermute | solution.py:111
  80.8 4.9 %collective-permute-start.3 = (bf16[1,256,2048]{2,1,0:T(8,128)(2,1)}, bf16[1,256,2048]{2,1,0:T(8,128)(2,1)}, u32[]{:S(2)}, u32[]{:S(2)}) collective-permute-start(bf16[1,256,2048]{2,1,0:T(8,128)(2,1)} %down_0.1), channel_id=1, source_target_pairs={{0,8},{8,0},{1,9},{9,1},{2,10},{10,2},{3,11},{11,3},{4,12},{12,4},... | collective-permute-start | bytes 3145736 | tf_op jit(solution)/shard_map/ppermute | solution.py:111
  82.8 1.0 copy-start.8
  83.8 1.0 copy-start.9
  200.9 6.8 %copy-start.3 = (s32[128,2]{0,1:T(2,128)S(1)}, s32[128,2]{0,1:T(2,128)}, u32[]{:S(2)}) copy-start(s32[128,2]{0,1:T(2,128)} %param.19) | copy-start | bytes 3076
  200.9 6.8 %copy-start.6 = (f32[128,2]{0,1:T(2,128)S(1)}, f32[128,2]{0,1:T(2,128)}, u32[]{:S(2)}) copy-start(f32[128,2]{0,1:T(2,128)} %param.20) | copy-start | bytes 3076
  201.0 7.3 %copy-start.4 = (bf16[1024,256]{1,0:T(8,128)(2,1)S(1)}, bf16[1024,256]{1,0:T(8,128)(2,1)}, u32[]{:S(2)}) copy-start(bf16[1024,256]{1,0:T(8,128)(2,1)} %weight.1) | copy-start | bytes 1572868
  201.0 7.3 %copy-start.5 = (f32[1024]{0:T(1024)S(1)}, f32[1024]{0:T(1024)}, u32[]{:S(2)}) copy-start(f32[1024]{0:T(1024)} %param.15) | copy-start | bytes 12292
  202.0 17.9 %all-to-all-start.4 = ((bf16[16,24,256]{2,1,0:T(8,128)(2,1)}), bf16[16,24,256]{2,1,0:T(8,128)(2,1)S(1)}, u32[]{:S(2)}, u32[]{:S(2)}) async-start(bf16[16,24,256]{2,1,0:T(8,128)(2,1)} %bitcast.38), calls=%async_computation.4 | async-start | bytes 393216 | tf_op jit(solution)/shard_map/all_to_all | solution.py:221

commit v3 on v2

--- a/solution.py
+++ b/solution.py
@@ -7,6 +7,7 @@
 from jax.experimental.pallas import tpu as pltpu
 from jax.sharding import Mesh
 from jax.sharding import PartitionSpec as P
+
 
 eps = 1e-06
 f32 = jnp.float32
@@ -61,9 +62,10 @@
     out[...] = (dot(high[...], results[...]) + dot(low[...], results[...])).astype(bf16)
 
 
-def experts_kernel(x, gate_0, up_0, gate_1, up_1, down_0, down_1, out, wide, tall, sems):
-    blocks, width = x.shape[0], x.shape[2]
-    span = lambda b: slice(b * width, (b + 1) * width)
+def experts_kernel(
+    index, x_0, x_1, x_3, x_2a, x_2b, gate_0, up_0, gate_1, up_1, down_0, down_1, out, wide, tall, sems
+):
+    blocks, width = out.shape[0], out.shape[2]
     held = [wide.at[i] for i in range(4)] + [tall.at[i] for i in range(2)]
     weights = (gate_0, up_0, gate_1, up_1, down_0, down_1)
     copies = [
@@ -71,10 +73,17 @@
     ]
     for copy in copies:
         copy.start()
+    depth = x_0.shape[1]
+    parts = wide.shape[1] // depth
+    rows = (x_0[...], x_1[...], jnp.concatenate([x_2a[...], x_2b[...]], axis=0), x_3[...])
+    places = [lax.rem(index[0] + k, parts) * depth for k in range(parts)]
 
     def projected(i):
         copies[i].wait()
-        return functools.reduce(jnp.add, [dot(x[b], held[i][span(b), :]) for b in range(blocks)])
+        terms = [
+            dot(r, held[i][pl.ds(pl.multiple_of(p, depth), depth), :]) for r, p in zip(rows, places)
+        ]
+        return functools.reduce(jnp.add, terms)
 
     hidden = []
     for half in range(2):
@@ -83,7 +92,8 @@
     copies[4].wait()
     copies[5].wait()
     for b in range(blocks):
-        piece = dot(hidden[0], held[4][:, span(b)]) + dot(hidden[1], held[5][:, span(b)])
+        span = slice(b * width, (b + 1) * width)
+        piece = dot(hidden[0], held[4][:, span]) + dot(hidden[1], held[5][:, span])
         out[b] = piece.astype(bf16)
 
 
@@ -94,17 +104,24 @@
     out[...] = total.astype(bf16)
 
 
-def mixer_kernel(x, gain, weight, out):
-    values = jnp.concatenate([x[b] for b in range(x.shape[0])], axis=1).astype(f32)
+def mixer_kernel(index, *refs):
+    *pieces, gain, weight, out = refs
+    n, width = len(pieces), pieces[0].shape[1]
+    values = jnp.concatenate([p[...] for p in pieces], axis=1).astype(f32)
+    spans = [
+        pl.ds(pl.multiple_of(lax.rem(index[0] + n - k, n) * width, width), width) for k in range(n)
+    ]
+    gains = jnp.concatenate([gain[:, span] for span in spans], axis=1)
+    weights = jnp.concatenate([weight[span, :] for span in spans], axis=0)
     centered = values - jnp.mean(values, axis=-1, keepdims=True)
     scale = lax.rsqrt(jnp.mean(centered * centered, axis=-1, keepdims=True) + eps)
-    activated = jax.nn.silu(centered * scale * gain[...]).astype(bf16)
-    out[...] = dot(activated, weight[...]).astype(bf16)
-
-
-def from_each(value, axis):
-    copies = jnp.broadcast_to(value, (lax.axis_size(axis), *value.shape))
-    return lax.all_to_all(copies, axis, split_axis=0, concat_axis=0, tiled=True)
+    activated = jax.nn.silu(centered * scale * gains).astype(bf16)
+    out[...] = dot(activated, weights).astype(bf16)
+
+
+def moved(value, by):
+    n = lax.axis_size("tp")
+    return lax.ppermute(value, "tp", [(i, (i + by) % n) for i in range(n)])
 
 
 def partner(value):
@@ -119,7 +136,7 @@
     return pl.CostEstimate(flops=flops, bytes_accessed=moved, transcendentals=0)
 
 
-def on_device(
+def step_on_device(
     value_in,
     gate_in,
     conv_taps,
@@ -144,20 +161,24 @@
     smem = pl.BlockSpec(memory_space=pltpu.SMEM)
 
     routes_t = routes.T
+    me = lax.axis_index("tp")
+    parts = n_tp // 2
+    wide = width // parts
+    quarter = lax.rem(me, parts).astype(jnp.int32).reshape(1)
     outgoing = pl.pallas_call(
         functools.partial(dispatch_kernel, experts, capacity),
-        out_shape=jax.ShapeDtypeStruct((slots, columns), bf16),
-        in_specs=[smem, vmem, vmem, vmem],
-        out_specs=vmem,
-        compiler_params=params(16),
+        grid=(1,),
+        out_shape=jax.ShapeDtypeStruct((slots, wide), bf16),
+        in_specs=[smem] + [pl.BlockSpec(s, lambda i: (0, 0)) for s in ((top, tokens), (tokens, width), (1, width))],
+        out_specs=pl.BlockSpec((slots, wide), lambda i: (0, 0)),
+        compiler_params=params(60),
         cost_estimate=cost(10**8, 10**6),
-    )(lax.axis_index("tp").reshape(1), routes_t, second_rows, expert_gain.reshape(1, -1))
+    )(quarter, routes_t, second_rows, expert_gain.reshape(1, -1))
     arrived = lax.all_to_all(
-        outgoing.reshape(experts, capacity, columns), "z", split_axis=0, concat_axis=0, tiled=True
-    )
-    rows = n_z * capacity
-    gate_b, up_b, down_b = (partner(w) for w in (gate_w, up_w, down_w))
-
+        outgoing.reshape(experts, capacity, wide), "z", split_axis=0, concat_axis=0, tiled=True
+    )
+
+    value_in, gate_in, outgoing = lax.optimization_barrier((value_in, gate_in, outgoing))
     taps = conv_taps.shape[0]
     halo = -(-(taps - 1) // 16) * 16
     glu = (value_in.astype(f32) * jax.nn.sigmoid(gate_in.astype(f32))).astype(bf16)
@@ -172,41 +193,31 @@
         start = halo - taps + 1 + offset
         total = total + conv_taps[offset][None, :] * padded[start : start + length]
     convolved = total.astype(bf16)
-    gathered = from_each(convolved, "tp")
-    arrived, gathered, gate_b, up_b, down_b = lax.optimization_barrier(
-        (arrived, gathered, gate_b, up_b, down_b)
-    )
-    incoming = from_each(arrived.reshape(rows, columns), "tp")
-    step = length // 2
-    mixer_rows = pl.pallas_call(
-        mixer_kernel,
-        grid=(length // step,),
-        out_shape=jax.ShapeDtypeStruct((length, out_weight.shape[1]), bf16),
-        in_specs=[
-            pl.BlockSpec((n_tp, step, channels), lambda i: (0, i, 0)),
-            pl.BlockSpec((1, n_tp * channels), lambda i: (0, 0)),
-            pl.BlockSpec(out_weight.shape, lambda i: (0, 0)),
-        ],
-        out_specs=pl.BlockSpec((step, out_weight.shape[1]), lambda i: (i, 0)),
-        compiler_params=params(16),
-        cost_estimate=cost(10**9, 2 * 10**6),
-    )(gathered, chan_gain.reshape(1, -1), out_weight)
-
+    from_back = [moved(convolved, k) for k in range(1, parts)]
+    from_front = [moved(convolved, -k) for k in range(1, parts)]
+
+    rows = n_z * capacity
+    arrived, from_back, from_front = lax.optimization_barrier((arrived, from_back, from_front))
+    x_0 = arrived.reshape(rows, wide)
+    x_2a, x_2b = moved(x_0[: rows // 2], -2), moved(x_0[rows // 2 :], 2)
+    x_1, x_3 = moved(x_0, -1), moved(x_0, 1)
+    own = lax.optimization_barrier((x_0, gate_w, up_w, down_w))
+    gate_b, up_b, down_b = (partner(w) for w in own[1:])
     hbm = pl.BlockSpec(memory_space=pl.ANY)
     units = gate_w.shape[2]
     pieces = pl.pallas_call(
         experts_kernel,
         out_shape=jax.ShapeDtypeStruct((n_tp, rows, columns), bf16),
-        in_specs=[vmem] + [hbm] * 6,
+        in_specs=[smem] + [vmem] * 5 + [hbm] * 6,
         out_specs=vmem,
         scratch_shapes=[
             pltpu.VMEM((4, width, units), bf16),
             pltpu.VMEM((2, units, width), bf16),
             pltpu.SemaphoreType.DMA((6,)),
         ],
-        compiler_params=params(56),
+        compiler_params=params(24),
         cost_estimate=cost(3 * 10**9, 10**7),
-    )(incoming, gate_w, up_w, gate_b, up_b, down_w, down_b)
+    )(quarter, x_0, x_1, x_3, x_2a, x_2b, gate_w, up_w, gate_b, up_b, down_w, down_b)
     pieces = lax.all_to_all(pieces, "tp", split_axis=0, concat_axis=0, tiled=True)
     step = rows // 2
     sums = pl.pallas_call(
@@ -218,6 +229,8 @@
         compiler_params=params(16),
         cost_estimate=cost(10**8, 2 * 10**6),
     )(pieces)
+    sums, convolved = lax.optimization_barrier((sums, convolved))
+    across = moved(convolved, parts)
     results = lax.all_to_all(
         sums.reshape(n_z, capacity, columns), "z", split_axis=0, concat_axis=0, tiled=True
     ).reshape(slots, columns)
@@ -238,6 +251,22 @@
         compiler_params=params(16),
         cost_estimate=cost(10**8, 10**6),
     )(high, low, results)
+    step = length // 2
+    gathered = [convolved, *from_back, across, *from_front[::-1]]
+    mixer_rows = pl.pallas_call(
+        mixer_kernel,
+        grid=(length // step,),
+        out_shape=jax.ShapeDtypeStruct((length, out_weight.shape[1]), bf16),
+        in_specs=[smem]
+        + [pl.BlockSpec((step, channels), lambda i: (i, 0))] * n_tp
+        + [
+            pl.BlockSpec((1, n_tp * channels), lambda i: (0, 0)),
+            pl.BlockSpec(out_weight.shape, lambda i: (0, 0)),
+        ],
+        out_specs=pl.BlockSpec((step, out_weight.shape[1]), lambda i: (i, 0)),
+        compiler_params=params(16),
+        cost_estimate=cost(10**9, 2 * 10**6),
+    )(me.astype(jnp.int32).reshape(1), *gathered, chan_gain.reshape(1, -1), out_weight)
     return (mixer_rows, routed_rows)
 
 
@@ -260,7 +289,7 @@
         P(("z", "core"), "tp", None),
     )
     return jax.shard_map(
-        on_device,
+        step_on_device,
         mesh=finer,
         in_specs=placed,
         out_specs=(P(tok, "tp"), P(tok, "tp")),

time: 225 us -> 218 us (0.969)
  the two profiles are of different devices: /device:TPU:65 before, /device:TPU:80 now
where the time goes in v3:
time: 218 us; the launch traced here: 217 us
  starting transfers between devices  115 us (53%)
  blocking collectives  43.7 us (20%)
  waiting for transfers between devices  43 us (20%)
  Pallas kernels  12 us (6%)
    all_to_all x1, blocking collectives, step_on_device(): lax.all_to_all(pieces, 'tp', split_axis=0, concat_axis=0, tiled=True)  43.7 us
    all_to_all x1, starting transfers between devices, step_on_device(): lax.all_to_all(outgoing.reshape(experts, capacity, wide), 'z', split_axis...  43.7 us
    ppermute x11, waiting for transfers between devices, moved(): return lax.ppermute(value, 'tp', [(i, (i + by) % n) for i in range(n)])  40.2 us
    ppermute x11, starting transfers between devices, moved(): return lax.ppermute(value, 'tp', [(i, (i + by) % n) for i in range(n)])  38.7 us
    all_to_all x1, starting transfers between devices, step_on_device(): lax.all_to_all(sums.reshape(n_z, capacity, columns), 'z', split_axis=0, c...  25.1 us
    ppermute x3, starting transfers between devices, partner(): return lax.ppermute(value, 'core', [(0, 1), (1, 0)])  6.33 us
    pallas_call x1, Pallas kernels, step_on_device(): pl.pallas_call(experts_kernel, out_shape=jax.ShapeDtypeStruct((n_tp, rows...  5.41 us
  transfers between devices with their start and end apart: 17, of which 9 were waited for; matrix products, arithmetic and copies ran while one was open for 0% of the time, Pallas kernels for 1%

profile of v3, /device:TPU:80, one launch (start us, length us, event | category | flops | bytes accessed | tf_op | source)
XLA Modules:
  0.0 217.1 jit_solution(7726574199356121534)
XLA Ops:
  0.7 2.5 %shard_map.131 = bf16[384,512]{1,0:T(8,128)(2,1)} custom-call(s32[1]{0:T(128)} %bitcast.1.index, s32[2,128]{1,0:T(2,128)} %bitcast.78, bf16[128,2048]{1,0:T(8,128)(2,1)} %rows.1, f32[1,2048]{1,0:T(1,128)} %bitcast.85), custom_call_target="tpu_custom_call" | custom-call | flops 100000000 | bytes 1000000 | tf_op jit(solution)/shard_map/pallas_call | solution.py:168
  3.1 43.7 %all-to-all-start = ((bf16[16,24,512]{2,1,0:T(8,128)(2,1)}), bf16[16,24,512]{2,1,0:T(8,128)(2,1)S(1)}, u32[]{:S(2)}, u32[]{:S(2)}) async-start(bf16[16,24,512]{2,1,0:T(8,128)(2,1)} %bitcast.82), calls=%async_computation | async-start | bytes 786432 | tf_op jit(solution)/shard_map/all_to_all | solution.py:177
  50.1 3.6 %collective-permute-start.1 = (bf16[512,128]{1,0:T(8,128)(2,1)S(1)}, bf16[512,128]{1,0:T(8,128)(2,1)S(1)}, u32[]{:S(2)}, u32[]{:S(2)}) collective-permute-start(bf16[512,128]{1,0:T(8,128)(2,1)S(1)} %fusion.1.refs_0_), channel_id=1, source_target_pairs={{0,1},{1,2},{2,3},{3,4},{4,5},{5,6},{6,7},{7,0},{8,9},{9,10},{10,1... | collective-permute-start | bytes 393224 | tf_op jit(solution)/shard_map/ppermute | solution.py:124
  53.6 4.6 %collective-permute-start.2 = (bf16[512,128]{1,0:T(8,128)(2,1)S(1)}, bf16[512,128]{1,0:T(8,128)(2,1)S(1)}, u32[]{:S(2)}, u32[]{:S(2)}) collective-permute-start(bf16[512,128]{1,0:T(8,128)(2,1)S(1)} %fusion.1.refs_0_), channel_id=1, source_target_pairs={{0,2},{1,3},{2,4},{3,5},{4,6},{5,7},{6,0},{7,1},{8,10},{9,11},{10,... | collective-permute-start | bytes 393224 | tf_op jit(solution)/shard_map/ppermute | solution.py:124
  58.3 5.1 %collective-permute-start.3 = (bf16[512,128]{1,0:T(8,128)(2,1)S(1)}, bf16[512,128]{1,0:T(8,128)(2,1)S(1)}, u32[]{:S(2)}, u32[]{:S(2)}) collective-permute-start(bf16[512,128]{1,0:T(8,128)(2,1)S(1)} %fusion.1.refs_0_), channel_id=1, source_target_pairs={{0,3},{1,4},{2,5},{3,6},{4,7},{5,0},{6,1},{7,2},{8,11},{9,12},{10,... | collective-permute-start | bytes 393224 | tf_op jit(solution)/shard_map/ppermute | solution.py:124
  63.4 4.4 %collective-permute-start.4 = (bf16[512,128]{1,0:T(8,128)(2,1)S(1)}, bf16[512,128]{1,0:T(8,128)(2,1)S(1)}, u32[]{:S(2)}, u32[]{:S(2)}) collective-permute-start(bf16[512,128]{1,0:T(8,128)(2,1)S(1)} %fusion.1.refs_0_), channel_id=1, source_target_pairs={{0,7},{1,0},{2,1},{3,2},{4,3},{5,4},{6,5},{7,6},{8,15},{9,8},{10,9... | collective-permute-start | bytes 393224 | tf_op jit(solution)/shard_map/ppermute | solution.py:124
  67.8 2.7 %collective-permute-start.5 = (bf16[512,128]{1,0:T(8,128)(2,1)S(1)}, bf16[512,128]{1,0:T(8,128)(2,1)S(1)}, u32[]{:S(2)}, u32[]{:S(2)}) collective-permute-start(bf16[512,128]{1,0:T(8,128)(2,1)S(1)} %fusion.1.refs_0_), channel_id=1, source_target_pairs={{0,6},{1,7},{2,0},{3,1},{4,2},{5,3},{6,4},{7,5},{8,14},{9,15},{10,... | collective-permute-start | bytes 393224 | tf_op jit(solution)/shard_map/ppermute | solution.py:124
  70.5 3.0 %collective-permute-start.6 = (bf16[512,128]{1,0:T(8,128)(2,1)S(1)}, bf16[512,128]{1,0:T(8,128)(2,1)S(1)}, u32[]{:S(2)}, u32[]{:S(2)}) collective-permute-start(bf16[512,128]{1,0:T(8,128)(2,1)S(1)} %fusion.1.refs_0_), channel_id=1, source_target_pairs={{0,5},{1,6},{2,7},{3,0},{4,1},{5,2},{6,3},{7,4},{8,13},{9,14},{10,... | collective-permute-start | bytes 393224 | tf_op jit(solution)/shard_map/ppermute | solution.py:124
  73.6 4.9 %collective-permute-done.5.refs_6_ = bf16[512,128]{1,0:T(8,128)(2,1)S(1)} collective-permute-done((bf16[512,128]{1,0:T(8,128)(2,1)S(1)}, bf16[512,128]{1,0:T(8,128)(2,1)S(1)}, u32[]{:S(2)}, u32[]{:S(2)}) %collective-permute-start.5) | collective-permute-done | bytes 131104 | tf_op jit(solution)/shard_map/ppermute | solution.py:124
  78.4 9.3 %collective-permute-done.6.refs_5_ = bf16[512,128]{1,0:T(8,128)(2,1)S(1)} collective-permute-done((bf16[512,128]{1,0:T(8,128)(2,1)S(1)}, bf16[512,128]{1,0:T(8,128)(2,1)S(1)}, u32[]{:S(2)}, u32[]{:S(2)}) %collective-permute-start.6) | collective-permute-done | bytes 131104 | tf_op jit(solution)/shard_map/ppermute | solution.py:124
  89.7 2.4 %collective-permute-start.12 = (bf16[1,2048,256]{2,1,0:T(8,128)(2,1)S(1)}, bf16[1,2048,256]{2,1,0:T(8,128)(2,1)S(1)}, u32[]{:S(2)}, u32[]{:S(2)}) collective-permute-start(bf16[1,2048,256]{2,1,0:T(8,128)(2,1)S(1)} %copy-done.2), channel_id=1, source_target_pairs={{0,8},{8,0},{1,9},{9,1},{2,10},{10,2},{3,11},{11,3},{4,12},{12,4},... | collective-permute-start | bytes 3145736 | tf_op jit(solution)/shard_map/ppermute | solution.py:128
  92.2 2.0 collective-permute-start.13
  94.2 2.0 collective-permute-start.10
  96.1 6.1 %collective-permute-start.9 = (bf16[192,512]{1,0:T(8,128)(2,1)S(1)}, bf16[192,512]{1,0:T(8,128)(2,1)S(1)}, u32[]{:S(2)}, u32[]{:S(2)}) collective-permute-start(bf16[192,512]{1,0:T(8,128)(2,1)S(1)} %bitcast.83), channel_id=1, source_target_pairs={{0,6},{1,7},{2,0},{3,1},{4,2},{5,3},{6,4},{7,5},{8,14},{9,15},{10,... | collective-permute-start | bytes 589832 | tf_op jit(solution)/shard_map/ppermute | solution.py:124
  102.2 5.5 %collective-permute-done.10.x_2b = bf16[192,512]{1,0:T(8,128)(2,1)S(1)} collective-permute-done((bf16[192,512]{1,0:T(8,128)(2,1)S(1)}, bf16[192,512]{1,0:T(8,128)(2,1)S(1)}, u32[]{:S(2)}, u32[]{:S(2)}) %collective-permute-start.10) | collective-permute-done | bytes 196640 | tf_op jit(solution)/shard_map/ppermute | solution.py:124
  110.8 2.8 %collective-permute-start.8 = (bf16[384,512]{1,0:T(8,128)(2,1)S(1)}, bf16[384,512]{1,0:T(8,128)(2,1)S(1)}, u32[]{:S(2)}, u32[]{:S(2)}) collective-permute-start(bf16[384,512]{1,0:T(8,128)(2,1)S(1)} %bitcast.75), channel_id=1, source_target_pairs={{0,1},{1,2},{2,3},{3,4},{4,5},{5,6},{6,7},{7,0},{8,9},{9,10},{10,1... | collective-permute-start | bytes 1179656 | tf_op jit(solution)/shard_map/ppermute | solution.py:124
  113.6 7.1 %collective-permute-done.7.x_1 = bf16[384,512]{1,0:T(8,128)(2,1)S(1)} collective-permute-done((bf16[384,512]{1,0:T(8,128)(2,1)S(1)}, bf16[384,512]{1,0:T(8,128)(2,1)S(1)}, u32[]{:S(2)}, u32[]{:S(2)}) %collective-permute-start.7) | collective-permute-done | bytes 393248 | tf_op jit(solution)/shard_map/ppermute | solution.py:124
  120.7 4.3 %collective-permute-done.8.x_3 = bf16[384,512]{1,0:T(8,128)(2,1)S(1)} collective-permute-done((bf16[384,512]{1,0:T(8,128)(2,1)S(1)}, bf16[384,512]{1,0:T(8,128)(2,1)S(1)}, u32[]{:S(2)}, u32[]{:S(2)}) %collective-permute-start.8) | collective-permute-done | bytes 393248 | tf_op jit(solution)/shard_map/ppermute | solution.py:124
  126.2 5.4 %shard_map.132 = bf16[8,384,256]{2,1,0:T(8,128)(2,1)S(1)} custom-call(s32[1]{0:T(128)} %bitcast.1.index, bf16[384,512]{1,0:T(8,128)(2,1)S(1)} %bitcast.76, bf16[384,512]{1,0:T(8,128)(2,1)S(1)} %collective-permute-done.7.x_1, bf16[384,512]{1,0:T(8,128)(2,1)S(1)} %collective-permute-done.8.x_3, bf16[192,512]{1,0:T(8,128)(2,1)S(1)} %collective-permute-done.9.x_2a, ...), custom_call_target="tpu_custom_call" | custom-call | flops 3000000000 | bytes 10000000 | tf_op jit(solution)/shard_map/pallas_call | solution.py:208
  131.6 43.7 %all_to_all.15.pieces = bf16[8,384,256]{2,1,0:T(8,128)(2,1)S(1)} all-to-all(bf16[8,384,256]{2,1,0:T(8,128)(2,1)S(1)} %shard_map.132), channel_id=1, replica_groups=mesh['grp'=2,'z'=16,'core'=2,'tp'=8] {'tp'}, dimensions={0} | all-to-all | bytes 3145728 | tf_op jit(solution)/shard_map/all_to_all | solution.py:221
  176.3 25.1 %all-to-all-start.2 = ((bf16[16,24,256]{2,1,0:T(8,128)(2,1)}), bf16[16,24,256]{2,1,0:T(8,128)(2,1)S(1)}, u32[]{:S(2)}, u32[]{:S(2)}) async-start(bf16[16,24,256]{2,1,0:T(8,128)(2,1)} %bitcast.41), calls=%async_computation.2 | async-start | bytes 393216 | tf_op jit(solution)/shard_map/all_to_all | solution.py:234
  201.5 2.5 %collective-permute-start.14 = (bf16[512,128]{1,0:T(8,128)(2,1)S(1)}, bf16[512,128]{1,0:T(8,128)(2,1)S(1)}, u32[]{:S(2)}, u32[]{:S(2)}) collective-permute-start(bf16[512,128]{1,0:T(8,128)(2,1)S(1)} %fusion.1.refs_0_), channel_id=1, source_target_pairs={{0,4},{1,5},{2,6},{3,7},{4,0},{5,1},{6,2},{7,3},{8,12},{9,13},{10,... | collective-permute-start | bytes 393224 | tf_op jit(solution)/shard_map/ppermute | solution.py:124
  204.4 8.0 %collective-permute-done.14.refs_4_ = bf16[512,128]{1,0:T(8,128)(2,1)S(1)} collective-permute-done((bf16[512,128]{1,0:T(8,128)(2,1)S(1)}, bf16[512,128]{1,0:T(8,128)(2,1)S(1)}, u32[]{:S(2)}, u32[]{:S(2)}) %collective-permute-start.14) | collective-permute-done | bytes 131104 | tf_op jit(solution)/shard_map/ppermute | solution.py:124
  214.2 2.0 all-to-all-done.2
  (44 shorter events, 13.6 us)
Async XLA Ops:
  0.6 46.2 %copy-start.8 = (bf16[512,128]{1,0:T(8,128)(2,1)S(1)}, bf16[512,128]{1,0:T(8,128)(2,1)}, u32[]{:S(2)}) copy-start(bf16[512,128]{1,0:T(8,128)(2,1)} %param.12) | copy-start | bytes 393220
  0.6 46.2 %copy-start.7 = (bf16[512,128]{1,0:T(8,128)(2,1)S(1)}, bf16[512,128]{1,0:T(8,128)(2,1)}, u32[]{:S(2)}) copy-start(bf16[512,128]{1,0:T(8,128)(2,1)} %param.13) | copy-start | bytes 393220
  0.7 47.8 %copy-start.9 = (f32[31,128]{1,0:T(8,128)S(1)}, f32[31,128]{1,0:T(8,128)}, u32[]{:S(2)}) copy-start(f32[31,128]{1,0:T(8,128)} %param.14) | copy-start | bytes 47620
  3.1 84.6 %all-to-all-start = ((bf16[16,24,512]{2,1,0:T(8,128)(2,1)}), bf16[16,24,512]{2,1,0:T(8,128)(2,1)S(1)}, u32[]{:S(2)}, u32[]{:S(2)}) async-start(bf16[16,24,512]{2,1,0:T(8,128)(2,1)} %bitcast.82), calls=%async_computation | async-start | bytes 786432 | tf_op jit(solution)/shard_map/all_to_all | solution.py:177
  46.9 2.4 %collective-permute-start = (bf16[32,128]{1,0:T(8,128)(2,1)S(1)}, bf16[32,128]{1,0:T(8,128)(2,1)S(1)}, u32[]{:S(2)}, u32[]{:S(2)}) collective-permute-start(bf16[32,128]{1,0:T(8,128)(2,1)S(1)} %slice.268), channel_id=1, source_target_pairs={{0,8},{8,16},{16,24},{24,32},{32,40},{40,48},{48,56},{56,64},{64,7... | collective-permute-start | bytes 24584 | tf_op jit(solution)/shard_map/ppermute | solution.py:187
  49.3 38.4 %copy-start.1 = (bf16[1,2048,256]{2,1,0:T(8,128)(2,1)S(1)}, bf16[1,2048,256]{2,1,0:T(8,128)(2,1)}, u32[]{:S(2)}) copy-start(bf16[1,2048,256]{2,1,0:T(8,128)(2,1)} %gate_0.1) | copy-start | bytes 3145732
  49.3 40.4 %copy-start.2 = (bf16[1,2048,256]{2,1,0:T(8,128)(2,1)S(1)}, bf16[1,2048,256]{2,1,0:T(8,128)(2,1)}, u32[]{:S(2)}) copy-start(bf16[1,2048,256]{2,1,0:T(8,128)(2,1)} %up_0.1) | copy-start | bytes 3145732
  50.1 20.5 %collective-permute-start.1 = (bf16[512,128]{1,0:T(8,128)(2,1)S(1)}, bf16[512,128]{1,0:T(8,128)(2,1)S(1)}, u32[]{:S(2)}, u32[]{:S(2)}) collective-permute-start(bf16[512,128]{1,0:T(8,128)(2,1)S(1)} %fusion.1.refs_0_), channel_id=1, source_target_pairs={{0,1},{1,2},{2,3},{3,4},{4,5},{5,6},{6,7},{7,0},{8,9},{9,10},{10,1... | collective-permute-start | bytes 393224 | tf_op jit(solution)/shard_map/ppermute | solution.py:124
  53.6 19.9 %collective-permute-start.2 = (bf16[512,128]{1,0:T(8,128)(2,1)S(1)}, bf16[512,128]{1,0:T(8,128)(2,1)S(1)}, u32[]{:S(2)}, u32[]{:S(2)}) collective-permute-start(bf16[512,128]{1,0:T(8,128)(2,1)S(1)} %fusion.1.refs_0_), channel_id=1, source_target_pairs={{0,2},{1,3},{2,4},{3,5},{4,6},{5,7},{6,0},{7,1},{8,10},{9,11},{10,... | collective-permute-start | bytes 393224 | tf_op jit(solution)/shard_map/ppermute | solution.py:124
  58.3 15.3 %collective-permute-start.3 = (bf16[512,128]{1,0:T(8,128)(2,1)S(1)}, bf16[512,128]{1,0:T(8,128)(2,1)S(1)}, u32[]{:S(2)}, u32[]{:S(2)}) collective-permute-start(bf16[512,128]{1,0:T(8,128)(2,1)S(1)} %fusion.1.refs_0_), channel_id=1, source_target_pairs={{0,3},{1,4},{2,5},{3,6},{4,7},{5,0},{6,1},{7,2},{8,11},{9,12},{10,... | collective-permute-start | bytes 393224 | tf_op jit(solution)/shard_map/ppermute | solution.py:124
  63.4 10.2 %collective-permute-start.4 = (bf16[512,128]{1,0:T(8,128)(2,1)S(1)}, bf16[512,128]{1,0:T(8,128)(2,1)S(1)}, u32[]{:S(2)}, u32[]{:S(2)}) collective-permute-start(bf16[512,128]{1,0:T(8,128)(2,1)S(1)} %fusion.1.refs_0_), channel_id=1, source_target_pairs={{0,7},{1,0},{2,1},{3,2},{4,3},{5,4},{6,5},{7,6},{8,15},{9,8},{10,9... | collective-permute-start | bytes 393224 | tf_op jit(solution)/shard_map/ppermute | solution.py:124
  67.8 10.6 %collective-permute-start.5 = (bf16[512,128]{1,0:T(8,128)(2,1)S(1)}, bf16[512,128]{1,0:T(8,128)(2,1)S(1)}, u32[]{:S(2)}, u32[]{:S(2)}) collective-permute-start(bf16[512,128]{1,0:T(8,128)(2,1)S(1)} %fusion.1.refs_0_), channel_id=1, source_target_pairs={{0,6},{1,7},{2,0},{3,1},{4,2},{5,3},{6,4},{7,5},{8,14},{9,15},{10,... | collective-permute-start | bytes 393224 | tf_op jit(solution)/shard_map/ppermute | solution.py:124
  70.5 17.2 %collective-permute-start.6 = (bf16[512,128]{1,0:T(8,128)(2,1)S(1)}, bf16[512,128]{1,0:T(8,128)(2,1)S(1)}, u32[]{:S(2)}, u32[]{:S(2)}) collective-permute-start(bf16[512,128]{1,0:T(8,128)(2,1)S(1)} %fusion.1.refs_0_), channel_id=1, source_target_pairs={{0,5},{1,6},{2,7},{3,0},{4,1},{5,2},{6,3},{7,4},{8,13},{9,14},{10,... | collective-permute-start | bytes 393224 | tf_op jit(solution)/shard_map/ppermute | solution.py:124
  87.8 37.2 %collective-permute-start.11 = (bf16[1,2048,256]{2,1,0:T(8,128)(2,1)S(1)}, bf16[1,2048,256]{2,1,0:T(8,128)(2,1)S(1)}, u32[]{:S(2)}, u32[]{:S(2)}) collective-permute-start(bf16[1,2048,256]{2,1,0:T(8,128)(2,1)S(1)} %copy-done.1), channel_id=1, source_target_pairs={{0,8},{8,0},{1,9},{9,1},{2,10},{10,2},{3,11},{11,3},{4,12},{12,4},... | collective-permute-start | bytes 3145736 | tf_op jit(solution)/shard_map/ppermute | solution.py:128
  89.7 35.2 %collective-permute-start.12 = (bf16[1,2048,256]{2,1,0:T(8,128)(2,1)S(1)}, bf16[1,2048,256]{2,1,0:T(8,128)(2,1)S(1)}, u32[]{:S(2)}, u32[]{:S(2)}) collective-permute-start(bf16[1,2048,256]{2,1,0:T(8,128)(2,1)S(1)} %copy-done.2), channel_id=1, source_target_pairs={{0,8},{8,0},{1,9},{9,1},{2,10},{10,2},{3,11},{11,3},{4,12},{12,4},... | collective-permute-start | bytes 3145736 | tf_op jit(solution)/shard_map/ppermute | solution.py:128
  92.2 32.8 %collective-permute-start.13 = (bf16[1,256,2048]{2,1,0:T(8,128)(2,1)}, bf16[1,256,2048]{2,1,0:T(8,128)(2,1)S(1)}, u32[]{:S(2)}, u32[]{:S(2)}) collective-permute-start(bf16[1,256,2048]{2,1,0:T(8,128)(2,1)} %down_0.1), channel_id=1, source_target_pairs={{0,8},{8,0},{1,9},{9,1},{2,10},{10,2},{3,11},{11,3},{4,12},{12,4},... | collective-permute-start | bytes 3145736 | tf_op jit(solution)/shard_map/ppermute | solution.py:128
  94.2 13.5 %collective-permute-start.10 = (bf16[192,512]{1,0:T(8,128)(2,1)S(1)}, bf16[192,512]{1,0:T(8,128)(2,1)S(1)}, u32[]{:S(2)}, u32[]{:S(2)}) collective-permute-start(bf16[192,512]{1,0:T(8,128)(2,1)S(1)} %bitcast.84), channel_id=1, source_target_pairs={{0,2},{1,3},{2,4},{3,5},{4,6},{5,7},{6,0},{7,1},{8,10},{9,11},{10,... | collective-permute-start | bytes 589832 | tf_op jit(solution)/shard_map/ppermute | solution.py:124
  96.1 14.7 %collective-permute-start.9 = (bf16[192,512]{1,0:T(8,128)(2,1)S(1)}, bf16[192,512]{1,0:T(8,128)(2,1)S(1)}, u32[]{:S(2)}, u32[]{:S(2)}) collective-permute-start(bf16[192,512]{1,0:T(8,128)(2,1)S(1)} %bitcast.83), channel_id=1, source_target_pairs={{0,6},{1,7},{2,0},{3,1},{4,2},{5,3},{6,4},{7,5},{8,14},{9,15},{10,... | collective-permute-start | bytes 589832 | tf_op jit(solution)/shard_map/ppermute | solution.py:124
  107.7 13.0 %collective-permute-start.7 = (bf16[384,512]{1,0:T(8,128)(2,1)S(1)}, bf16[384,512]{1,0:T(8,128)(2,1)S(1)}, u32[]{:S(2)}, u32[]{:S(2)}) collective-permute-start(bf16[384,512]{1,0:T(8,128)(2,1)S(1)} %bitcast.74), channel_id=1, source_target_pairs={{0,7},{1,0},{2,1},{3,2},{4,3},{5,4},{6,5},{7,6},{8,15},{9,8},{10,9... | collective-permute-start | bytes 1179656 | tf_op jit(solution)/shard_map/ppermute | solution.py:124
  110.8 14.1 %collective-permute-start.8 = (bf16[384,512]{1,0:T(8,128)(2,1)S(1)}, bf16[384,512]{1,0:T(8,128)(2,1)S(1)}, u32[]{:S(2)}, u32[]{:S(2)}) collective-permute-start(bf16[384,512]{1,0:T(8,128)(2,1)S(1)} %bitcast.75), channel_id=1, source_target_pairs={{0,1},{1,2},{2,3},{3,4},{4,5},{5,6},{6,7},{7,0},{8,9},{9,10},{10,1... | collective-permute-start | bytes 1179656 | tf_op jit(solution)/shard_map/ppermute | solution.py:124
  175.3 37.1 %copy-start.4 = (bf16[1024,256]{1,0:T(8,128)(2,1)S(1)}, bf16[1024,256]{1,0:T(8,128)(2,1)}, u32[]{:S(2)}) copy-start(bf16[1024,256]{1,0:T(8,128)(2,1)} %refs_9_.1) | copy-start | bytes 1572868
  175.3 37.1 %copy-start.5 = (f32[1024]{0:T(1024)S(1)}, f32[1024]{0:T(1024)}, u32[]{:S(2)}) copy-start(f32[1024]{0:T(1024)} %param.15) | copy-start | bytes 12292
  176.3 39.9 %all-to-all-start.2 = ((bf16[16,24,256]{2,1,0:T(8,128)(2,1)}), bf16[16,24,256]{2,1,0:T(8,128)(2,1)S(1)}, u32[]{:S(2)}, u32[]{:S(2)}) async-start(bf16[16,24,256]{2,1,0:T(8,128)(2,1)} %bitcast.41), calls=%async_computation.2 | async-start | bytes 393216 | tf_op jit(solution)/shard_map/all_to_all | solution.py:234
  201.5 10.9 %collective-permute-start.14 = (bf16[512,128]{1,0:T(8,128)(2,1)S(1)}, bf16[512,128]{1,0:T(8,128)(2,1)S(1)}, u32[]{:S(2)}, u32[]{:S(2)}) collective-permute-start(bf16[512,128]{1,0:T(8,128)(2,1)S(1)} %fusion.1.refs_0_), channel_id=1, source_target_pairs={{0,4},{1,5},{2,6},{3,7},{4,0},{5,1},{6,2},{7,3},{8,12},{9,13},{10,... | collective-permute-start | bytes 393224 | tf_op jit(solution)/shard_map/ppermute | solution.py:124
  (3 other events, 58.5 us)

commit v4 on v3

--- a/solution.py
+++ b/solution.py
@@ -63,7 +63,7 @@
 
 
 def experts_kernel(
-    index, x_0, x_1, x_3, x_2a, x_2b, gate_0, up_0, gate_1, up_1, down_0, down_1, out, wide, tall, sems
+    index, x_0, x_1, x_3, x_2a, x_2b, gate_0, up_0, gate_1, up_1, down_0, down_1, out, wide, tall, held_out, sems, out_sems
 ):
     blocks, width = out.shape[0], out.shape[2]
     held = [wide.at[i] for i in range(4)] + [tall.at[i] for i in range(2)]
@@ -91,32 +91,23 @@
         hidden.append((jax.nn.silu(gate) * projected(2 * half + 1)).astype(bf16))
     copies[4].wait()
     copies[5].wait()
+    stores = []
     for b in range(blocks):
         span = slice(b * width, (b + 1) * width)
         piece = dot(hidden[0], held[4][:, span]) + dot(hidden[1], held[5][:, span])
-        out[b] = piece.astype(bf16)
-
-
-def sum_kernel(pieces, out):
-    total = pieces[0].astype(f32)
-    for b in range(1, pieces.shape[0]):
-        total = total + pieces[b].astype(f32)
-    out[...] = total.astype(bf16)
-
-
-def mixer_kernel(index, *refs):
-    *pieces, gain, weight, out = refs
-    n, width = len(pieces), pieces[0].shape[1]
-    values = jnp.concatenate([p[...] for p in pieces], axis=1).astype(f32)
-    spans = [
-        pl.ds(pl.multiple_of(lax.rem(index[0] + n - k, n) * width, width), width) for k in range(n)
-    ]
-    gains = jnp.concatenate([gain[:, span] for span in spans], axis=1)
-    weights = jnp.concatenate([weight[span, :] for span in spans], axis=0)
+        held_out[b] = piece.astype(bf16)
+        stores.append(pltpu.make_async_copy(held_out.at[b], out.at[b], out_sems.at[b]))
+        stores[-1].start()
+    for store in stores:
+        store.wait()
+
+
+def mixer_kernel(x, gain, weight, out):
+    values = jnp.concatenate([x[b] for b in range(x.shape[0])], axis=1).astype(f32)
     centered = values - jnp.mean(values, axis=-1, keepdims=True)
     scale = lax.rsqrt(jnp.mean(centered * centered, axis=-1, keepdims=True) + eps)
-    activated = jax.nn.silu(centered * scale * gains).astype(bf16)
-    out[...] = dot(activated, weights).astype(bf16)
+    activated = jax.nn.silu(centered * scale * gain[...]).astype(bf16)
+    out[...] = dot(activated, weight[...]).astype(bf16)
 
 
 def moved(value, by):
@@ -178,7 +169,8 @@
         outgoing.reshape(experts, capacity, wide), "z", split_axis=0, concat_axis=0, tiled=True
     )
 
-    value_in, gate_in, outgoing = lax.optimization_barrier((value_in, gate_in, outgoing))
+    own = (value_in, gate_in, gate_w, up_w, down_w)
+    value_in, gate_in, *own, outgoing = lax.optimization_barrier((*own, outgoing))
     taps = conv_taps.shape[0]
     halo = -(-(taps - 1) // 16) * 16
     glu = (value_in.astype(f32) * jax.nn.sigmoid(gate_in.astype(f32))).astype(bf16)
@@ -187,50 +179,38 @@
     before = lax.ppermute(
         glu[length - halo :], ("z", "core"), [(i, i + 1) for i in range(n_ep - 1)]
     )
+    gate_b, up_b, down_b = (partner(w) for w in own)
     padded = jnp.concatenate([before, glu], axis=0).astype(f32)
     total = jnp.zeros(glu.shape, f32)
     for offset in range(taps):
         start = halo - taps + 1 + offset
         total = total + conv_taps[offset][None, :] * padded[start : start + length]
     convolved = total.astype(bf16)
-    from_back = [moved(convolved, k) for k in range(1, parts)]
-    from_front = [moved(convolved, -k) for k in range(1, parts)]
+    arrived, _ = lax.optimization_barrier((arrived, convolved))
+    gathered = lax.all_gather(convolved, "tp", axis=0, tiled=False)
 
     rows = n_z * capacity
-    arrived, from_back, from_front = lax.optimization_barrier((arrived, from_back, from_front))
     x_0 = arrived.reshape(rows, wide)
     x_2a, x_2b = moved(x_0[: rows // 2], -2), moved(x_0[rows // 2 :], 2)
     x_1, x_3 = moved(x_0, -1), moved(x_0, 1)
-    own = lax.optimization_barrier((x_0, gate_w, up_w, down_w))
-    gate_b, up_b, down_b = (partner(w) for w in own[1:])
     hbm = pl.BlockSpec(memory_space=pl.ANY)
     units = gate_w.shape[2]
     pieces = pl.pallas_call(
         experts_kernel,
         out_shape=jax.ShapeDtypeStruct((n_tp, rows, columns), bf16),
         in_specs=[smem] + [vmem] * 5 + [hbm] * 6,
-        out_specs=vmem,
+        out_specs=hbm,
         scratch_shapes=[
             pltpu.VMEM((4, width, units), bf16),
             pltpu.VMEM((2, units, width), bf16),
+            pltpu.VMEM((n_tp, rows, columns), bf16),
             pltpu.SemaphoreType.DMA((6,)),
+            pltpu.SemaphoreType.DMA((n_tp,)),
         ],
         compiler_params=params(24),
         cost_estimate=cost(3 * 10**9, 10**7),
     )(quarter, x_0, x_1, x_3, x_2a, x_2b, gate_w, up_w, gate_b, up_b, down_w, down_b)
-    pieces = lax.all_to_all(pieces, "tp", split_axis=0, concat_axis=0, tiled=True)
-    step = rows // 2
-    sums = pl.pallas_call(
-        sum_kernel,
-        grid=(rows // step,),
-        out_shape=jax.ShapeDtypeStruct((rows, columns), bf16),
-        in_specs=[pl.BlockSpec((n_tp, step, columns), lambda i: (0, i, 0))],
-        out_specs=pl.BlockSpec((step, columns), lambda i: (i, 0)),
-        compiler_params=params(16),
-        cost_estimate=cost(10**8, 2 * 10**6),
-    )(pieces)
-    sums, convolved = lax.optimization_barrier((sums, convolved))
-    across = moved(convolved, parts)
+    sums = lax.psum_scatter(pieces, "tp", scatter_dimension=0, tiled=True)
     results = lax.all_to_all(
         sums.reshape(n_z, capacity, columns), "z", split_axis=0, concat_axis=0, tiled=True
     ).reshape(slots, columns)
@@ -252,21 +232,20 @@
         cost_estimate=cost(10**8, 10**6),
     )(high, low, results)
     step = length // 2
-    gathered = [convolved, *from_back, across, *from_front[::-1]]
     mixer_rows = pl.pallas_call(
         mixer_kernel,
         grid=(length // step,),
         out_shape=jax.ShapeDtypeStruct((length, out_weight.shape[1]), bf16),
-        in_specs=[smem]
-        + [pl.BlockSpec((step, channels), lambda i: (i, 0))] * n_tp
-        + [
+        in_specs=[
+            pl.BlockSpec((n_tp, step, channels), lambda i: (0, i, 0)),
             pl.BlockSpec((1, n_tp * channels), lambda i: (0, 0)),
             pl.BlockSpec(out_weight.shape, lambda i: (0, 0)),
         ],
         out_specs=pl.BlockSpec((step, out_weight.shape[1]), lambda i: (i, 0)),
         compiler_params=params(16),
         cost_estimate=cost(10**9, 2 * 10**6),
-    )(me.astype(jnp.int32).reshape(1), *gathered, chan_gain.reshape(1, -1), out_weight)
+    )(gathered, chan_gain.reshape(1, -1), out_weight)
+
     return (mixer_rows, routed_rows)
 
 

time: 218 us -> 209 us (0.959)
  the two profiles are of different devices: /device:TPU:80 before, /device:TPU:65 now
where the time goes in v4:
time: 209 us; the launch traced here: 205 us
  waiting for transfers between devices  93.6 us (45%)
  starting transfers between devices  81.2 us (39%)
  between operations  14.3 us (7%)
  Pallas kernels  11.8 us (6%)
  other arithmetic  2.43 us (1%)
    reduce_scatter x1, waiting for transfers between devices, step_on_device(): sums = lax.psum_scatter(pieces, 'tp', scatter_dimension=0, tiled=True)  45 us
    all_to_all x1, starting transfers between devices, step_on_device(): lax.all_to_all(outgoing.reshape(experts, capacity, wide), 'z', split_axis...  44.2 us
    all_gather x1, waiting for transfers between devices, step_on_device(): gathered = lax.all_gather(convolved, 'tp', axis=0, tiled=False)  32.8 us
    ppermute x4, starting transfers between devices, moved(): return lax.ppermute(value, 'tp', [(i, (i + by) % n) for i in range(n)])  13.7 us
    all_to_all x1, starting transfers between devices, step_on_device(): lax.all_to_all(sums.reshape(n_z, capacity, columns), 'z', split_axis=0, c...  12.7 us
    ppermute x4, waiting for transfers between devices, moved(): return lax.ppermute(value, 'tp', [(i, (i + by) % n) for i in range(n)])  10.1 us
    ppermute x3, starting transfers between devices, partner(): return lax.ppermute(value, 'core', [(0, 1), (1, 0)])  6.34 us
    pallas_call x1, Pallas kernels, step_on_device(): pl.pallas_call(experts_kernel, out_shape=jax.ShapeDtypeStruct((n_tp, rows...  6.07 us
  transfers between devices with their start and end apart: 12, of which 5 were waited for; matrix products, arithmetic and copies ran while one was open for 1% of the time, Pallas kernels for 1%

profile of v4, /device:TPU:65, one launch (start us, length us, event | category | flops | bytes accessed | tf_op | source)
XLA Modules:
  0.0 204.7 jit_solution(12433107882258361757)
XLA Ops:
  7.2 2.6 %shard_map.131 = bf16[384,512]{1,0:T(8,128)(2,1)} custom-call(s32[1]{0:T(128)} %bitcast.1.index, s32[2,128]{1,0:T(2,128)} %bitcast.78, bf16[128,2048]{1,0:T(8,128)(2,1)} %rows.1, f32[1,2048]{1,0:T(1,128)} %bitcast.87), custom_call_target="tpu_custom_call" | custom-call | flops 100000000 | bytes 1000000 | tf_op jit(solution)/shard_map/pallas_call | solution.py:159
  9.8 44.2 %all-to-all-start = ((bf16[16,24,512]{2,1,0:T(8,128)(2,1)}), bf16[16,24,512]{2,1,0:T(8,128)(2,1)S(1)}, u32[]{:S(2)}, u32[]{:S(2)}) async-start(bf16[16,24,512]{2,1,0:T(8,128)(2,1)} %bitcast.83), calls=%async_computation | async-start | bytes 786432 | tf_op jit(solution)/shard_map/all_to_all | solution.py:168
  54.1 1.0 multiply_convert_fusion
  55.1 4.1 %collective-permute-start = (bf16[32,128]{1,0:T(8,128)(2,1)S(1)}, bf16[32,128]{1,0:T(8,128)(2,1)S(1)}, u32[]{:S(2)}, u32[]{:S(2)}) collective-permute-start(bf16[32,128]{1,0:T(8,128)(2,1)S(1)} %slice.268), channel_id=1, source_target_pairs={{0,8},{8,16},{16,24},{24,32},{32,40},{40,48},{48,56},{56,64},{64,7... | collective-permute-start | bytes 24584 | tf_op jit(solution)/shard_map/ppermute | solution.py:179
  59.3 2.0 collective-permute-start.5
  61.3 2.4 %collective-permute-start.6 = (bf16[1,2048,256]{2,1,0:T(8,128)(2,1)S(1)}, bf16[1,2048,256]{2,1,0:T(8,128)(2,1)}, u32[]{:S(2)}, u32[]{:S(2)}) collective-permute-start(bf16[1,2048,256]{2,1,0:T(8,128)(2,1)S(1)} %copy-done.2), channel_id=1, source_target_pairs={{0,8},{8,0},{1,9},{9,1},{2,10},{10,2},{3,11},{11,3},{4,12},{12,4},... | collective-permute-start | bytes 3145736 | tf_op jit(solution)/shard_map/ppermute | solution.py:119
  63.7 2.0 collective-permute-start.7
  65.8 1.4 fusion.1
  67.1 4.8 %all-to-all-done = bf16[16,24,512]{2,1,0:T(8,128)(2,1)S(1)} async-done(((bf16[16,24,512]{2,1,0:T(8,128)(2,1)}), bf16[16,24,512]{2,1,0:T(8,128)(2,1)S(1)}, u32[]{:S(2)}, u32[]{:S(2)}) %all-to-all-start) | async-done | bytes 393248 | tf_op jit(solution)/shard_map/all_to_all | solution.py:168
  72.0 5.5 %collective-permute-start.1 = (bf16[384,512]{1,0:T(8,128)(2,1)S(1)}, bf16[384,512]{1,0:T(8,128)(2,1)S(1)}, u32[]{:S(2)}, u32[]{:S(2)}) collective-permute-start(bf16[384,512]{1,0:T(8,128)(2,1)S(1)} %bitcast.74), channel_id=1, source_target_pairs={{0,7},{1,0},{2,1},{3,2},{4,3},{5,4},{6,5},{7,6},{8,15},{9,8},{10,9... | collective-permute-start | bytes 1179656 | tf_op jit(solution)/shard_map/ppermute | solution.py:115
  77.4 2.0 collective-permute-start.2
  79.5 4.1 %collective-permute-start.3 = (bf16[192,512]{1,0:T(8,128)(2,1)S(1)}, bf16[192,512]{1,0:T(8,128)(2,1)S(1)}, u32[]{:S(2)}, u32[]{:S(2)}) collective-permute-start(bf16[192,512]{1,0:T(8,128)(2,1)S(1)} %bitcast.86), channel_id=1, source_target_pairs={{0,6},{1,7},{2,0},{3,1},{4,2},{5,3},{6,4},{7,5},{8,14},{9,15},{10,... | collective-permute-start | bytes 589832 | tf_op jit(solution)/shard_map/ppermute | solution.py:115
  83.6 2.1 %collective-permute-start.4 = (bf16[192,512]{1,0:T(8,128)(2,1)S(1)}, bf16[192,512]{1,0:T(8,128)(2,1)S(1)}, u32[]{:S(2)}, u32[]{:S(2)}) collective-permute-start(bf16[192,512]{1,0:T(8,128)(2,1)S(1)} %bitcast.85), channel_id=1, source_target_pairs={{0,2},{1,3},{2,4},{3,5},{4,6},{5,7},{6,0},{7,1},{8,10},{9,11},{10,... | collective-permute-start | bytes 589832 | tf_op jit(solution)/shard_map/ppermute | solution.py:115
  85.7 5.6 %collective-permute-done.3.x_2a = bf16[192,512]{1,0:T(8,128)(2,1)S(1)} collective-permute-done((bf16[192,512]{1,0:T(8,128)(2,1)S(1)}, bf16[192,512]{1,0:T(8,128)(2,1)S(1)}, u32[]{:S(2)}, u32[]{:S(2)}) %collective-permute-start.3) | collective-permute-done | bytes 196640 | tf_op jit(solution)/shard_map/ppermute | solution.py:115
  91.3 4.6 %collective-permute-done.4.x_2b = bf16[192,512]{1,0:T(8,128)(2,1)S(1)} collective-permute-done((bf16[192,512]{1,0:T(8,128)(2,1)S(1)}, bf16[192,512]{1,0:T(8,128)(2,1)S(1)}, u32[]{:S(2)}, u32[]{:S(2)}) %collective-permute-start.4) | collective-permute-done | bytes 196640 | tf_op jit(solution)/shard_map/ppermute | solution.py:115
  95.9 6.1 %shard_map.134 = bf16[8,384,256]{2,1,0:T(8,128)(2,1)} custom-call(s32[1]{0:T(128)} %bitcast.1.index, bf16[384,512]{1,0:T(8,128)(2,1)S(1)} %bitcast.76, bf16[384,512]{1,0:T(8,128)(2,1)S(1)} %collective-permute-done.1.x_1, bf16[384,512]{1,0:T(8,128)(2,1)S(1)} %collective-permute-done.2.x_3, bf16[192,512]{1,0:T(8,128)(2,1)S(1)} %collective-permute-done.3.x_2a, ...), custom_call_target="tpu_custom_call" | custom-call | flops 3000000000 | bytes 10000000 | tf_op jit(solution)/shard_map/pallas_call | solution.py:198
  102.1 0.7 all-gather.3.cloned.1.call-update
  102.9 45.0 %reduce-scatter.2.cloned.1.call-done = bf16[1,384,256]{2,1,0:T(8,128)(2,1)} async-done(((bf16[8,384,256]{2,1,0:T(8,128)(2,1)}), bf16[1,384,256]{2,1,0:T(8,128)(2,1)}) %reduce-scatter.2.cloned.1.call-update) | async-done | bytes 196624 | tf_op jit(solution)/shard_map/reduce_scatter | solution.py:213
  147.9 12.7 %all-to-all-start.1 = ((bf16[16,24,256]{2,1,0:T(8,128)(2,1)}), bf16[16,24,256]{2,1,0:T(8,128)(2,1)S(1)}, u32[]{:S(2)}, u32[]{:S(2)}) async-start(bf16[16,24,256]{2,1,0:T(8,128)(2,1)} %bitcast.84), calls=%async_computation.2 | async-start | bytes 393216 | tf_op jit(solution)/shard_map/all_to_all | solution.py:214
  160.6 0.5 shard_map.133
  161.1 32.8 %all-gather.3.cloned.1.call-done = bf16[4096,128]{1,0:T(8,128)(2,1)} async-done(((bf16[512,128]{1,0:T(8,128)(2,1)}), bf16[4096,128]{1,0:T(8,128)(2,1)}) %all-gather.3.cloned.1.call-update) | async-done | bytes 1048592 | tf_op jit(solution)/shard_map/all_gather | solution.py:190
  193.9 1.2 copy-done.4
  195.1 1.9 shard_map.132
  197.0 0.9 shard_map.135
  (32 shorter events, 0.3 us)
Async XLA Ops:
  7.2 52.1 %copy-start.1 = (bf16[1,2048,256]{2,1,0:T(8,128)(2,1)S(1)}, bf16[1,2048,256]{2,1,0:T(8,128)(2,1)}, u32[]{:S(2)}) copy-start(bf16[1,2048,256]{2,1,0:T(8,128)(2,1)} %gate_0.1) | copy-start | bytes 3145732
  7.2 54.1 %copy-start.2 = (bf16[1,2048,256]{2,1,0:T(8,128)(2,1)S(1)}, bf16[1,2048,256]{2,1,0:T(8,128)(2,1)}, u32[]{:S(2)}) copy-start(bf16[1,2048,256]{2,1,0:T(8,128)(2,1)} %up_0.1) | copy-start | bytes 3145732
  7.2 58.5 %copy-start.8 = (f32[31,128]{1,0:T(8,128)S(1)}, f32[31,128]{1,0:T(8,128)}, u32[]{:S(2)}) copy-start(f32[31,128]{1,0:T(8,128)} %param.14) | copy-start | bytes 47620
  9.8 62.2 %all-to-all-start = ((bf16[16,24,512]{2,1,0:T(8,128)(2,1)}), bf16[16,24,512]{2,1,0:T(8,128)(2,1)S(1)}, u32[]{:S(2)}, u32[]{:S(2)}) async-start(bf16[16,24,512]{2,1,0:T(8,128)(2,1)} %bitcast.83), calls=%async_computation | async-start | bytes 786432 | tf_op jit(solution)/shard_map/all_to_all | solution.py:168
  54.0 93.9 %reduce-scatter.2.cloned.1.call-start = ((), (), s32[]{:S(2)}) async-start(), calls=%async_computation.3 | async-start | bytes 1769472 | tf_op jit(solution)/shard_map/reduce_scatter | solution.py:213
  55.1 10.6 %collective-permute-start = (bf16[32,128]{1,0:T(8,128)(2,1)S(1)}, bf16[32,128]{1,0:T(8,128)(2,1)S(1)}, u32[]{:S(2)}, u32[]{:S(2)}) collective-permute-start(bf16[32,128]{1,0:T(8,128)(2,1)S(1)} %slice.268), channel_id=1, source_target_pairs={{0,8},{8,16},{16,24},{24,32},{32,40},{40,48},{48,56},{56,64},{64,7... | collective-permute-start | bytes 24584 | tf_op jit(solution)/shard_map/ppermute | solution.py:179
  59.3 20.2 %collective-permute-start.5 = (bf16[1,2048,256]{2,1,0:T(8,128)(2,1)S(1)}, bf16[1,2048,256]{2,1,0:T(8,128)(2,1)}, u32[]{:S(2)}, u32[]{:S(2)}) collective-permute-start(bf16[1,2048,256]{2,1,0:T(8,128)(2,1)S(1)} %copy-done.1), channel_id=1, source_target_pairs={{0,8},{8,0},{1,9},{9,1},{2,10},{10,2},{3,11},{11,3},{4,12},{12,4},... | collective-permute-start | bytes 3145736 | tf_op jit(solution)/shard_map/ppermute | solution.py:119
  61.3 22.3 %collective-permute-start.6 = (bf16[1,2048,256]{2,1,0:T(8,128)(2,1)S(1)}, bf16[1,2048,256]{2,1,0:T(8,128)(2,1)}, u32[]{:S(2)}, u32[]{:S(2)}) collective-permute-start(bf16[1,2048,256]{2,1,0:T(8,128)(2,1)S(1)} %copy-done.2), channel_id=1, source_target_pairs={{0,8},{8,0},{1,9},{9,1},{2,10},{10,2},{3,11},{11,3},{4,12},{12,4},... | collective-permute-start | bytes 3145736 | tf_op jit(solution)/shard_map/ppermute | solution.py:119
  63.7 22.0 %collective-permute-start.7 = (bf16[1,256,2048]{2,1,0:T(8,128)(2,1)}, bf16[1,256,2048]{2,1,0:T(8,128)(2,1)}, u32[]{:S(2)}, u32[]{:S(2)}) collective-permute-start(bf16[1,256,2048]{2,1,0:T(8,128)(2,1)} %down_0.1), channel_id=1, source_target_pairs={{0,8},{8,0},{1,9},{9,1},{2,10},{10,2},{3,11},{11,3},{4,12},{12,4},... | collective-permute-start | bytes 3145736 | tf_op jit(solution)/shard_map/ppermute | solution.py:119
  65.8 30.1 %copy-start.3 = (bf16[1,256,2048]{2,1,0:T(8,128)(2,1)S(1)}, bf16[1,256,2048]{2,1,0:T(8,128)(2,1)}, u32[]{:S(2)}) copy-start(bf16[1,256,2048]{2,1,0:T(8,128)(2,1)} %down_0.1) | copy-start | bytes 3145732
  72.0 23.9 %collective-permute-start.1 = (bf16[384,512]{1,0:T(8,128)(2,1)S(1)}, bf16[384,512]{1,0:T(8,128)(2,1)S(1)}, u32[]{:S(2)}, u32[]{:S(2)}) collective-permute-start(bf16[384,512]{1,0:T(8,128)(2,1)S(1)} %bitcast.74), channel_id=1, source_target_pairs={{0,7},{1,0},{2,1},{3,2},{4,3},{5,4},{6,5},{7,6},{8,15},{9,8},{10,9... | collective-permute-start | bytes 1179656 | tf_op jit(solution)/shard_map/ppermute | solution.py:115
  77.4 18.4 %collective-permute-start.2 = (bf16[384,512]{1,0:T(8,128)(2,1)S(1)}, bf16[384,512]{1,0:T(8,128)(2,1)S(1)}, u32[]{:S(2)}, u32[]{:S(2)}) collective-permute-start(bf16[384,512]{1,0:T(8,128)(2,1)S(1)} %bitcast.75), channel_id=1, source_target_pairs={{0,1},{1,2},{2,3},{3,4},{4,5},{5,6},{6,7},{7,0},{8,9},{9,10},{10,1... | collective-permute-start | bytes 1179656 | tf_op jit(solution)/shard_map/ppermute | solution.py:115
  79.5 11.8 %collective-permute-start.3 = (bf16[192,512]{1,0:T(8,128)(2,1)S(1)}, bf16[192,512]{1,0:T(8,128)(2,1)S(1)}, u32[]{:S(2)}, u32[]{:S(2)}) collective-permute-start(bf16[192,512]{1,0:T(8,128)(2,1)S(1)} %bitcast.86), channel_id=1, source_target_pairs={{0,6},{1,7},{2,0},{3,1},{4,2},{5,3},{6,4},{7,5},{8,14},{9,15},{10,... | collective-permute-start | bytes 589832 | tf_op jit(solution)/shard_map/ppermute | solution.py:115
  83.6 12.3 %collective-permute-start.4 = (bf16[192,512]{1,0:T(8,128)(2,1)S(1)}, bf16[192,512]{1,0:T(8,128)(2,1)S(1)}, u32[]{:S(2)}, u32[]{:S(2)}) collective-permute-start(bf16[192,512]{1,0:T(8,128)(2,1)S(1)} %bitcast.85), channel_id=1, source_target_pairs={{0,2},{1,3},{2,4},{3,5},{4,6},{5,7},{6,0},{7,1},{8,10},{9,11},{10,... | collective-permute-start | bytes 589832 | tf_op jit(solution)/shard_map/ppermute | solution.py:115
  102.0 58.6 %copy-start = (s32[128,2]{0,1:T(2,128)S(1)}, s32[128,2]{0,1:T(2,128)}, u32[]{:S(2)}) copy-start(s32[128,2]{0,1:T(2,128)} %param.19) | copy-start | bytes 3076
  102.0 58.6 %copy-start.7 = (f32[128,2]{0,1:T(2,128)S(1)}, f32[128,2]{0,1:T(2,128)}, u32[]{:S(2)}) copy-start(f32[128,2]{0,1:T(2,128)} %param.20) | copy-start | bytes 3076
  102.0 91.9 %copy-start.5 = (bf16[1024,256]{1,0:T(8,128)(2,1)S(1)}, bf16[1024,256]{1,0:T(8,128)(2,1)}, u32[]{:S(2)}) copy-start(bf16[1024,256]{1,0:T(8,128)(2,1)} %weight.1) | copy-start | bytes 1572868
  102.0 91.9 %copy-start.6 = (f32[1024]{0:T(1024)S(1)}, f32[1024]{0:T(1024)}, u32[]{:S(2)}) copy-start(f32[1024]{0:T(1024)} %param.15) | copy-start | bytes 12292
  102.1 91.8 %all-gather.3.cloned.1.call-start = ((), (), s32[]{:S(2)}) async-start(), calls=%async_computation.4 | async-start | bytes 1179648 | tf_op jit(solution)/shard_map/all_gather | solution.py:190
  147.9 49.1 %all-to-all-start.1 = ((bf16[16,24,256]{2,1,0:T(8,128)(2,1)}), bf16[16,24,256]{2,1,0:T(8,128)(2,1)S(1)}, u32[]{:S(2)}, u32[]{:S(2)}) async-start(bf16[16,24,256]{2,1,0:T(8,128)(2,1)} %bitcast.84), calls=%async_computation.2 | async-start | bytes 393216 | tf_op jit(solution)/shard_map/all_to_all | solution.py:214
  193.9 1.2 copy-start.4
Sparse Core Ops, SparseCore 0:
  102.2 45.6 reduce-scatter.1
  150.6 43.2 all-gather.2

commit v5 on v3

--- a/solution.py
+++ b/solution.py
@@ -63,7 +63,7 @@
 
 
 def experts_kernel(
-    index, x_0, x_1, x_3, x_2a, x_2b, gate_0, up_0, gate_1, up_1, down_0, down_1, out, wide, tall, sems
+    index, x_0, x_1, x_3, x_2a, x_2b, gate_0, up_0, gate_1, up_1, down_0, down_1, out, wide, tall, held_out, sems, out_sems
 ):
     blocks, width = out.shape[0], out.shape[2]
     held = [wide.at[i] for i in range(4)] + [tall.at[i] for i in range(2)]
@@ -91,10 +91,15 @@
         hidden.append((jax.nn.silu(gate) * projected(2 * half + 1)).astype(bf16))
     copies[4].wait()
     copies[5].wait()
+    stores = []
     for b in range(blocks):
         span = slice(b * width, (b + 1) * width)
         piece = dot(hidden[0], held[4][:, span]) + dot(hidden[1], held[5][:, span])
-        out[b] = piece.astype(bf16)
+        held_out[b] = piece.astype(bf16)
+        stores.append(pltpu.make_async_copy(held_out.at[b], out.at[b], out_sems.at[b]))
+        stores[-1].start()
+    for store in stores:
+        store.wait()
 
 
 def sum_kernel(pieces, out):
@@ -178,7 +183,6 @@
         outgoing.reshape(experts, capacity, wide), "z", split_axis=0, concat_axis=0, tiled=True
     )
 
-    value_in, gate_in, outgoing = lax.optimization_barrier((value_in, gate_in, outgoing))
     taps = conv_taps.shape[0]
     halo = -(-(taps - 1) // 16) * 16
     glu = (value_in.astype(f32) * jax.nn.sigmoid(gate_in.astype(f32))).astype(bf16)
@@ -193,27 +197,31 @@
         start = halo - taps + 1 + offset
         total = total + conv_taps[offset][None, :] * padded[start : start + length]
     convolved = total.astype(bf16)
-    from_back = [moved(convolved, k) for k in range(1, parts)]
-    from_front = [moved(convolved, -k) for k in range(1, parts)]
+    across = moved(convolved, parts)
+    from_back = [moved(convolved, k) for k in range(1, parts - 1)]
+    from_front = [moved(convolved, -k) for k in range(1, parts - 1)]
+    from_back.append(moved(convolved, parts - 1))
+    from_front.append(moved(convolved, 1 - parts))
 
     rows = n_z * capacity
-    arrived, from_back, from_front = lax.optimization_barrier((arrived, from_back, from_front))
+    arrived, _ = lax.optimization_barrier((arrived, convolved))
     x_0 = arrived.reshape(rows, wide)
     x_2a, x_2b = moved(x_0[: rows // 2], -2), moved(x_0[rows // 2 :], 2)
     x_1, x_3 = moved(x_0, -1), moved(x_0, 1)
-    own = lax.optimization_barrier((x_0, gate_w, up_w, down_w))
-    gate_b, up_b, down_b = (partner(w) for w in own[1:])
+    gate_b, up_b, down_b = (partner(w) for w in (gate_w, up_w, down_w))
     hbm = pl.BlockSpec(memory_space=pl.ANY)
     units = gate_w.shape[2]
     pieces = pl.pallas_call(
         experts_kernel,
         out_shape=jax.ShapeDtypeStruct((n_tp, rows, columns), bf16),
         in_specs=[smem] + [vmem] * 5 + [hbm] * 6,
-        out_specs=vmem,
+        out_specs=hbm,
         scratch_shapes=[
             pltpu.VMEM((4, width, units), bf16),
             pltpu.VMEM((2, units, width), bf16),
+            pltpu.VMEM((n_tp, rows, columns), bf16),
             pltpu.SemaphoreType.DMA((6,)),
+            pltpu.SemaphoreType.DMA((n_tp,)),
         ],
         compiler_params=params(24),
         cost_estimate=cost(3 * 10**9, 10**7),
@@ -229,8 +237,6 @@
         compiler_params=params(16),
         cost_estimate=cost(10**8, 2 * 10**6),
     )(pieces)
-    sums, convolved = lax.optimization_barrier((sums, convolved))
-    across = moved(convolved, parts)
     results = lax.all_to_all(
         sums.reshape(n_z, capacity, columns), "z", split_axis=0, concat_axis=0, tiled=True
     ).reshape(slots, columns)

time: 218 us -> 198 us (0.908)
  the two profiles are of different devices: /device:TPU:80 before, /device:TPU:65 now
where the time goes in v5:
time: 198 us; the launch traced here: 196 us
  starting transfers between devices  112 us (57%)
  blocking collectives  35.7 us (18%)
  waiting for transfers between devices  28.6 us (14%)
  Pallas kernels  15.8 us (8%)
    all_to_all x1, starting transfers between devices, step_on_device(): lax.all_to_all(outgoing.reshape(experts, capacity, wide), 'z', split_axis...  44.2 us
    ppermute x11, starting transfers between devices, moved(): return lax.ppermute(value, 'tp', [(i, (i + by) % n) for i in range(n)])  38.3 us
    all_to_all x1, blocking collectives, step_on_device(): lax.all_to_all(pieces, 'tp', split_axis=0, concat_axis=0, tiled=True)  35.7 us
    ppermute x11, waiting for transfers between devices, moved(): return lax.ppermute(value, 'tp', [(i, (i + by) % n) for i in range(n)])  23 us
    all_to_all x1, starting transfers between devices, step_on_device(): lax.all_to_all(sums.reshape(n_z, capacity, columns), 'z', split_axis=0, c...  19.4 us
    pallas_call x1, Pallas kernels, step_on_device(): pl.pallas_call(experts_kernel, out_shape=jax.ShapeDtypeStruct((n_tp, rows...  9.08 us
    ppermute x3, starting transfers between devices, partner(): return lax.ppermute(value, 'core', [(0, 1), (1, 0)])  6.34 us
    all_to_all x1, waiting for transfers between devices, step_on_device(): lax.all_to_all(outgoing.reshape(experts, capacity, wide), 'z', split_axis...  5.6 us
  transfers between devices with their start and end apart: 17, of which 6 were waited for; matrix products, arithmetic and copies ran while one was open for 1% of the time, Pallas kernels for 1%

profile of v5, /device:TPU:65, one launch (start us, length us, event | category | flops | bytes accessed | tf_op | source)
XLA Modules:
  0.0 196.5 jit_solution(14803174705672379137)
XLA Ops:
  0.7 2.6 %shard_map.133 = bf16[384,512]{1,0:T(8,128)(2,1)} custom-call(s32[1]{0:T(128)} %bitcast.35.index, s32[2,128]{1,0:T(2,128)} %bitcast.78, bf16[128,2048]{1,0:T(8,128)(2,1)} %rows.1, f32[1,2048]{1,0:T(1,128)} %bitcast.85), custom_call_target="tpu_custom_call" | custom-call | flops 100000000 | bytes 1000000 | tf_op jit(solution)/shard_map/pallas_call | solution.py:173
  3.2 44.2 %all-to-all-start = ((bf16[16,24,512]{2,1,0:T(8,128)(2,1)}), bf16[16,24,512]{2,1,0:T(8,128)(2,1)S(1)}, u32[]{:S(2)}, u32[]{:S(2)}) async-start(bf16[16,24,512]{2,1,0:T(8,128)(2,1)} %bitcast.82), calls=%async_computation | async-start | bytes 786432 | tf_op jit(solution)/shard_map/all_to_all | solution.py:182
  48.5 4.1 %collective-permute-start = (bf16[32,128]{1,0:T(8,128)(2,1)S(1)}, bf16[32,128]{1,0:T(8,128)(2,1)S(1)}, u32[]{:S(2)}, u32[]{:S(2)}) collective-permute-start(bf16[32,128]{1,0:T(8,128)(2,1)S(1)} %slice.268), channel_id=1, source_target_pairs={{0,8},{8,16},{16,24},{24,32},{32,40},{40,48},{48,56},{56,64},{64,7... | collective-permute-start | bytes 24584 | tf_op jit(solution)/shard_map/ppermute | solution.py:191
  52.7 2.0 collective-permute-start.12
  54.6 2.4 %collective-permute-start.13 = (bf16[1,2048,256]{2,1,0:T(8,128)(2,1)S(1)}, bf16[1,2048,256]{2,1,0:T(8,128)(2,1)}, u32[]{:S(2)}, u32[]{:S(2)}) collective-permute-start(bf16[1,2048,256]{2,1,0:T(8,128)(2,1)S(1)} %copy-done.2), channel_id=1, source_target_pairs={{0,8},{8,0},{1,9},{9,1},{2,10},{10,2},{3,11},{11,3},{4,12},{12,4},... | collective-permute-start | bytes 3145736 | tf_op jit(solution)/shard_map/ppermute | solution.py:133
  57.1 2.0 collective-permute-start.14
  59.8 5.6 %all-to-all-done = bf16[16,24,512]{2,1,0:T(8,128)(2,1)S(1)} async-done(((bf16[16,24,512]{2,1,0:T(8,128)(2,1)}), bf16[16,24,512]{2,1,0:T(8,128)(2,1)S(1)}, u32[]{:S(2)}, u32[]{:S(2)}) %all-to-all-start) | async-done | bytes 393248 | tf_op jit(solution)/shard_map/all_to_all | solution.py:182
  65.4 5.4 %collective-permute-start.8 = (bf16[384,512]{1,0:T(8,128)(2,1)S(1)}, bf16[384,512]{1,0:T(8,128)(2,1)S(1)}, u32[]{:S(2)}, u32[]{:S(2)}) collective-permute-start(bf16[384,512]{1,0:T(8,128)(2,1)S(1)} %bitcast.74), channel_id=1, source_target_pairs={{0,7},{1,0},{2,1},{3,2},{4,3},{5,4},{6,5},{7,6},{8,15},{9,8},{10,9... | collective-permute-start | bytes 1179656 | tf_op jit(solution)/shard_map/ppermute | solution.py:129
  72.9 4.1 %collective-permute-start.10 = (bf16[192,512]{1,0:T(8,128)(2,1)S(1)}, bf16[192,512]{1,0:T(8,128)(2,1)S(1)}, u32[]{:S(2)}, u32[]{:S(2)}) collective-permute-start(bf16[192,512]{1,0:T(8,128)(2,1)S(1)} %bitcast.84), channel_id=1, source_target_pairs={{0,6},{1,7},{2,0},{3,1},{4,2},{5,3},{6,4},{7,5},{8,14},{9,15},{10,... | collective-permute-start | bytes 589832 | tf_op jit(solution)/shard_map/ppermute | solution.py:129
  77.1 2.1 %collective-permute-start.11 = (bf16[192,512]{1,0:T(8,128)(2,1)S(1)}, bf16[192,512]{1,0:T(8,128)(2,1)S(1)}, u32[]{:S(2)}, u32[]{:S(2)}) collective-permute-start(bf16[192,512]{1,0:T(8,128)(2,1)S(1)} %bitcast.83), channel_id=1, source_target_pairs={{0,2},{1,3},{2,4},{3,5},{4,6},{5,7},{6,0},{7,1},{8,10},{9,11},{10,... | collective-permute-start | bytes 589832 | tf_op jit(solution)/shard_map/ppermute | solution.py:129
  79.2 5.6 %collective-permute-done.10.x_2a = bf16[192,512]{1,0:T(8,128)(2,1)S(1)} collective-permute-done((bf16[192,512]{1,0:T(8,128)(2,1)S(1)}, bf16[192,512]{1,0:T(8,128)(2,1)S(1)}, u32[]{:S(2)}, u32[]{:S(2)}) %collective-permute-start.10) | collective-permute-done | bytes 196640 | tf_op jit(solution)/shard_map/ppermute | solution.py:129
  84.7 4.6 %collective-permute-done.11.x_2b = bf16[192,512]{1,0:T(8,128)(2,1)S(1)} collective-permute-done((bf16[192,512]{1,0:T(8,128)(2,1)S(1)}, bf16[192,512]{1,0:T(8,128)(2,1)S(1)}, u32[]{:S(2)}, u32[]{:S(2)}) %collective-permute-start.11) | collective-permute-done | bytes 196640 | tf_op jit(solution)/shard_map/ppermute | solution.py:129
  90.6 9.1 %shard_map.134 = bf16[8,384,256]{2,1,0:T(8,128)(2,1)S(1)} custom-call(s32[1]{0:T(128)} %bitcast.35.index, bf16[384,512]{1,0:T(8,128)(2,1)S(1)} %bitcast.76, bf16[384,512]{1,0:T(8,128)(2,1)S(1)} %collective-permute-done.8.x_1, bf16[384,512]{1,0:T(8,128)(2,1)S(1)} %collective-permute-done.9.x_3, bf16[192,512]{1,0:T(8,128)(2,1)S(1)} %collective-permute-done.10.x_2a, ...), custom_call_target="tpu_custom_call" | custom-call | flops 3000000000 | bytes 10000000 | tf_op jit(solution)/shard_map/pallas_call | solution.py:214
  99.7 35.7 %all_to_all.15.pieces = bf16[8,384,256]{2,1,0:T(8,128)(2,1)S(1)} all-to-all(bf16[8,384,256]{2,1,0:T(8,128)(2,1)S(1)} %shard_map.134), channel_id=1, replica_groups=mesh['grp'=2,'z'=16,'core'=2,'tp'=8] {'tp'}, dimensions={0} | all-to-all | bytes 3145728 | tf_op jit(solution)/shard_map/all_to_all | solution.py:229
  136.4 19.4 %all-to-all-start.2 = ((bf16[16,24,256]{2,1,0:T(8,128)(2,1)}), bf16[16,24,256]{2,1,0:T(8,128)(2,1)S(1)}, u32[]{:S(2)}, u32[]{:S(2)}) async-start(bf16[16,24,256]{2,1,0:T(8,128)(2,1)} %bitcast.41), calls=%async_computation.2 | async-start | bytes 393216 | tf_op jit(solution)/shard_map/all_to_all | solution.py:240
  155.8 2.3 %collective-permute-start.1 = (bf16[512,128]{1,0:T(8,128)(2,1)S(1)}, bf16[512,128]{1,0:T(8,128)(2,1)S(1)}, u32[]{:S(2)}, u32[]{:S(2)}) collective-permute-start(bf16[512,128]{1,0:T(8,128)(2,1)S(1)} %fusion.1.refs_0_), channel_id=1, source_target_pairs={{0,1},{1,2},{2,3},{3,4},{4,5},{5,6},{6,7},{7,0},{8,9},{9,10},{10,1... | collective-permute-start | bytes 393224 | tf_op jit(solution)/shard_map/ppermute | solution.py:129
  158.1 3.7 %collective-permute-start.2 = (bf16[512,128]{1,0:T(8,128)(2,1)S(1)}, bf16[512,128]{1,0:T(8,128)(2,1)S(1)}, u32[]{:S(2)}, u32[]{:S(2)}) collective-permute-start(bf16[512,128]{1,0:T(8,128)(2,1)S(1)} %fusion.1.refs_0_), channel_id=1, source_target_pairs={{0,2},{1,3},{2,4},{3,5},{4,6},{5,7},{6,0},{7,1},{8,10},{9,11},{10,... | collective-permute-start | bytes 393224 | tf_op jit(solution)/shard_map/ppermute | solution.py:129
  161.8 4.3 %collective-permute-start.3 = (bf16[512,128]{1,0:T(8,128)(2,1)S(1)}, bf16[512,128]{1,0:T(8,128)(2,1)S(1)}, u32[]{:S(2)}, u32[]{:S(2)}) collective-permute-start(bf16[512,128]{1,0:T(8,128)(2,1)S(1)} %fusion.1.refs_0_), channel_id=1, source_target_pairs={{0,3},{1,4},{2,5},{3,6},{4,7},{5,0},{6,1},{7,2},{8,11},{9,12},{10,... | collective-permute-start | bytes 393224 | tf_op jit(solution)/shard_map/ppermute | solution.py:129
  166.2 3.2 %collective-permute-start.4 = (bf16[512,128]{1,0:T(8,128)(2,1)S(1)}, bf16[512,128]{1,0:T(8,128)(2,1)S(1)}, u32[]{:S(2)}, u32[]{:S(2)}) collective-permute-start(bf16[512,128]{1,0:T(8,128)(2,1)S(1)} %fusion.1.refs_0_), channel_id=1, source_target_pairs={{0,4},{1,5},{2,6},{3,7},{4,0},{5,1},{6,2},{7,3},{8,12},{9,13},{10,... | collective-permute-start | bytes 393224 | tf_op jit(solution)/shard_map/ppermute | solution.py:129
  169.4 4.8 %collective-permute-start.5 = (bf16[512,128]{1,0:T(8,128)(2,1)S(1)}, bf16[512,128]{1,0:T(8,128)(2,1)S(1)}, u32[]{:S(2)}, u32[]{:S(2)}) collective-permute-start(bf16[512,128]{1,0:T(8,128)(2,1)S(1)} %fusion.1.refs_0_), channel_id=1, source_target_pairs={{0,5},{1,6},{2,7},{3,0},{4,1},{5,2},{6,3},{7,4},{8,13},{9,14},{10,... | collective-permute-start | bytes 393224 | tf_op jit(solution)/shard_map/ppermute | solution.py:129
  174.3 3.1 %collective-permute-start.6 = (bf16[512,128]{1,0:T(8,128)(2,1)S(1)}, bf16[512,128]{1,0:T(8,128)(2,1)S(1)}, u32[]{:S(2)}, u32[]{:S(2)}) collective-permute-start(bf16[512,128]{1,0:T(8,128)(2,1)S(1)} %fusion.1.refs_0_), channel_id=1, source_target_pairs={{0,6},{1,7},{2,0},{3,1},{4,2},{5,3},{6,4},{7,5},{8,14},{9,15},{10,... | collective-permute-start | bytes 393224 | tf_op jit(solution)/shard_map/ppermute | solution.py:129
  177.4 3.1 %collective-permute-start.7 = (bf16[512,128]{1,0:T(8,128)(2,1)S(1)}, bf16[512,128]{1,0:T(8,128)(2,1)S(1)}, u32[]{:S(2)}, u32[]{:S(2)}) collective-permute-start(bf16[512,128]{1,0:T(8,128)(2,1)S(1)} %fusion.1.refs_0_), channel_id=1, source_target_pairs={{0,7},{1,0},{2,1},{3,2},{4,3},{5,4},{6,5},{7,6},{8,15},{9,8},{10,9... | collective-permute-start | bytes 393224 | tf_op jit(solution)/shard_map/ppermute | solution.py:129
  182.9 6.5 %collective-permute-done.6.refs_6_ = bf16[512,128]{1,0:T(8,128)(2,1)S(1)} collective-permute-done((bf16[512,128]{1,0:T(8,128)(2,1)S(1)}, bf16[512,128]{1,0:T(8,128)(2,1)S(1)}, u32[]{:S(2)}, u32[]{:S(2)}) %collective-permute-start.6) | collective-permute-done | bytes 131104 | tf_op jit(solution)/shard_map/ppermute | solution.py:129
  189.4 4.4 %collective-permute-done.7.refs_7_ = bf16[512,128]{1,0:T(8,128)(2,1)S(1)} collective-permute-done((bf16[512,128]{1,0:T(8,128)(2,1)S(1)}, bf16[512,128]{1,0:T(8,128)(2,1)S(1)}, u32[]{:S(2)}, u32[]{:S(2)}) %collective-permute-start.7) | collective-permute-done | bytes 131104 | tf_op jit(solution)/shard_map/ppermute | solution.py:129
  (40 shorter events, 11.1 us)
Async XLA Ops:
  0.6 52.0 %copy-start.1 = (bf16[1,2048,256]{2,1,0:T(8,128)(2,1)S(1)}, bf16[1,2048,256]{2,1,0:T(8,128)(2,1)}, u32[]{:S(2)}) copy-start(bf16[1,2048,256]{2,1,0:T(8,128)(2,1)} %gate_0.1) | copy-start | bytes 3145732
  0.6 54.0 %copy-start.2 = (bf16[1,2048,256]{2,1,0:T(8,128)(2,1)S(1)}, bf16[1,2048,256]{2,1,0:T(8,128)(2,1)}, u32[]{:S(2)}) copy-start(bf16[1,2048,256]{2,1,0:T(8,128)(2,1)} %up_0.1) | copy-start | bytes 3145732
  0.7 58.4 %copy-start.7 = (f32[31,128]{1,0:T(8,128)S(1)}, f32[31,128]{1,0:T(8,128)}, u32[]{:S(2)}) copy-start(f32[31,128]{1,0:T(8,128)} %param.14) | copy-start | bytes 47620
  3.2 62.2 %all-to-all-start = ((bf16[16,24,512]{2,1,0:T(8,128)(2,1)}), bf16[16,24,512]{2,1,0:T(8,128)(2,1)S(1)}, u32[]{:S(2)}, u32[]{:S(2)}) async-start(bf16[16,24,512]{2,1,0:T(8,128)(2,1)} %bitcast.82), calls=%async_computation | async-start | bytes 786432 | tf_op jit(solution)/shard_map/all_to_all | solution.py:182
  48.5 10.6 %collective-permute-start = (bf16[32,128]{1,0:T(8,128)(2,1)S(1)}, bf16[32,128]{1,0:T(8,128)(2,1)S(1)}, u32[]{:S(2)}, u32[]{:S(2)}) collective-permute-start(bf16[32,128]{1,0:T(8,128)(2,1)S(1)} %slice.268), channel_id=1, source_target_pairs={{0,8},{8,16},{16,24},{24,32},{32,40},{40,48},{48,56},{56,64},{64,7... | collective-permute-start | bytes 24584 | tf_op jit(solution)/shard_map/ppermute | solution.py:191
  52.7 20.2 %collective-permute-start.12 = (bf16[1,2048,256]{2,1,0:T(8,128)(2,1)S(1)}, bf16[1,2048,256]{2,1,0:T(8,128)(2,1)}, u32[]{:S(2)}, u32[]{:S(2)}) collective-permute-start(bf16[1,2048,256]{2,1,0:T(8,128)(2,1)S(1)} %copy-done.1), channel_id=1, source_target_pairs={{0,8},{8,0},{1,9},{9,1},{2,10},{10,2},{3,11},{11,3},{4,12},{12,4},... | collective-permute-start | bytes 3145736 | tf_op jit(solution)/shard_map/ppermute | solution.py:133
  54.6 22.4 %collective-permute-start.13 = (bf16[1,2048,256]{2,1,0:T(8,128)(2,1)S(1)}, bf16[1,2048,256]{2,1,0:T(8,128)(2,1)}, u32[]{:S(2)}, u32[]{:S(2)}) collective-permute-start(bf16[1,2048,256]{2,1,0:T(8,128)(2,1)S(1)} %copy-done.2), channel_id=1, source_target_pairs={{0,8},{8,0},{1,9},{9,1},{2,10},{10,2},{3,11},{11,3},{4,12},{12,4},... | collective-permute-start | bytes 3145736 | tf_op jit(solution)/shard_map/ppermute | solution.py:133
  57.1 22.1 %collective-permute-start.14 = (bf16[1,256,2048]{2,1,0:T(8,128)(2,1)}, bf16[1,256,2048]{2,1,0:T(8,128)(2,1)}, u32[]{:S(2)}, u32[]{:S(2)}) collective-permute-start(bf16[1,256,2048]{2,1,0:T(8,128)(2,1)} %down_0.1), channel_id=1, source_target_pairs={{0,8},{8,0},{1,9},{9,1},{2,10},{10,2},{3,11},{11,3},{4,12},{12,4},... | collective-permute-start | bytes 3145736 | tf_op jit(solution)/shard_map/ppermute | solution.py:133
  65.4 23.9 %collective-permute-start.8 = (bf16[384,512]{1,0:T(8,128)(2,1)S(1)}, bf16[384,512]{1,0:T(8,128)(2,1)S(1)}, u32[]{:S(2)}, u32[]{:S(2)}) collective-permute-start(bf16[384,512]{1,0:T(8,128)(2,1)S(1)} %bitcast.74), channel_id=1, source_target_pairs={{0,7},{1,0},{2,1},{3,2},{4,3},{5,4},{6,5},{7,6},{8,15},{9,8},{10,9... | collective-permute-start | bytes 1179656 | tf_op jit(solution)/shard_map/ppermute | solution.py:129
  70.9 18.5 %collective-permute-start.9 = (bf16[384,512]{1,0:T(8,128)(2,1)S(1)}, bf16[384,512]{1,0:T(8,128)(2,1)S(1)}, u32[]{:S(2)}, u32[]{:S(2)}) collective-permute-start(bf16[384,512]{1,0:T(8,128)(2,1)S(1)} %bitcast.75), channel_id=1, source_target_pairs={{0,1},{1,2},{2,3},{3,4},{4,5},{5,6},{6,7},{7,0},{8,9},{9,10},{10,1... | collective-permute-start | bytes 1179656 | tf_op jit(solution)/shard_map/ppermute | solution.py:129
  72.9 11.8 %collective-permute-start.10 = (bf16[192,512]{1,0:T(8,128)(2,1)S(1)}, bf16[192,512]{1,0:T(8,128)(2,1)S(1)}, u32[]{:S(2)}, u32[]{:S(2)}) collective-permute-start(bf16[192,512]{1,0:T(8,128)(2,1)S(1)} %bitcast.84), channel_id=1, source_target_pairs={{0,6},{1,7},{2,0},{3,1},{4,2},{5,3},{6,4},{7,5},{8,14},{9,15},{10,... | collective-permute-start | bytes 589832 | tf_op jit(solution)/shard_map/ppermute | solution.py:129
  77.1 12.3 %collective-permute-start.11 = (bf16[192,512]{1,0:T(8,128)(2,1)S(1)}, bf16[192,512]{1,0:T(8,128)(2,1)S(1)}, u32[]{:S(2)}, u32[]{:S(2)}) collective-permute-start(bf16[192,512]{1,0:T(8,128)(2,1)S(1)} %bitcast.83), channel_id=1, source_target_pairs={{0,2},{1,3},{2,4},{3,5},{4,6},{5,7},{6,0},{7,1},{8,10},{9,11},{10,... | collective-permute-start | bytes 589832 | tf_op jit(solution)/shard_map/ppermute | solution.py:129
  135.4 45.2 %copy-start = (s32[128,2]{0,1:T(2,128)S(1)}, s32[128,2]{0,1:T(2,128)}, u32[]{:S(2)}) copy-start(s32[128,2]{0,1:T(2,128)} %param.19) | copy-start | bytes 3076
  135.4 45.2 %copy-start.6 = (f32[128,2]{0,1:T(2,128)S(1)}, f32[128,2]{0,1:T(2,128)}, u32[]{:S(2)}) copy-start(f32[128,2]{0,1:T(2,128)} %param.20) | copy-start | bytes 3076
  135.4 58.5 %copy-start.4 = (bf16[1024,256]{1,0:T(8,128)(2,1)S(1)}, bf16[1024,256]{1,0:T(8,128)(2,1)}, u32[]{:S(2)}) copy-start(bf16[1024,256]{1,0:T(8,128)(2,1)} %refs_9_.1) | copy-start | bytes 1572868
  135.4 58.5 %copy-start.5 = (f32[1024]{0:T(1024)S(1)}, f32[1024]{0:T(1024)}, u32[]{:S(2)}) copy-start(f32[1024]{0:T(1024)} %param.15) | copy-start | bytes 12292
  136.4 59.3 %all-to-all-start.2 = ((bf16[16,24,256]{2,1,0:T(8,128)(2,1)}), bf16[16,24,256]{2,1,0:T(8,128)(2,1)S(1)}, u32[]{:S(2)}, u32[]{:S(2)}) async-start(bf16[16,24,256]{2,1,0:T(8,128)(2,1)} %bitcast.41), calls=%async_computation.2 | async-start | bytes 393216 | tf_op jit(solution)/shard_map/all_to_all | solution.py:240
  155.8 18.4 %collective-permute-start.1 = (bf16[512,128]{1,0:T(8,128)(2,1)S(1)}, bf16[512,128]{1,0:T(8,128)(2,1)S(1)}, u32[]{:S(2)}, u32[]{:S(2)}) collective-permute-start(bf16[512,128]{1,0:T(8,128)(2,1)S(1)} %fusion.1.refs_0_), channel_id=1, source_target_pairs={{0,1},{1,2},{2,3},{3,4},{4,5},{5,6},{6,7},{7,0},{8,9},{9,10},{10,1... | collective-permute-start | bytes 393224 | tf_op jit(solution)/shard_map/ppermute | solution.py:129
  158.1 19.2 %collective-permute-start.2 = (bf16[512,128]{1,0:T(8,128)(2,1)S(1)}, bf16[512,128]{1,0:T(8,128)(2,1)S(1)}, u32[]{:S(2)}, u32[]{:S(2)}) collective-permute-start(bf16[512,128]{1,0:T(8,128)(2,1)S(1)} %fusion.1.refs_0_), channel_id=1, source_target_pairs={{0,2},{1,3},{2,4},{3,5},{4,6},{5,7},{6,0},{7,1},{8,10},{9,11},{10,... | collective-permute-start | bytes 393224 | tf_op jit(solution)/shard_map/ppermute | solution.py:129
  161.8 19.2 %collective-permute-start.3 = (bf16[512,128]{1,0:T(8,128)(2,1)S(1)}, bf16[512,128]{1,0:T(8,128)(2,1)S(1)}, u32[]{:S(2)}, u32[]{:S(2)}) collective-permute-start(bf16[512,128]{1,0:T(8,128)(2,1)S(1)} %fusion.1.refs_0_), channel_id=1, source_target_pairs={{0,3},{1,4},{2,5},{3,6},{4,7},{5,0},{6,1},{7,2},{8,11},{9,12},{10,... | collective-permute-start | bytes 393224 | tf_op jit(solution)/shard_map/ppermute | solution.py:129
  166.2 16.7 %collective-permute-start.4 = (bf16[512,128]{1,0:T(8,128)(2,1)S(1)}, bf16[512,128]{1,0:T(8,128)(2,1)S(1)}, u32[]{:S(2)}, u32[]{:S(2)}) collective-permute-start(bf16[512,128]{1,0:T(8,128)(2,1)S(1)} %fusion.1.refs_0_), channel_id=1, source_target_pairs={{0,4},{1,5},{2,6},{3,7},{4,0},{5,1},{6,2},{7,3},{8,12},{9,13},{10,... | collective-permute-start | bytes 393224 | tf_op jit(solution)/shard_map/ppermute | solution.py:129
  169.4 13.5 %collective-permute-start.5 = (bf16[512,128]{1,0:T(8,128)(2,1)S(1)}, bf16[512,128]{1,0:T(8,128)(2,1)S(1)}, u32[]{:S(2)}, u32[]{:S(2)}) collective-permute-start(bf16[512,128]{1,0:T(8,128)(2,1)S(1)} %fusion.1.refs_0_), channel_id=1, source_target_pairs={{0,5},{1,6},{2,7},{3,0},{4,1},{5,2},{6,3},{7,4},{8,13},{9,14},{10,... | collective-permute-start | bytes 393224 | tf_op jit(solution)/shard_map/ppermute | solution.py:129
  174.3 15.2 %collective-permute-start.6 = (bf16[512,128]{1,0:T(8,128)(2,1)S(1)}, bf16[512,128]{1,0:T(8,128)(2,1)S(1)}, u32[]{:S(2)}, u32[]{:S(2)}) collective-permute-start(bf16[512,128]{1,0:T(8,128)(2,1)S(1)} %fusion.1.refs_0_), channel_id=1, source_target_pairs={{0,6},{1,7},{2,0},{3,1},{4,2},{5,3},{6,4},{7,5},{8,14},{9,15},{10,... | collective-permute-start | bytes 393224 | tf_op jit(solution)/shard_map/ppermute | solution.py:129
  177.4 16.4 %collective-permute-start.7 = (bf16[512,128]{1,0:T(8,128)(2,1)S(1)}, bf16[512,128]{1,0:T(8,128)(2,1)S(1)}, u32[]{:S(2)}, u32[]{:S(2)}) collective-permute-start(bf16[512,128]{1,0:T(8,128)(2,1)S(1)} %fusion.1.refs_0_), channel_id=1, source_target_pairs={{0,7},{1,0},{2,1},{3,2},{4,3},{5,4},{6,5},{7,6},{8,15},{9,8},{10,9... | collective-permute-start | bytes 393224 | tf_op jit(solution)/shard_map/ppermute | solution.py:129
  (1 other events, 1.2 us)

commit v6 on v5

--- a/solution.py
+++ b/solution.py
@@ -63,38 +63,36 @@
 
 
 def experts_kernel(
-    index, x_0, x_1, x_3, x_2a, x_2b, gate_0, up_0, gate_1, up_1, down_0, down_1, out, wide, tall, held_out, sems, out_sems
+    index, x_0, x_1, x_3, x_2a, x_2b, gate_0, up_0, down_0, gate_1, up_1, down_1, out, wide, tall, held_out, sems, out_sems
 ):
     blocks, width = out.shape[0], out.shape[2]
-    held = [wide.at[i] for i in range(4)] + [tall.at[i] for i in range(2)]
-    weights = (gate_0, up_0, gate_1, up_1, down_0, down_1)
+    arriving = (wide.at[0], wide.at[1], tall)
     copies = [
-        pltpu.make_async_copy(w.at[0], h, sems.at[i]) for i, (w, h) in enumerate(zip(weights, held))
+        pltpu.make_async_copy(w.at[0], h, sems.at[i])
+        for i, (w, h) in enumerate(zip((gate_1, up_1, down_1), arriving))
     ]
     for copy in copies:
         copy.start()
     depth = x_0.shape[1]
-    parts = wide.shape[1] // depth
+    parts = gate_0.shape[1] // depth
     rows = (x_0[...], x_1[...], jnp.concatenate([x_2a[...], x_2b[...]], axis=0), x_3[...])
     places = [lax.rem(index[0] + k, parts) * depth for k in range(parts)]
 
-    def projected(i):
-        copies[i].wait()
-        terms = [
-            dot(r, held[i][pl.ds(pl.multiple_of(p, depth), depth), :]) for r, p in zip(rows, places)
-        ]
-        return functools.reduce(jnp.add, terms)
-
-    hidden = []
-    for half in range(2):
-        gate = projected(2 * half)
-        hidden.append((jax.nn.silu(gate) * projected(2 * half + 1)).astype(bf16))
-    copies[4].wait()
-    copies[5].wait()
+    def projected(weight):
+        spans = [pl.ds(pl.multiple_of(p, depth), depth) for p in places]
+        return functools.reduce(jnp.add, [dot(r, weight[s, :]) for r, s in zip(rows, spans)])
+
+    gate = projected(gate_0.at[0])
+    hidden = [(jax.nn.silu(gate) * projected(up_0.at[0])).astype(bf16)]
+    copies[0].wait()
+    gate = projected(wide.at[0])
+    copies[1].wait()
+    hidden.append((jax.nn.silu(gate) * projected(wide.at[1])).astype(bf16))
+    copies[2].wait()
     stores = []
     for b in range(blocks):
         span = slice(b * width, (b + 1) * width)
-        piece = dot(hidden[0], held[4][:, span]) + dot(hidden[1], held[5][:, span])
+        piece = dot(hidden[0], down_0[0, :, span]) + dot(hidden[1], tall[:, span])
         held_out[b] = piece.astype(bf16)
         stores.append(pltpu.make_async_copy(held_out.at[b], out.at[b], out_sems.at[b]))
         stores[-1].start()
@@ -197,11 +195,9 @@
         start = halo - taps + 1 + offset
         total = total + conv_taps[offset][None, :] * padded[start : start + length]
     convolved = total.astype(bf16)
-    across = moved(convolved, parts)
-    from_back = [moved(convolved, k) for k in range(1, parts - 1)]
-    from_front = [moved(convolved, -k) for k in range(1, parts - 1)]
+    across, from_back = moved(convolved, parts), [moved(convolved, k) for k in (1, 2)]
+    from_front = [moved(convolved, -k) for k in range(1, parts)]
     from_back.append(moved(convolved, parts - 1))
-    from_front.append(moved(convolved, 1 - parts))
 
     rows = n_z * capacity
     arrived, _ = lax.optimization_barrier((arrived, convolved))
@@ -214,19 +210,20 @@
     pieces = pl.pallas_call(
         experts_kernel,
         out_shape=jax.ShapeDtypeStruct((n_tp, rows, columns), bf16),
-        in_specs=[smem] + [vmem] * 5 + [hbm] * 6,
+        in_specs=[smem] + [vmem] * 8 + [hbm] * 3,
         out_specs=hbm,
         scratch_shapes=[
-            pltpu.VMEM((4, width, units), bf16),
-            pltpu.VMEM((2, units, width), bf16),
+            pltpu.VMEM((2, width, units), bf16),
+            pltpu.VMEM((units, width), bf16),
             pltpu.VMEM((n_tp, rows, columns), bf16),
-            pltpu.SemaphoreType.DMA((6,)),
+            pltpu.SemaphoreType.DMA((3,)),
             pltpu.SemaphoreType.DMA((n_tp,)),
         ],
         compiler_params=params(24),
         cost_estimate=cost(3 * 10**9, 10**7),
-    )(quarter, x_0, x_1, x_3, x_2a, x_2b, gate_w, up_w, gate_b, up_b, down_w, down_b)
+    )(quarter, x_0, x_1, x_3, x_2a, x_2b, gate_w, up_w, down_w, gate_b, up_b, down_b)
     pieces = lax.all_to_all(pieces, "tp", split_axis=0, concat_axis=0, tiled=True)
+    pieces, from_front = lax.optimization_barrier((pieces, from_front))
     step = rows // 2
     sums = pl.pallas_call(
         sum_kernel,

time: 198 us -> 198 us (level)
  the two profiles are of different devices: /device:TPU:65 before, /device:TPU:68 now
where the time goes in v6:
time: 198 us; the launch traced here: 197 us
  starting transfers between devices  120 us (61%)
  waiting for transfers between devices  60.4 us (31%)
  Pallas kernels  12.6 us (6%)
    ppermute x11, waiting for transfers between devices, moved(): return lax.ppermute(value, 'tp', [(i, (i + by) % n) for i in range(n)])  48.5 us
    all_to_all x1, starting transfers between devices, step_on_device(): lax.all_to_all(outgoing.reshape(experts, capacity, wide), 'z', split_axis...  43.7 us
    ppermute x11, starting transfers between devices, moved(): return lax.ppermute(value, 'tp', [(i, (i + by) % n) for i in range(n)])  42.7 us
    all_to_all x1, starting transfers between devices, step_on_device(): lax.all_to_all(sums.reshape(n_z, capacity, columns), 'z', split_axis=0, c...  14.6 us
    all_to_all x1, waiting for transfers between devices, step_on_device(): lax.all_to_all(outgoing.reshape(experts, capacity, wide), 'z', split_axis...  11.9 us
    all_to_all x1, starting transfers between devices, step_on_device(): lax.all_to_all(pieces, 'tp', split_axis=0, concat_axis=0, tiled=True)  9.32 us
    ppermute x3, starting transfers between devices, partner(): return lax.ppermute(value, 'core', [(0, 1), (1, 0)])  8.55 us
    pallas_call x1, Pallas kernels, step_on_device(): pl.pallas_call(experts_kernel, out_shape=jax.ShapeDtypeStruct((n_tp, rows...  5.88 us
  transfers between devices with their start and end apart: 18, of which 8 were waited for; matrix products, arithmetic and copies ran while one was open for 1% of the time, Pallas kernels for 1%

profile of v6, /device:TPU:68, one launch (start us, length us, event | category | flops | bytes accessed | tf_op | source)
XLA Modules:
  0.0 197.5 jit_solution(13842065643228499838)
XLA Ops:
  0.7 2.6 %shard_map.131 = bf16[384,512]{1,0:T(8,128)(2,1)} custom-call(s32[1]{0:T(128)} %bitcast.32.index, s32[2,128]{1,0:T(2,128)} %bitcast.78, bf16[128,2048]{1,0:T(8,128)(2,1)} %rows.1, f32[1,2048]{1,0:T(1,128)} %bitcast.85), custom_call_target="tpu_custom_call" | custom-call | flops 100000000 | bytes 1000000 | tf_op jit(solution)/shard_map/pallas_call | solution.py:171
  3.2 43.7 %all-to-all-start = ((bf16[16,24,512]{2,1,0:T(8,128)(2,1)}), bf16[16,24,512]{2,1,0:T(8,128)(2,1)S(1)}, u32[]{:S(2)}, u32[]{:S(2)}) async-start(bf16[16,24,512]{2,1,0:T(8,128)(2,1)} %bitcast.82), calls=%async_computation | async-start | bytes 786432 | tf_op jit(solution)/shard_map/all_to_all | solution.py:180
  49.6 4.2 %collective-permute-start.10 = (bf16[1,2048,256]{2,1,0:T(8,128)(2,1)S(1)}, bf16[1,2048,256]{2,1,0:T(8,128)(2,1)}, u32[]{:S(2)}, u32[]{:S(2)}) collective-permute-start(bf16[1,2048,256]{2,1,0:T(8,128)(2,1)S(1)} %copy-done.2), channel_id=1, source_target_pairs={{0,8},{8,0},{1,9},{9,1},{2,10},{10,2},{3,11},{11,3},{4,12},{12,4},... | collective-permute-start | bytes 3145736 | tf_op jit(solution)/shard_map/ppermute | solution.py:131
  55.7 2.4 %collective-permute-start.9 = (bf16[1,2048,256]{2,1,0:T(8,128)(2,1)S(1)}, bf16[1,2048,256]{2,1,0:T(8,128)(2,1)}, u32[]{:S(2)}, u32[]{:S(2)}) collective-permute-start(bf16[1,2048,256]{2,1,0:T(8,128)(2,1)S(1)} %copy-done.1), channel_id=1, source_target_pairs={{0,8},{8,0},{1,9},{9,1},{2,10},{10,2},{3,11},{11,3},{4,12},{12,4},... | collective-permute-start | bytes 3145736 | tf_op jit(solution)/shard_map/ppermute | solution.py:131
  58.9 11.9 %all-to-all-done = bf16[16,24,512]{2,1,0:T(8,128)(2,1)S(1)} async-done(((bf16[16,24,512]{2,1,0:T(8,128)(2,1)}), bf16[16,24,512]{2,1,0:T(8,128)(2,1)S(1)}, u32[]{:S(2)}, u32[]{:S(2)}) %all-to-all-start) | async-done | bytes 393248 | tf_op jit(solution)/shard_map/all_to_all | solution.py:180
  70.8 2.3 %collective-permute-start.5 = (bf16[384,512]{1,0:T(8,128)(2,1)S(1)}, bf16[384,512]{1,0:T(8,128)(2,1)S(1)}, u32[]{:S(2)}, u32[]{:S(2)}) collective-permute-start(bf16[384,512]{1,0:T(8,128)(2,1)S(1)} %bitcast.74), channel_id=1, source_target_pairs={{0,7},{1,0},{2,1},{3,2},{4,3},{5,4},{6,5},{7,6},{8,15},{9,8},{10,9... | collective-permute-start | bytes 1179656 | tf_op jit(solution)/shard_map/ppermute | solution.py:127
  73.2 3.6 %collective-permute-start.6 = (bf16[384,512]{1,0:T(8,128)(2,1)S(1)}, bf16[384,512]{1,0:T(8,128)(2,1)S(1)}, u32[]{:S(2)}, u32[]{:S(2)}) collective-permute-start(bf16[384,512]{1,0:T(8,128)(2,1)S(1)} %bitcast.75), channel_id=1, source_target_pairs={{0,1},{1,2},{2,3},{3,4},{4,5},{5,6},{6,7},{7,0},{8,9},{9,10},{10,1... | collective-permute-start | bytes 1179656 | tf_op jit(solution)/shard_map/ppermute | solution.py:127
  76.8 4.0 %collective-permute-start.7 = (bf16[192,512]{1,0:T(8,128)(2,1)S(1)}, bf16[192,512]{1,0:T(8,128)(2,1)S(1)}, u32[]{:S(2)}, u32[]{:S(2)}) collective-permute-start(bf16[192,512]{1,0:T(8,128)(2,1)S(1)} %bitcast.84), channel_id=1, source_target_pairs={{0,6},{1,7},{2,0},{3,1},{4,2},{5,3},{6,4},{7,5},{8,14},{9,15},{10,... | collective-permute-start | bytes 589832 | tf_op jit(solution)/shard_map/ppermute | solution.py:127
  80.8 4.0 %collective-permute-start.8 = (bf16[192,512]{1,0:T(8,128)(2,1)S(1)}, bf16[192,512]{1,0:T(8,128)(2,1)S(1)}, u32[]{:S(2)}, u32[]{:S(2)}) collective-permute-start(bf16[192,512]{1,0:T(8,128)(2,1)S(1)} %bitcast.83), channel_id=1, source_target_pairs={{0,2},{1,3},{2,4},{3,5},{4,6},{5,7},{6,0},{7,1},{8,10},{9,11},{10,... | collective-permute-start | bytes 589832 | tf_op jit(solution)/shard_map/ppermute | solution.py:127
  84.8 2.4 %collective-permute-done.7.x_2a = bf16[192,512]{1,0:T(8,128)(2,1)S(1)} collective-permute-done((bf16[192,512]{1,0:T(8,128)(2,1)S(1)}, bf16[192,512]{1,0:T(8,128)(2,1)S(1)}, u32[]{:S(2)}, u32[]{:S(2)}) %collective-permute-start.7) | collective-permute-done | bytes 196640 | tf_op jit(solution)/shard_map/ppermute | solution.py:127
  87.2 2.8 %collective-permute-done.8.x_2b = bf16[192,512]{1,0:T(8,128)(2,1)S(1)} collective-permute-done((bf16[192,512]{1,0:T(8,128)(2,1)S(1)}, bf16[192,512]{1,0:T(8,128)(2,1)S(1)}, u32[]{:S(2)}, u32[]{:S(2)}) %collective-permute-start.8) | collective-permute-done | bytes 196640 | tf_op jit(solution)/shard_map/ppermute | solution.py:127
  91.3 5.9 %shard_map.132 = bf16[8,384,256]{2,1,0:T(8,128)(2,1)} custom-call(s32[1]{0:T(128)} %bitcast.32.index, bf16[384,512]{1,0:T(8,128)(2,1)S(1)} %bitcast.76, bf16[384,512]{1,0:T(8,128)(2,1)S(1)} %collective-permute-done.5.x_1, bf16[384,512]{1,0:T(8,128)(2,1)S(1)} %collective-permute-done.6.x_3, bf16[192,512]{1,0:T(8,128)(2,1)S(1)} %collective-permute-done.7.x_2a, ...), custom_call_target="tpu_custom_call" | custom-call | flops 3000000000 | bytes 10000000 | tf_op jit(solution)/shard_map/pallas_call | solution.py:210
  97.1 9.3 %all-to-all-start.1 = ((bf16[8,384,256]{2,1,0:T(8,128)(2,1)}), bf16[8,384,256]{2,1,0:T(8,128)(2,1)S(1)}, u32[]{:S(2)}, u32[]{:S(2)}) async-start(bf16[8,384,256]{2,1,0:T(8,128)(2,1)} %shard_map.132), calls=%async_computation.1 | async-start | bytes 3145728 | tf_op jit(solution)/shard_map/all_to_all | solution.py:225
  106.5 2.6 %collective-permute-start.12 = (bf16[512,128]{1,0:T(8,128)(2,1)S(1)}, bf16[512,128]{1,0:T(8,128)(2,1)S(1)}, u32[]{:S(2)}, u32[]{:S(2)}) collective-permute-start(bf16[512,128]{1,0:T(8,128)(2,1)S(1)} %fusion.1.refs_0_), channel_id=1, source_target_pairs={{0,7},{1,0},{2,1},{3,2},{4,3},{5,4},{6,5},{7,6},{8,15},{9,8},{10,9... | collective-permute-start | bytes 393224 | tf_op jit(solution)/shard_map/ppermute | solution.py:127
  109.1 4.6 %collective-permute-start.13 = (bf16[512,128]{1,0:T(8,128)(2,1)S(1)}, bf16[512,128]{1,0:T(8,128)(2,1)S(1)}, u32[]{:S(2)}, u32[]{:S(2)}) collective-permute-start(bf16[512,128]{1,0:T(8,128)(2,1)S(1)} %fusion.1.refs_0_), channel_id=1, source_target_pairs={{0,6},{1,7},{2,0},{3,1},{4,2},{5,3},{6,4},{7,5},{8,14},{9,15},{10,... | collective-permute-start | bytes 393224 | tf_op jit(solution)/shard_map/ppermute | solution.py:127
  113.7 5.2 %collective-permute-start.14 = (bf16[512,128]{1,0:T(8,128)(2,1)S(1)}, bf16[512,128]{1,0:T(8,128)(2,1)S(1)}, u32[]{:S(2)}, u32[]{:S(2)}) collective-permute-start(bf16[512,128]{1,0:T(8,128)(2,1)S(1)} %fusion.1.refs_0_), channel_id=1, source_target_pairs={{0,5},{1,6},{2,7},{3,0},{4,1},{5,2},{6,3},{7,4},{8,13},{9,14},{10,... | collective-permute-start | bytes 393224 | tf_op jit(solution)/shard_map/ppermute | solution.py:127
  119.0 25.2 %collective-permute-done.12.refs_7_ = bf16[512,128]{1,0:T(8,128)(2,1)S(1)} collective-permute-done((bf16[512,128]{1,0:T(8,128)(2,1)S(1)}, bf16[512,128]{1,0:T(8,128)(2,1)S(1)}, u32[]{:S(2)}, u32[]{:S(2)}) %collective-permute-start.12) | collective-permute-done | bytes 131104 | tf_op jit(solution)/shard_map/ppermute | solution.py:127
  144.1 7.0 %collective-permute-done.13.refs_6_ = bf16[512,128]{1,0:T(8,128)(2,1)S(1)} collective-permute-done((bf16[512,128]{1,0:T(8,128)(2,1)S(1)}, bf16[512,128]{1,0:T(8,128)(2,1)S(1)}, u32[]{:S(2)}, u32[]{:S(2)}) %collective-permute-start.13) | collective-permute-done | bytes 131104 | tf_op jit(solution)/shard_map/ppermute | solution.py:127
  153.5 14.6 %all-to-all-start.2 = ((bf16[16,24,256]{2,1,0:T(8,128)(2,1)}), bf16[16,24,256]{2,1,0:T(8,128)(2,1)S(1)}, u32[]{:S(2)}, u32[]{:S(2)}) async-start(bf16[16,24,256]{2,1,0:T(8,128)(2,1)} %bitcast.41), calls=%async_computation.2 | async-start | bytes 393216 | tf_op jit(solution)/shard_map/all_to_all | solution.py:237
  168.1 4.5 %collective-permute-start.1 = (bf16[512,128]{1,0:T(8,128)(2,1)S(1)}, bf16[512,128]{1,0:T(8,128)(2,1)S(1)}, u32[]{:S(2)}, u32[]{:S(2)}) collective-permute-start(bf16[512,128]{1,0:T(8,128)(2,1)S(1)} %fusion.1.refs_0_), channel_id=1, source_target_pairs={{0,1},{1,2},{2,3},{3,4},{4,5},{5,6},{6,7},{7,0},{8,9},{9,10},{10,1... | collective-permute-start | bytes 393224 | tf_op jit(solution)/shard_map/ppermute | solution.py:127
  174.6 3.4 %collective-permute-start.3 = (bf16[512,128]{1,0:T(8,128)(2,1)S(1)}, bf16[512,128]{1,0:T(8,128)(2,1)S(1)}, u32[]{:S(2)}, u32[]{:S(2)}) collective-permute-start(bf16[512,128]{1,0:T(8,128)(2,1)S(1)} %fusion.1.refs_0_), channel_id=1, source_target_pairs={{0,3},{1,4},{2,5},{3,6},{4,7},{5,0},{6,1},{7,2},{8,11},{9,12},{10,... | collective-permute-start | bytes 393224 | tf_op jit(solution)/shard_map/ppermute | solution.py:127
  178.0 6.5 %collective-permute-start.4 = (bf16[512,128]{1,0:T(8,128)(2,1)S(1)}, bf16[512,128]{1,0:T(8,128)(2,1)S(1)}, u32[]{:S(2)}, u32[]{:S(2)}) collective-permute-start(bf16[512,128]{1,0:T(8,128)(2,1)S(1)} %fusion.1.refs_0_), channel_id=1, source_target_pairs={{0,4},{1,5},{2,6},{3,7},{4,0},{5,1},{6,2},{7,3},{8,12},{9,13},{10,... | collective-permute-start | bytes 393224 | tf_op jit(solution)/shard_map/ppermute | solution.py:127
  185.0 2.0 collective-permute-done.2.refs_2_
  186.9 7.8 %collective-permute-done.3.refs_3_ = bf16[512,128]{1,0:T(8,128)(2,1)S(1)} collective-permute-done((bf16[512,128]{1,0:T(8,128)(2,1)S(1)}, bf16[512,128]{1,0:T(8,128)(2,1)S(1)}, u32[]{:S(2)}, u32[]{:S(2)}) %collective-permute-start.3) | collective-permute-done | bytes 131104 | tf_op jit(solution)/shard_map/ppermute | solution.py:127
  (41 shorter events, 14.0 us)
Async XLA Ops:
  0.6 55.0 %copy-start.1 = (bf16[1,2048,256]{2,1,0:T(8,128)(2,1)S(1)}, bf16[1,2048,256]{2,1,0:T(8,128)(2,1)}, u32[]{:S(2)}) copy-start(bf16[1,2048,256]{2,1,0:T(8,128)(2,1)} %gate_0.1) | copy-start | bytes 3145732
  0.7 57.5 %copy-start.7 = (f32[31,128]{1,0:T(8,128)S(1)}, f32[31,128]{1,0:T(8,128)}, u32[]{:S(2)}) copy-start(f32[31,128]{1,0:T(8,128)} %param.14) | copy-start | bytes 47620
  3.2 67.6 %all-to-all-start = ((bf16[16,24,512]{2,1,0:T(8,128)(2,1)}), bf16[16,24,512]{2,1,0:T(8,128)(2,1)S(1)}, u32[]{:S(2)}, u32[]{:S(2)}) async-start(bf16[16,24,512]{2,1,0:T(8,128)(2,1)} %bitcast.82), calls=%async_computation | async-start | bytes 786432 | tf_op jit(solution)/shard_map/all_to_all | solution.py:180
  48.0 10.2 %collective-permute-start = (bf16[32,128]{1,0:T(8,128)(2,1)S(1)}, bf16[32,128]{1,0:T(8,128)(2,1)S(1)}, u32[]{:S(2)}, u32[]{:S(2)}) collective-permute-start(bf16[32,128]{1,0:T(8,128)(2,1)S(1)} %slice.268), channel_id=1, source_target_pairs={{0,8},{8,16},{16,24},{24,32},{32,40},{40,48},{48,56},{56,64},{64,7... | collective-permute-start | bytes 24584 | tf_op jit(solution)/shard_map/ppermute | solution.py:189
  49.6 27.2 %collective-permute-start.10 = (bf16[1,2048,256]{2,1,0:T(8,128)(2,1)S(1)}, bf16[1,2048,256]{2,1,0:T(8,128)(2,1)}, u32[]{:S(2)}, u32[]{:S(2)}) collective-permute-start(bf16[1,2048,256]{2,1,0:T(8,128)(2,1)S(1)} %copy-done.2), channel_id=1, source_target_pairs={{0,8},{8,0},{1,9},{9,1},{2,10},{10,2},{3,11},{11,3},{4,12},{12,4},... | collective-permute-start | bytes 3145736 | tf_op jit(solution)/shard_map/ppermute | solution.py:131
  53.7 27.1 %collective-permute-start.11 = (bf16[1,256,2048]{2,1,0:T(8,128)(2,1)}, bf16[1,256,2048]{2,1,0:T(8,128)(2,1)}, u32[]{:S(2)}, u32[]{:S(2)}) collective-permute-start(bf16[1,256,2048]{2,1,0:T(8,128)(2,1)} %down_0.1), channel_id=1, source_target_pairs={{0,8},{8,0},{1,9},{9,1},{2,10},{10,2},{3,11},{11,3},{4,12},{12,4},... | collective-permute-start | bytes 3145736 | tf_op jit(solution)/shard_map/ppermute | solution.py:131
  55.7 29.2 %collective-permute-start.9 = (bf16[1,2048,256]{2,1,0:T(8,128)(2,1)S(1)}, bf16[1,2048,256]{2,1,0:T(8,128)(2,1)}, u32[]{:S(2)}, u32[]{:S(2)}) collective-permute-start(bf16[1,2048,256]{2,1,0:T(8,128)(2,1)S(1)} %copy-done.1), channel_id=1, source_target_pairs={{0,8},{8,0},{1,9},{9,1},{2,10},{10,2},{3,11},{11,3},{4,12},{12,4},... | collective-permute-start | bytes 3145736 | tf_op jit(solution)/shard_map/ppermute | solution.py:131
  70.8 19.2 %collective-permute-start.5 = (bf16[384,512]{1,0:T(8,128)(2,1)S(1)}, bf16[384,512]{1,0:T(8,128)(2,1)S(1)}, u32[]{:S(2)}, u32[]{:S(2)}) collective-permute-start(bf16[384,512]{1,0:T(8,128)(2,1)S(1)} %bitcast.74), channel_id=1, source_target_pairs={{0,7},{1,0},{2,1},{3,2},{4,3},{5,4},{6,5},{7,6},{8,15},{9,8},{10,9... | collective-permute-start | bytes 1179656 | tf_op jit(solution)/shard_map/ppermute | solution.py:127
  73.2 16.9 %collective-permute-start.6 = (bf16[384,512]{1,0:T(8,128)(2,1)S(1)}, bf16[384,512]{1,0:T(8,128)(2,1)S(1)}, u32[]{:S(2)}, u32[]{:S(2)}) collective-permute-start(bf16[384,512]{1,0:T(8,128)(2,1)S(1)} %bitcast.75), channel_id=1, source_target_pairs={{0,1},{1,2},{2,3},{3,4},{4,5},{5,6},{6,7},{7,0},{8,9},{9,10},{10,1... | collective-permute-start | bytes 1179656 | tf_op jit(solution)/shard_map/ppermute | solution.py:127
  76.8 10.4 %collective-permute-start.7 = (bf16[192,512]{1,0:T(8,128)(2,1)S(1)}, bf16[192,512]{1,0:T(8,128)(2,1)S(1)}, u32[]{:S(2)}, u32[]{:S(2)}) collective-permute-start(bf16[192,512]{1,0:T(8,128)(2,1)S(1)} %bitcast.84), channel_id=1, source_target_pairs={{0,6},{1,7},{2,0},{3,1},{4,2},{5,3},{6,4},{7,5},{8,14},{9,15},{10,... | collective-permute-start | bytes 589832 | tf_op jit(solution)/shard_map/ppermute | solution.py:127
  80.8 9.2 %collective-permute-start.8 = (bf16[192,512]{1,0:T(8,128)(2,1)S(1)}, bf16[192,512]{1,0:T(8,128)(2,1)S(1)}, u32[]{:S(2)}, u32[]{:S(2)}) collective-permute-start(bf16[192,512]{1,0:T(8,128)(2,1)S(1)} %bitcast.83), channel_id=1, source_target_pairs={{0,2},{1,3},{2,4},{3,5},{4,6},{5,7},{6,0},{7,1},{8,10},{9,11},{10,... | collective-permute-start | bytes 589832 | tf_op jit(solution)/shard_map/ppermute | solution.py:127
  97.1 55.3 %all-to-all-start.1 = ((bf16[8,384,256]{2,1,0:T(8,128)(2,1)}), bf16[8,384,256]{2,1,0:T(8,128)(2,1)S(1)}, u32[]{:S(2)}, u32[]{:S(2)}) async-start(bf16[8,384,256]{2,1,0:T(8,128)(2,1)} %shard_map.132), calls=%async_computation.1 | async-start | bytes 3145728 | tf_op jit(solution)/shard_map/all_to_all | solution.py:225
  106.5 78.0 %copy-start = (s32[128,2]{0,1:T(2,128)S(1)}, s32[128,2]{0,1:T(2,128)}, u32[]{:S(2)}) copy-start(s32[128,2]{0,1:T(2,128)} %param.19) | copy-start | bytes 3076
  106.5 78.0 %copy-start.6 = (f32[128,2]{0,1:T(2,128)S(1)}, f32[128,2]{0,1:T(2,128)}, u32[]{:S(2)}) copy-start(f32[128,2]{0,1:T(2,128)} %param.20) | copy-start | bytes 3076
  106.5 88.3 %copy-start.4 = (bf16[1024,256]{1,0:T(8,128)(2,1)S(1)}, bf16[1024,256]{1,0:T(8,128)(2,1)}, u32[]{:S(2)}) copy-start(bf16[1024,256]{1,0:T(8,128)(2,1)} %refs_9_.1) | copy-start | bytes 1572868
  106.5 88.3 %copy-start.5 = (f32[1024]{0:T(1024)S(1)}, f32[1024]{0:T(1024)}, u32[]{:S(2)}) copy-start(f32[1024]{0:T(1024)} %param.15) | copy-start | bytes 12292
  106.5 37.6 %collective-permute-start.12 = (bf16[512,128]{1,0:T(8,128)(2,1)S(1)}, bf16[512,128]{1,0:T(8,128)(2,1)S(1)}, u32[]{:S(2)}, u32[]{:S(2)}) collective-permute-start(bf16[512,128]{1,0:T(8,128)(2,1)S(1)} %fusion.1.refs_0_), channel_id=1, source_target_pairs={{0,7},{1,0},{2,1},{3,2},{4,3},{5,4},{6,5},{7,6},{8,15},{9,8},{10,9... | collective-permute-start | bytes 393224 | tf_op jit(solution)/shard_map/ppermute | solution.py:127
  109.1 42.0 %collective-permute-start.13 = (bf16[512,128]{1,0:T(8,128)(2,1)S(1)}, bf16[512,128]{1,0:T(8,128)(2,1)S(1)}, u32[]{:S(2)}, u32[]{:S(2)}) collective-permute-start(bf16[512,128]{1,0:T(8,128)(2,1)S(1)} %fusion.1.refs_0_), channel_id=1, source_target_pairs={{0,6},{1,7},{2,0},{3,1},{4,2},{5,3},{6,4},{7,5},{8,14},{9,15},{10,... | collective-permute-start | bytes 393224 | tf_op jit(solution)/shard_map/ppermute | solution.py:127
  113.7 38.7 %collective-permute-start.14 = (bf16[512,128]{1,0:T(8,128)(2,1)S(1)}, bf16[512,128]{1,0:T(8,128)(2,1)S(1)}, u32[]{:S(2)}, u32[]{:S(2)}) collective-permute-start(bf16[512,128]{1,0:T(8,128)(2,1)S(1)} %fusion.1.refs_0_), channel_id=1, source_target_pairs={{0,5},{1,6},{2,7},{3,0},{4,1},{5,2},{6,3},{7,4},{8,13},{9,14},{10,... | collective-permute-start | bytes 393224 | tf_op jit(solution)/shard_map/ppermute | solution.py:127
  153.5 43.2 %all-to-all-start.2 = ((bf16[16,24,256]{2,1,0:T(8,128)(2,1)}), bf16[16,24,256]{2,1,0:T(8,128)(2,1)S(1)}, u32[]{:S(2)}, u32[]{:S(2)}) async-start(bf16[16,24,256]{2,1,0:T(8,128)(2,1)} %bitcast.41), calls=%async_computation.2 | async-start | bytes 393216 | tf_op jit(solution)/shard_map/all_to_all | solution.py:237
  168.1 16.9 %collective-permute-start.1 = (bf16[512,128]{1,0:T(8,128)(2,1)S(1)}, bf16[512,128]{1,0:T(8,128)(2,1)S(1)}, u32[]{:S(2)}, u32[]{:S(2)}) collective-permute-start(bf16[512,128]{1,0:T(8,128)(2,1)S(1)} %fusion.1.refs_0_), channel_id=1, source_target_pairs={{0,1},{1,2},{2,3},{3,4},{4,5},{5,6},{6,7},{7,0},{8,9},{9,10},{10,1... | collective-permute-start | bytes 393224 | tf_op jit(solution)/shard_map/ppermute | solution.py:127
  172.7 14.3 %collective-permute-start.2 = (bf16[512,128]{1,0:T(8,128)(2,1)S(1)}, bf16[512,128]{1,0:T(8,128)(2,1)S(1)}, u32[]{:S(2)}, u32[]{:S(2)}) collective-permute-start(bf16[512,128]{1,0:T(8,128)(2,1)S(1)} %fusion.1.refs_0_), channel_id=1, source_target_pairs={{0,2},{1,3},{2,4},{3,5},{4,6},{5,7},{6,0},{7,1},{8,10},{9,11},{10,... | collective-permute-start | bytes 393224 | tf_op jit(solution)/shard_map/ppermute | solution.py:127
  174.6 20.1 %collective-permute-start.3 = (bf16[512,128]{1,0:T(8,128)(2,1)S(1)}, bf16[512,128]{1,0:T(8,128)(2,1)S(1)}, u32[]{:S(2)}, u32[]{:S(2)}) collective-permute-start(bf16[512,128]{1,0:T(8,128)(2,1)S(1)} %fusion.1.refs_0_), channel_id=1, source_target_pairs={{0,3},{1,4},{2,5},{3,6},{4,7},{5,0},{6,1},{7,2},{8,11},{9,12},{10,... | collective-permute-start | bytes 393224 | tf_op jit(solution)/shard_map/ppermute | solution.py:127
  178.0 16.7 %collective-permute-start.4 = (bf16[512,128]{1,0:T(8,128)(2,1)S(1)}, bf16[512,128]{1,0:T(8,128)(2,1)S(1)}, u32[]{:S(2)}, u32[]{:S(2)}) collective-permute-start(bf16[512,128]{1,0:T(8,128)(2,1)S(1)} %fusion.1.refs_0_), channel_id=1, source_target_pairs={{0,4},{1,5},{2,6},{3,7},{4,0},{5,1},{6,2},{7,3},{8,12},{9,13},{10,... | collective-permute-start | bytes 393224 | tf_op jit(solution)/shard_map/ppermute | solution.py:127
  (2 other events, 50.1 us)

commit v7 on v6

--- a/solution.py
+++ b/solution.py
@@ -195,9 +195,11 @@
         start = halo - taps + 1 + offset
         total = total + conv_taps[offset][None, :] * padded[start : start + length]
     convolved = total.astype(bf16)
-    across, from_back = moved(convolved, parts), [moved(convolved, k) for k in (1, 2)]
-    from_front = [moved(convolved, -k) for k in range(1, parts)]
+    across = moved(convolved, parts)
+    from_back = [moved(convolved, k) for k in range(1, parts - 1)]
+    from_front = [moved(convolved, -k) for k in range(1, parts - 1)]
     from_back.append(moved(convolved, parts - 1))
+    from_front.append(moved(convolved, 1 - parts))
 
     rows = n_z * capacity
     arrived, _ = lax.optimization_barrier((arrived, convolved))
@@ -223,7 +225,6 @@
         cost_estimate=cost(3 * 10**9, 10**7),
     )(quarter, x_0, x_1, x_3, x_2a, x_2b, gate_w, up_w, down_w, gate_b, up_b, down_b)
     pieces = lax.all_to_all(pieces, "tp", split_axis=0, concat_axis=0, tiled=True)
-    pieces, from_front = lax.optimization_barrier((pieces, from_front))
     step = rows // 2
     sums = pl.pallas_call(
         sum_kernel,

time: 198 us -> 198 us (level)
  the two profiles are of different devices: /device:TPU:68 before, /device:TPU:65 now
where the time goes in v7:
time: 198 us; the launch traced here: 196 us
  starting transfers between devices  112 us (57%)
  blocking collectives  35.7 us (18%)
  waiting for transfers between devices  28.6 us (14%)
  Pallas kernels  15.6 us (8%)
    all_to_all x1, starting transfers between devices, step_on_device(): lax.all_to_all(outgoing.reshape(experts, capacity, wide), 'z', split_axis...  44.2 us
    ppermute x11, starting transfers between devices, moved(): return lax.ppermute(value, 'tp', [(i, (i + by) % n) for i in range(n)])  38.3 us
    all_to_all x1, blocking collectives, step_on_device(): lax.all_to_all(pieces, 'tp', split_axis=0, concat_axis=0, tiled=True)  35.7 us
    ppermute x11, waiting for transfers between devices, moved(): return lax.ppermute(value, 'tp', [(i, (i + by) % n) for i in range(n)])  23 us
    all_to_all x1, starting transfers between devices, step_on_device(): lax.all_to_all(sums.reshape(n_z, capacity, columns), 'z', split_axis=0, c...  19.4 us
    pallas_call x1, Pallas kernels, step_on_device(): pl.pallas_call(experts_kernel, out_shape=jax.ShapeDtypeStruct((n_tp, rows...  8.89 us
    ppermute x3, starting transfers between devices, partner(): return lax.ppermute(value, 'core', [(0, 1), (1, 0)])  6.34 us
    all_to_all x1, waiting for transfers between devices, step_on_device(): lax.all_to_all(outgoing.reshape(experts, capacity, wide), 'z', split_axis...  5.6 us
  transfers between devices with their start and end apart: 17, of which 6 were waited for; matrix products, arithmetic and copies ran while one was open for 1% of the time, Pallas kernels for 1%

profile of v7, /device:TPU:65, one launch (start us, length us, event | category | flops | bytes accessed | tf_op | source)
XLA Modules:
  0.0 196.3 jit_solution(13758753683679020568)
XLA Ops:
  0.7 2.6 %shard_map.133 = bf16[384,512]{1,0:T(8,128)(2,1)} custom-call(s32[1]{0:T(128)} %bitcast.35.index, s32[2,128]{1,0:T(2,128)} %bitcast.78, bf16[128,2048]{1,0:T(8,128)(2,1)} %rows.1, f32[1,2048]{1,0:T(1,128)} %bitcast.85), custom_call_target="tpu_custom_call" | custom-call | flops 100000000 | bytes 1000000 | tf_op jit(solution)/shard_map/pallas_call | solution.py:171
  3.2 44.2 %all-to-all-start = ((bf16[16,24,512]{2,1,0:T(8,128)(2,1)}), bf16[16,24,512]{2,1,0:T(8,128)(2,1)S(1)}, u32[]{:S(2)}, u32[]{:S(2)}) async-start(bf16[16,24,512]{2,1,0:T(8,128)(2,1)} %bitcast.82), calls=%async_computation | async-start | bytes 786432 | tf_op jit(solution)/shard_map/all_to_all | solution.py:180
  48.5 4.1 %collective-permute-start = (bf16[32,128]{1,0:T(8,128)(2,1)S(1)}, bf16[32,128]{1,0:T(8,128)(2,1)S(1)}, u32[]{:S(2)}, u32[]{:S(2)}) collective-permute-start(bf16[32,128]{1,0:T(8,128)(2,1)S(1)} %slice.268), channel_id=1, source_target_pairs={{0,8},{8,16},{16,24},{24,32},{32,40},{40,48},{48,56},{56,64},{64,7... | collective-permute-start | bytes 24584 | tf_op jit(solution)/shard_map/ppermute | solution.py:189
  52.7 2.0 collective-permute-start.12
  54.6 2.4 %collective-permute-start.13 = (bf16[1,2048,256]{2,1,0:T(8,128)(2,1)S(1)}, bf16[1,2048,256]{2,1,0:T(8,128)(2,1)}, u32[]{:S(2)}, u32[]{:S(2)}) collective-permute-start(bf16[1,2048,256]{2,1,0:T(8,128)(2,1)S(1)} %copy-done.2), channel_id=1, source_target_pairs={{0,8},{8,0},{1,9},{9,1},{2,10},{10,2},{3,11},{11,3},{4,12},{12,4},... | collective-permute-start | bytes 3145736 | tf_op jit(solution)/shard_map/ppermute | solution.py:131
  57.1 2.0 collective-permute-start.14
  59.8 5.6 %all-to-all-done = bf16[16,24,512]{2,1,0:T(8,128)(2,1)S(1)} async-done(((bf16[16,24,512]{2,1,0:T(8,128)(2,1)}), bf16[16,24,512]{2,1,0:T(8,128)(2,1)S(1)}, u32[]{:S(2)}, u32[]{:S(2)}) %all-to-all-start) | async-done | bytes 393248 | tf_op jit(solution)/shard_map/all_to_all | solution.py:180
  65.4 5.4 %collective-permute-start.8 = (bf16[384,512]{1,0:T(8,128)(2,1)S(1)}, bf16[384,512]{1,0:T(8,128)(2,1)S(1)}, u32[]{:S(2)}, u32[]{:S(2)}) collective-permute-start(bf16[384,512]{1,0:T(8,128)(2,1)S(1)} %bitcast.74), channel_id=1, source_target_pairs={{0,7},{1,0},{2,1},{3,2},{4,3},{5,4},{6,5},{7,6},{8,15},{9,8},{10,9... | collective-permute-start | bytes 1179656 | tf_op jit(solution)/shard_map/ppermute | solution.py:127
  72.9 4.1 %collective-permute-start.10 = (bf16[192,512]{1,0:T(8,128)(2,1)S(1)}, bf16[192,512]{1,0:T(8,128)(2,1)S(1)}, u32[]{:S(2)}, u32[]{:S(2)}) collective-permute-start(bf16[192,512]{1,0:T(8,128)(2,1)S(1)} %bitcast.84), channel_id=1, source_target_pairs={{0,6},{1,7},{2,0},{3,1},{4,2},{5,3},{6,4},{7,5},{8,14},{9,15},{10,... | collective-permute-start | bytes 589832 | tf_op jit(solution)/shard_map/ppermute | solution.py:127
  77.1 2.1 %collective-permute-start.11 = (bf16[192,512]{1,0:T(8,128)(2,1)S(1)}, bf16[192,512]{1,0:T(8,128)(2,1)S(1)}, u32[]{:S(2)}, u32[]{:S(2)}) collective-permute-start(bf16[192,512]{1,0:T(8,128)(2,1)S(1)} %bitcast.83), channel_id=1, source_target_pairs={{0,2},{1,3},{2,4},{3,5},{4,6},{5,7},{6,0},{7,1},{8,10},{9,11},{10,... | collective-permute-start | bytes 589832 | tf_op jit(solution)/shard_map/ppermute | solution.py:127
  79.2 5.6 %collective-permute-done.10.x_2a = bf16[192,512]{1,0:T(8,128)(2,1)S(1)} collective-permute-done((bf16[192,512]{1,0:T(8,128)(2,1)S(1)}, bf16[192,512]{1,0:T(8,128)(2,1)S(1)}, u32[]{:S(2)}, u32[]{:S(2)}) %collective-permute-start.10) | collective-permute-done | bytes 196640 | tf_op jit(solution)/shard_map/ppermute | solution.py:127
  84.7 4.6 %collective-permute-done.11.x_2b = bf16[192,512]{1,0:T(8,128)(2,1)S(1)} collective-permute-done((bf16[192,512]{1,0:T(8,128)(2,1)S(1)}, bf16[192,512]{1,0:T(8,128)(2,1)S(1)}, u32[]{:S(2)}, u32[]{:S(2)}) %collective-permute-start.11) | collective-permute-done | bytes 196640 | tf_op jit(solution)/shard_map/ppermute | solution.py:127
  90.6 8.9 %shard_map.134 = bf16[8,384,256]{2,1,0:T(8,128)(2,1)S(1)} custom-call(s32[1]{0:T(128)} %bitcast.35.index, bf16[384,512]{1,0:T(8,128)(2,1)S(1)} %bitcast.76, bf16[384,512]{1,0:T(8,128)(2,1)S(1)} %collective-permute-done.8.x_1, bf16[384,512]{1,0:T(8,128)(2,1)S(1)} %collective-permute-done.9.x_3, bf16[192,512]{1,0:T(8,128)(2,1)S(1)} %collective-permute-done.10.x_2a, ...), custom_call_target="tpu_custom_call" | custom-call | flops 3000000000 | bytes 10000000 | tf_op jit(solution)/shard_map/pallas_call | solution.py:212
  99.5 35.7 %all_to_all.15.pieces = bf16[8,384,256]{2,1,0:T(8,128)(2,1)S(1)} all-to-all(bf16[8,384,256]{2,1,0:T(8,128)(2,1)S(1)} %shard_map.134), channel_id=1, replica_groups=mesh['grp'=2,'z'=16,'core'=2,'tp'=8] {'tp'}, dimensions={0} | all-to-all | bytes 3145728 | tf_op jit(solution)/shard_map/all_to_all | solution.py:227
  136.2 19.4 %all-to-all-start.2 = ((bf16[16,24,256]{2,1,0:T(8,128)(2,1)}), bf16[16,24,256]{2,1,0:T(8,128)(2,1)S(1)}, u32[]{:S(2)}, u32[]{:S(2)}) async-start(bf16[16,24,256]{2,1,0:T(8,128)(2,1)} %bitcast.41), calls=%async_computation.2 | async-start | bytes 393216 | tf_op jit(solution)/shard_map/all_to_all | solution.py:238
  155.6 2.3 %collective-permute-start.1 = (bf16[512,128]{1,0:T(8,128)(2,1)S(1)}, bf16[512,128]{1,0:T(8,128)(2,1)S(1)}, u32[]{:S(2)}, u32[]{:S(2)}) collective-permute-start(bf16[512,128]{1,0:T(8,128)(2,1)S(1)} %fusion.1.refs_0_), channel_id=1, source_target_pairs={{0,1},{1,2},{2,3},{3,4},{4,5},{5,6},{6,7},{7,0},{8,9},{9,10},{10,1... | collective-permute-start | bytes 393224 | tf_op jit(solution)/shard_map/ppermute | solution.py:127
  157.9 3.7 %collective-permute-start.2 = (bf16[512,128]{1,0:T(8,128)(2,1)S(1)}, bf16[512,128]{1,0:T(8,128)(2,1)S(1)}, u32[]{:S(2)}, u32[]{:S(2)}) collective-permute-start(bf16[512,128]{1,0:T(8,128)(2,1)S(1)} %fusion.1.refs_0_), channel_id=1, source_target_pairs={{0,2},{1,3},{2,4},{3,5},{4,6},{5,7},{6,0},{7,1},{8,10},{9,11},{10,... | collective-permute-start | bytes 393224 | tf_op jit(solution)/shard_map/ppermute | solution.py:127
  161.6 4.3 %collective-permute-start.3 = (bf16[512,128]{1,0:T(8,128)(2,1)S(1)}, bf16[512,128]{1,0:T(8,128)(2,1)S(1)}, u32[]{:S(2)}, u32[]{:S(2)}) collective-permute-start(bf16[512,128]{1,0:T(8,128)(2,1)S(1)} %fusion.1.refs_0_), channel_id=1, source_target_pairs={{0,3},{1,4},{2,5},{3,6},{4,7},{5,0},{6,1},{7,2},{8,11},{9,12},{10,... | collective-permute-start | bytes 393224 | tf_op jit(solution)/shard_map/ppermute | solution.py:127
  166.0 3.2 %collective-permute-start.4 = (bf16[512,128]{1,0:T(8,128)(2,1)S(1)}, bf16[512,128]{1,0:T(8,128)(2,1)S(1)}, u32[]{:S(2)}, u32[]{:S(2)}) collective-permute-start(bf16[512,128]{1,0:T(8,128)(2,1)S(1)} %fusion.1.refs_0_), channel_id=1, source_target_pairs={{0,4},{1,5},{2,6},{3,7},{4,0},{5,1},{6,2},{7,3},{8,12},{9,13},{10,... | collective-permute-start | bytes 393224 | tf_op jit(solution)/shard_map/ppermute | solution.py:127
  169.2 4.8 %collective-permute-start.5 = (bf16[512,128]{1,0:T(8,128)(2,1)S(1)}, bf16[512,128]{1,0:T(8,128)(2,1)S(1)}, u32[]{:S(2)}, u32[]{:S(2)}) collective-permute-start(bf16[512,128]{1,0:T(8,128)(2,1)S(1)} %fusion.1.refs_0_), channel_id=1, source_target_pairs={{0,5},{1,6},{2,7},{3,0},{4,1},{5,2},{6,3},{7,4},{8,13},{9,14},{10,... | collective-permute-start | bytes 393224 | tf_op jit(solution)/shard_map/ppermute | solution.py:127
  174.1 3.1 %collective-permute-start.6 = (bf16[512,128]{1,0:T(8,128)(2,1)S(1)}, bf16[512,128]{1,0:T(8,128)(2,1)S(1)}, u32[]{:S(2)}, u32[]{:S(2)}) collective-permute-start(bf16[512,128]{1,0:T(8,128)(2,1)S(1)} %fusion.1.refs_0_), channel_id=1, source_target_pairs={{0,6},{1,7},{2,0},{3,1},{4,2},{5,3},{6,4},{7,5},{8,14},{9,15},{10,... | collective-permute-start | bytes 393224 | tf_op jit(solution)/shard_map/ppermute | solution.py:127
  177.2 3.1 %collective-permute-start.7 = (bf16[512,128]{1,0:T(8,128)(2,1)S(1)}, bf16[512,128]{1,0:T(8,128)(2,1)S(1)}, u32[]{:S(2)}, u32[]{:S(2)}) collective-permute-start(bf16[512,128]{1,0:T(8,128)(2,1)S(1)} %fusion.1.refs_0_), channel_id=1, source_target_pairs={{0,7},{1,0},{2,1},{3,2},{4,3},{5,4},{6,5},{7,6},{8,15},{9,8},{10,9... | collective-permute-start | bytes 393224 | tf_op jit(solution)/shard_map/ppermute | solution.py:127
  182.7 6.6 %collective-permute-done.6.refs_6_ = bf16[512,128]{1,0:T(8,128)(2,1)S(1)} collective-permute-done((bf16[512,128]{1,0:T(8,128)(2,1)S(1)}, bf16[512,128]{1,0:T(8,128)(2,1)S(1)}, u32[]{:S(2)}, u32[]{:S(2)}) %collective-permute-start.6) | collective-permute-done | bytes 131104 | tf_op jit(solution)/shard_map/ppermute | solution.py:127
  189.3 4.4 %collective-permute-done.7.refs_7_ = bf16[512,128]{1,0:T(8,128)(2,1)S(1)} collective-permute-done((bf16[512,128]{1,0:T(8,128)(2,1)S(1)}, bf16[512,128]{1,0:T(8,128)(2,1)S(1)}, u32[]{:S(2)}, u32[]{:S(2)}) %collective-permute-start.7) | collective-permute-done | bytes 131104 | tf_op jit(solution)/shard_map/ppermute | solution.py:127
  (40 shorter events, 11.0 us)
Async XLA Ops:
  0.6 52.0 %copy-start.1 = (bf16[1,2048,256]{2,1,0:T(8,128)(2,1)S(1)}, bf16[1,2048,256]{2,1,0:T(8,128)(2,1)}, u32[]{:S(2)}) copy-start(bf16[1,2048,256]{2,1,0:T(8,128)(2,1)} %gate_0.1) | copy-start | bytes 3145732
  0.6 54.0 %copy-start.2 = (bf16[1,2048,256]{2,1,0:T(8,128)(2,1)S(1)}, bf16[1,2048,256]{2,1,0:T(8,128)(2,1)}, u32[]{:S(2)}) copy-start(bf16[1,2048,256]{2,1,0:T(8,128)(2,1)} %up_0.1) | copy-start | bytes 3145732
  0.7 58.4 %copy-start.7 = (f32[31,128]{1,0:T(8,128)S(1)}, f32[31,128]{1,0:T(8,128)}, u32[]{:S(2)}) copy-start(f32[31,128]{1,0:T(8,128)} %param.14) | copy-start | bytes 47620
  3.2 62.2 %all-to-all-start = ((bf16[16,24,512]{2,1,0:T(8,128)(2,1)}), bf16[16,24,512]{2,1,0:T(8,128)(2,1)S(1)}, u32[]{:S(2)}, u32[]{:S(2)}) async-start(bf16[16,24,512]{2,1,0:T(8,128)(2,1)} %bitcast.82), calls=%async_computation | async-start | bytes 786432 | tf_op jit(solution)/shard_map/all_to_all | solution.py:180
  48.5 10.6 %collective-permute-start = (bf16[32,128]{1,0:T(8,128)(2,1)S(1)}, bf16[32,128]{1,0:T(8,128)(2,1)S(1)}, u32[]{:S(2)}, u32[]{:S(2)}) collective-permute-start(bf16[32,128]{1,0:T(8,128)(2,1)S(1)} %slice.268), channel_id=1, source_target_pairs={{0,8},{8,16},{16,24},{24,32},{32,40},{40,48},{48,56},{56,64},{64,7... | collective-permute-start | bytes 24584 | tf_op jit(solution)/shard_map/ppermute | solution.py:189
  52.7 20.2 %collective-permute-start.12 = (bf16[1,2048,256]{2,1,0:T(8,128)(2,1)S(1)}, bf16[1,2048,256]{2,1,0:T(8,128)(2,1)}, u32[]{:S(2)}, u32[]{:S(2)}) collective-permute-start(bf16[1,2048,256]{2,1,0:T(8,128)(2,1)S(1)} %copy-done.1), channel_id=1, source_target_pairs={{0,8},{8,0},{1,9},{9,1},{2,10},{10,2},{3,11},{11,3},{4,12},{12,4},... | collective-permute-start | bytes 3145736 | tf_op jit(solution)/shard_map/ppermute | solution.py:131
  54.6 22.4 %collective-permute-start.13 = (bf16[1,2048,256]{2,1,0:T(8,128)(2,1)S(1)}, bf16[1,2048,256]{2,1,0:T(8,128)(2,1)}, u32[]{:S(2)}, u32[]{:S(2)}) collective-permute-start(bf16[1,2048,256]{2,1,0:T(8,128)(2,1)S(1)} %copy-done.2), channel_id=1, source_target_pairs={{0,8},{8,0},{1,9},{9,1},{2,10},{10,2},{3,11},{11,3},{4,12},{12,4},... | collective-permute-start | bytes 3145736 | tf_op jit(solution)/shard_map/ppermute | solution.py:131
  57.1 22.1 %collective-permute-start.14 = (bf16[1,256,2048]{2,1,0:T(8,128)(2,1)}, bf16[1,256,2048]{2,1,0:T(8,128)(2,1)}, u32[]{:S(2)}, u32[]{:S(2)}) collective-permute-start(bf16[1,256,2048]{2,1,0:T(8,128)(2,1)} %down_0.1), channel_id=1, source_target_pairs={{0,8},{8,0},{1,9},{9,1},{2,10},{10,2},{3,11},{11,3},{4,12},{12,4},... | collective-permute-start | bytes 3145736 | tf_op jit(solution)/shard_map/ppermute | solution.py:131
  65.4 23.9 %collective-permute-start.8 = (bf16[384,512]{1,0:T(8,128)(2,1)S(1)}, bf16[384,512]{1,0:T(8,128)(2,1)S(1)}, u32[]{:S(2)}, u32[]{:S(2)}) collective-permute-start(bf16[384,512]{1,0:T(8,128)(2,1)S(1)} %bitcast.74), channel_id=1, source_target_pairs={{0,7},{1,0},{2,1},{3,2},{4,3},{5,4},{6,5},{7,6},{8,15},{9,8},{10,9... | collective-permute-start | bytes 1179656 | tf_op jit(solution)/shard_map/ppermute | solution.py:127
  70.9 18.5 %collective-permute-start.9 = (bf16[384,512]{1,0:T(8,128)(2,1)S(1)}, bf16[384,512]{1,0:T(8,128)(2,1)S(1)}, u32[]{:S(2)}, u32[]{:S(2)}) collective-permute-start(bf16[384,512]{1,0:T(8,128)(2,1)S(1)} %bitcast.75), channel_id=1, source_target_pairs={{0,1},{1,2},{2,3},{3,4},{4,5},{5,6},{6,7},{7,0},{8,9},{9,10},{10,1... | collective-permute-start | bytes 1179656 | tf_op jit(solution)/shard_map/ppermute | solution.py:127
  72.9 11.8 %collective-permute-start.10 = (bf16[192,512]{1,0:T(8,128)(2,1)S(1)}, bf16[192,512]{1,0:T(8,128)(2,1)S(1)}, u32[]{:S(2)}, u32[]{:S(2)}) collective-permute-start(bf16[192,512]{1,0:T(8,128)(2,1)S(1)} %bitcast.84), channel_id=1, source_target_pairs={{0,6},{1,7},{2,0},{3,1},{4,2},{5,3},{6,4},{7,5},{8,14},{9,15},{10,... | collective-permute-start | bytes 589832 | tf_op jit(solution)/shard_map/ppermute | solution.py:127
  77.1 12.3 %collective-permute-start.11 = (bf16[192,512]{1,0:T(8,128)(2,1)S(1)}, bf16[192,512]{1,0:T(8,128)(2,1)S(1)}, u32[]{:S(2)}, u32[]{:S(2)}) collective-permute-start(bf16[192,512]{1,0:T(8,128)(2,1)S(1)} %bitcast.83), channel_id=1, source_target_pairs={{0,2},{1,3},{2,4},{3,5},{4,6},{5,7},{6,0},{7,1},{8,10},{9,11},{10,... | collective-permute-start | bytes 589832 | tf_op jit(solution)/shard_map/ppermute | solution.py:127
  135.2 45.2 %copy-start = (s32[128,2]{0,1:T(2,128)S(1)}, s32[128,2]{0,1:T(2,128)}, u32[]{:S(2)}) copy-start(s32[128,2]{0,1:T(2,128)} %param.19) | copy-start | bytes 3076
  135.2 45.2 %copy-start.6 = (f32[128,2]{0,1:T(2,128)S(1)}, f32[128,2]{0,1:T(2,128)}, u32[]{:S(2)}) copy-start(f32[128,2]{0,1:T(2,128)} %param.20) | copy-start | bytes 3076
  135.2 58.5 %copy-start.4 = (bf16[1024,256]{1,0:T(8,128)(2,1)S(1)}, bf16[1024,256]{1,0:T(8,128)(2,1)}, u32[]{:S(2)}) copy-start(bf16[1024,256]{1,0:T(8,128)(2,1)} %refs_9_.1) | copy-start | bytes 1572868
  135.2 58.5 %copy-start.5 = (f32[1024]{0:T(1024)S(1)}, f32[1024]{0:T(1024)}, u32[]{:S(2)}) copy-start(f32[1024]{0:T(1024)} %param.15) | copy-start | bytes 12292
  136.2 59.3 %all-to-all-start.2 = ((bf16[16,24,256]{2,1,0:T(8,128)(2,1)}), bf16[16,24,256]{2,1,0:T(8,128)(2,1)S(1)}, u32[]{:S(2)}, u32[]{:S(2)}) async-start(bf16[16,24,256]{2,1,0:T(8,128)(2,1)} %bitcast.41), calls=%async_computation.2 | async-start | bytes 393216 | tf_op jit(solution)/shard_map/all_to_all | solution.py:238
  155.6 18.4 %collective-permute-start.1 = (bf16[512,128]{1,0:T(8,128)(2,1)S(1)}, bf16[512,128]{1,0:T(8,128)(2,1)S(1)}, u32[]{:S(2)}, u32[]{:S(2)}) collective-permute-start(bf16[512,128]{1,0:T(8,128)(2,1)S(1)} %fusion.1.refs_0_), channel_id=1, source_target_pairs={{0,1},{1,2},{2,3},{3,4},{4,5},{5,6},{6,7},{7,0},{8,9},{9,10},{10,1... | collective-permute-start | bytes 393224 | tf_op jit(solution)/shard_map/ppermute | solution.py:127
  157.9 19.2 %collective-permute-start.2 = (bf16[512,128]{1,0:T(8,128)(2,1)S(1)}, bf16[512,128]{1,0:T(8,128)(2,1)S(1)}, u32[]{:S(2)}, u32[]{:S(2)}) collective-permute-start(bf16[512,128]{1,0:T(8,128)(2,1)S(1)} %fusion.1.refs_0_), channel_id=1, source_target_pairs={{0,2},{1,3},{2,4},{3,5},{4,6},{5,7},{6,0},{7,1},{8,10},{9,11},{10,... | collective-permute-start | bytes 393224 | tf_op jit(solution)/shard_map/ppermute | solution.py:127
  161.6 19.2 %collective-permute-start.3 = (bf16[512,128]{1,0:T(8,128)(2,1)S(1)}, bf16[512,128]{1,0:T(8,128)(2,1)S(1)}, u32[]{:S(2)}, u32[]{:S(2)}) collective-permute-start(bf16[512,128]{1,0:T(8,128)(2,1)S(1)} %fusion.1.refs_0_), channel_id=1, source_target_pairs={{0,3},{1,4},{2,5},{3,6},{4,7},{5,0},{6,1},{7,2},{8,11},{9,12},{10,... | collective-permute-start | bytes 393224 | tf_op jit(solution)/shard_map/ppermute | solution.py:127
  166.0 16.7 %collective-permute-start.4 = (bf16[512,128]{1,0:T(8,128)(2,1)S(1)}, bf16[512,128]{1,0:T(8,128)(2,1)S(1)}, u32[]{:S(2)}, u32[]{:S(2)}) collective-permute-start(bf16[512,128]{1,0:T(8,128)(2,1)S(1)} %fusion.1.refs_0_), channel_id=1, source_target_pairs={{0,4},{1,5},{2,6},{3,7},{4,0},{5,1},{6,2},{7,3},{8,12},{9,13},{10,... | collective-permute-start | bytes 393224 | tf_op jit(solution)/shard_map/ppermute | solution.py:127
  169.2 13.5 %collective-permute-start.5 = (bf16[512,128]{1,0:T(8,128)(2,1)S(1)}, bf16[512,128]{1,0:T(8,128)(2,1)S(1)}, u32[]{:S(2)}, u32[]{:S(2)}) collective-permute-start(bf16[512,128]{1,0:T(8,128)(2,1)S(1)} %fusion.1.refs_0_), channel_id=1, source_target_pairs={{0,5},{1,6},{2,7},{3,0},{4,1},{5,2},{6,3},{7,4},{8,13},{9,14},{10,... | collective-permute-start | bytes 393224 | tf_op jit(solution)/shard_map/ppermute | solution.py:127
  174.1 15.2 %collective-permute-start.6 = (bf16[512,128]{1,0:T(8,128)(2,1)S(1)}, bf16[512,128]{1,0:T(8,128)(2,1)S(1)}, u32[]{:S(2)}, u32[]{:S(2)}) collective-permute-start(bf16[512,128]{1,0:T(8,128)(2,1)S(1)} %fusion.1.refs_0_), channel_id=1, source_target_pairs={{0,6},{1,7},{2,0},{3,1},{4,2},{5,3},{6,4},{7,5},{8,14},{9,15},{10,... | collective-permute-start | bytes 393224 | tf_op jit(solution)/shard_map/ppermute | solution.py:127
  177.2 16.4 %collective-permute-start.7 = (bf16[512,128]{1,0:T(8,128)(2,1)S(1)}, bf16[512,128]{1,0:T(8,128)(2,1)S(1)}, u32[]{:S(2)}, u32[]{:S(2)}) collective-permute-start(bf16[512,128]{1,0:T(8,128)(2,1)S(1)} %fusion.1.refs_0_), channel_id=1, source_target_pairs={{0,7},{1,0},{2,1},{3,2},{4,3},{5,4},{6,5},{7,6},{8,15},{9,8},{10,9... | collective-permute-start | bytes 393224 | tf_op jit(solution)/shard_map/ppermute | solution.py:127
  (1 other events, 1.2 us)

commit v8 on v7

--- a/solution.py
+++ b/solution.py
@@ -25,16 +25,13 @@
     named = functools.reduce(jnp.add, hits).astype(bf16)
     before = lax.broadcasted_iota(jnp.int32, (tokens, tokens), 0)
     after = lax.broadcasted_iota(jnp.int32, (tokens, tokens), 1)
-    places = dot(named, (before < after).astype(f32).astype(bf16)).astype(bf16)
+    places = dot(named, (before < after).astype(f32).astype(bf16))
+    place = lax.broadcasted_iota(jnp.int32, (experts, capacity, tokens), 1).astype(f32)
+    at_place = places[:, None, :] == place
     slots = experts * capacity
-    first = lax.broadcasted_iota(jnp.int32, (slots, experts), 1) * capacity
-    slot = lax.broadcasted_iota(jnp.int32, (slots, experts), 0)
-    own = (slot >= first) & (slot < first + capacity)
-    spread = own.astype(f32).astype(bf16)
-    first_of = jnp.sum(jnp.where(own, first, 0), axis=1, keepdims=True)
-    offset = (lax.broadcasted_iota(jnp.int32, (slots, 1), 0) - first_of).astype(f32)
-    at_place = dot(spread, places) == offset
-    return [(dot(spread, hit.astype(bf16)) > 0.5) & at_place for hit in hits]
+    return [
+        jnp.where(at_place, hit[:, None, :], 0.0).reshape(slots, tokens) for hit in hits
+    ]
 
 
 def dispatch_kernel(experts, capacity, index, routes, rows, gain, out):
@@ -45,13 +42,13 @@
     own = rows[:, pl.ds(start, width)].astype(f32)
     normed = (own * scale * gain[:, pl.ds(start, width)]).astype(bf16)
     matches = slot_hits(routes[...], experts, capacity)
-    picker = functools.reduce(jnp.logical_or, matches).astype(f32).astype(bf16)
+    picker = functools.reduce(jnp.add, matches).astype(bf16)
     out[...] = dot(picker, normed).astype(bf16)
 
 
 def combiner_kernel(experts, capacity, routes, weights, high, low):
     matches = slot_hits(routes[...], experts, capacity)
-    terms = [jnp.where(m, weights[j : j + 1, :], 0.0) for j, m in enumerate(matches)]
+    terms = [m * weights[j : j + 1, :] for j, m in enumerate(matches)]
     total = functools.reduce(jnp.add, terms).T
     rounded = total.astype(bf16)
     high[...] = rounded
@@ -63,16 +60,11 @@
 
 
 def experts_kernel(
-    index, x_0, x_1, x_3, x_2a, x_2b, gate_0, up_0, down_0, gate_1, up_1, down_1, out, wide, tall, held_out, sems, out_sems
+    index, x_0, x_1, x_3, x_2a, x_2b, gate_0, up_0, gate_1, up_1, down_1, down_0, out, tall, held_out, sem, out_sems
 ):
     blocks, width = out.shape[0], out.shape[2]
-    arriving = (wide.at[0], wide.at[1], tall)
-    copies = [
-        pltpu.make_async_copy(w.at[0], h, sems.at[i])
-        for i, (w, h) in enumerate(zip((gate_1, up_1, down_1), arriving))
-    ]
-    for copy in copies:
-        copy.start()
+    load = pltpu.make_async_copy(down_0.at[0], tall, sem)
+    load.start()
     depth = x_0.shape[1]
     parts = gate_0.shape[1] // depth
     rows = (x_0[...], x_1[...], jnp.concatenate([x_2a[...], x_2b[...]], axis=0), x_3[...])
@@ -80,19 +72,17 @@
 
     def projected(weight):
         spans = [pl.ds(pl.multiple_of(p, depth), depth) for p in places]
-        return functools.reduce(jnp.add, [dot(r, weight[s, :]) for r, s in zip(rows, spans)])
-
-    gate = projected(gate_0.at[0])
-    hidden = [(jax.nn.silu(gate) * projected(up_0.at[0])).astype(bf16)]
-    copies[0].wait()
-    gate = projected(wide.at[0])
-    copies[1].wait()
-    hidden.append((jax.nn.silu(gate) * projected(wide.at[1])).astype(bf16))
-    copies[2].wait()
+        return functools.reduce(jnp.add, [dot(r, weight[0, s, :]) for r, s in zip(rows, spans)])
+
+    hidden = [
+        (jax.nn.silu(projected(g)) * projected(u)).astype(bf16)
+        for g, u in ((gate_0, up_0), (gate_1, up_1))
+    ]
+    load.wait()
     stores = []
     for b in range(blocks):
         span = slice(b * width, (b + 1) * width)
-        piece = dot(hidden[0], down_0[0, :, span]) + dot(hidden[1], tall[:, span])
+        piece = dot(hidden[0], tall[:, span]) + dot(hidden[1], down_1[0, :, span])
         held_out[b] = piece.astype(bf16)
         stores.append(pltpu.make_async_copy(held_out.at[b], out.at[b], out_sems.at[b]))
         stores[-1].start()
@@ -212,18 +202,17 @@
     pieces = pl.pallas_call(
         experts_kernel,
         out_shape=jax.ShapeDtypeStruct((n_tp, rows, columns), bf16),
-        in_specs=[smem] + [vmem] * 8 + [hbm] * 3,
+        in_specs=[smem] + [vmem] * 10 + [pl.BlockSpec(memory_space=pltpu.HBM)],
         out_specs=hbm,
         scratch_shapes=[
-            pltpu.VMEM((2, width, units), bf16),
             pltpu.VMEM((units, width), bf16),
             pltpu.VMEM((n_tp, rows, columns), bf16),
-            pltpu.SemaphoreType.DMA((3,)),
+            pltpu.SemaphoreType.DMA,
             pltpu.SemaphoreType.DMA((n_tp,)),
         ],
         compiler_params=params(24),
         cost_estimate=cost(3 * 10**9, 10**7),
-    )(quarter, x_0, x_1, x_3, x_2a, x_2b, gate_w, up_w, down_w, gate_b, up_b, down_b)
+    )(quarter, x_0, x_1, x_3, x_2a, x_2b, gate_w, up_w, gate_b, up_b, down_b, down_w)
     pieces = lax.all_to_all(pieces, "tp", split_axis=0, concat_axis=0, tiled=True)
     step = rows // 2
     sums = pl.pallas_call(
@@ -255,6 +244,7 @@
         compiler_params=params(16),
         cost_estimate=cost(10**8, 10**6),
     )(high, low, results)
+    routed_rows, from_back = lax.optimization_barrier((routed_rows, from_back))
     step = length // 2
     gathered = [convolved, *from_back, across, *from_front[::-1]]
     mixer_rows = pl.pallas_call(

time: 198 us -> 196 us (0.990)
  transfers between devices with their start and end apart: 17 -> 17, of which waited for: 6 -> 5; matrix products, arithmetic and copies ran while one was open for 1% -> 1% of each run, Pallas kernels for 1% -> 1%
where the time goes in v8:
time: 196 us; the launch traced here: 195 us
  starting transfers between devices  112 us (57%)
  blocking collectives  35.7 us (18%)
  waiting for transfers between devices  27.9 us (14%)
  Pallas kernels  14.9 us (8%)
    all_to_all x1, starting transfers between devices, step_on_device(): lax.all_to_all(outgoing.reshape(experts, capacity, wide), 'z', split_axis...  44.2 us
    ppermute x11, starting transfers between devices, moved(): return lax.ppermute(value, 'tp', [(i, (i + by) % n) for i in range(n)])  38.3 us
    all_to_all x1, blocking collectives, step_on_device(): lax.all_to_all(pieces, 'tp', split_axis=0, concat_axis=0, tiled=True)  35.7 us
    ppermute x11, waiting for transfers between devices, moved(): return lax.ppermute(value, 'tp', [(i, (i + by) % n) for i in range(n)])  22.3 us
    all_to_all x1, starting transfers between devices, step_on_device(): lax.all_to_all(sums.reshape(n_z, capacity, columns), 'z', split_axis=0, c...  19.5 us
    pallas_call x1, Pallas kernels, step_on_device(): pl.pallas_call(experts_kernel, out_shape=jax.ShapeDtypeStruct((n_tp, rows...  8.6 us
    ppermute x3, starting transfers between devices, partner(): return lax.ppermute(value, 'core', [(0, 1), (1, 0)])  6.34 us
    all_to_all x1, waiting for transfers between devices, step_on_device(): lax.all_to_all(outgoing.reshape(experts, capacity, wide), 'z', split_axis...  5.59 us
  transfers between devices with their start and end apart: 17, of which 5 were waited for; matrix products, arithmetic and copies ran while one was open for 1% of the time, Pallas kernels for 1%

profile of v8, /device:TPU:65, one launch (start us, length us, event | category | flops | bytes accessed | tf_op | source)
XLA Modules:
  0.0 195.0 jit_solution(11421243809977262205)
XLA Ops:
  0.7 2.4 %shard_map.132 = bf16[384,512]{1,0:T(8,128)(2,1)} custom-call(s32[1]{0:T(128)} %bitcast.34.index, s32[2,128]{1,0:T(2,128)} %bitcast.78, bf16[128,2048]{1,0:T(8,128)(2,1)} %rows.1, f32[1,2048]{1,0:T(1,128)} %bitcast.85), custom_call_target="tpu_custom_call" | custom-call | flops 100000000 | bytes 1000000 | tf_op jit(solution)/shard_map/pallas_call | solution.py:161
  3.1 44.2 %all-to-all-start = ((bf16[16,24,512]{2,1,0:T(8,128)(2,1)}), bf16[16,24,512]{2,1,0:T(8,128)(2,1)S(1)}, u32[]{:S(2)}, u32[]{:S(2)}) async-start(bf16[16,24,512]{2,1,0:T(8,128)(2,1)} %bitcast.82), calls=%async_computation | async-start | bytes 786432 | tf_op jit(solution)/shard_map/all_to_all | solution.py:170
  48.3 4.2 %collective-permute-start = (bf16[32,128]{1,0:T(8,128)(2,1)S(1)}, bf16[32,128]{1,0:T(8,128)(2,1)S(1)}, u32[]{:S(2)}, u32[]{:S(2)}) collective-permute-start(bf16[32,128]{1,0:T(8,128)(2,1)S(1)} %slice.268), channel_id=1, source_target_pairs={{0,8},{8,16},{16,24},{24,32},{32,40},{40,48},{48,56},{56,64},{64,7... | collective-permute-start | bytes 24584 | tf_op jit(solution)/shard_map/ppermute | solution.py:179
  52.5 2.0 %collective-permute-start.5 = (bf16[1,2048,256]{2,1,0:T(8,128)(2,1)S(1)}, bf16[1,2048,256]{2,1,0:T(8,128)(2,1)}, u32[]{:S(2)}, u32[]{:S(2)}) collective-permute-start(bf16[1,2048,256]{2,1,0:T(8,128)(2,1)S(1)} %copy-done.1), channel_id=1, source_target_pairs={{0,8},{8,0},{1,9},{9,1},{2,10},{10,2},{3,11},{11,3},{4,12},{12,4},... | collective-permute-start | bytes 3145736 | tf_op jit(solution)/shard_map/ppermute | solution.py:121
  54.5 2.4 %collective-permute-start.6 = (bf16[1,2048,256]{2,1,0:T(8,128)(2,1)S(1)}, bf16[1,2048,256]{2,1,0:T(8,128)(2,1)}, u32[]{:S(2)}, u32[]{:S(2)}) collective-permute-start(bf16[1,2048,256]{2,1,0:T(8,128)(2,1)S(1)} %copy-done.2), channel_id=1, source_target_pairs={{0,8},{8,0},{1,9},{9,1},{2,10},{10,2},{3,11},{11,3},{4,12},{12,4},... | collective-permute-start | bytes 3145736 | tf_op jit(solution)/shard_map/ppermute | solution.py:121
  56.9 2.0 %collective-permute-start.7 = (bf16[1,256,2048]{2,1,0:T(8,128)(2,1)}, bf16[1,256,2048]{2,1,0:T(8,128)(2,1)}, u32[]{:S(2)}, u32[]{:S(2)}) collective-permute-start(bf16[1,256,2048]{2,1,0:T(8,128)(2,1)} %down_0.1), channel_id=1, source_target_pairs={{0,8},{8,0},{1,9},{9,1},{2,10},{10,2},{3,11},{11,3},{4,12},{12,4},... | collective-permute-start | bytes 3145736 | tf_op jit(solution)/shard_map/ppermute | solution.py:121
  59.7 5.6 %all-to-all-done = bf16[16,24,512]{2,1,0:T(8,128)(2,1)S(1)} async-done(((bf16[16,24,512]{2,1,0:T(8,128)(2,1)}), bf16[16,24,512]{2,1,0:T(8,128)(2,1)S(1)}, u32[]{:S(2)}, u32[]{:S(2)}) %all-to-all-start) | async-done | bytes 393248 | tf_op jit(solution)/shard_map/all_to_all | solution.py:170
  65.3 5.5 %collective-permute-start.1 = (bf16[384,512]{1,0:T(8,128)(2,1)S(1)}, bf16[384,512]{1,0:T(8,128)(2,1)S(1)}, u32[]{:S(2)}, u32[]{:S(2)}) collective-permute-start(bf16[384,512]{1,0:T(8,128)(2,1)S(1)} %bitcast.74), channel_id=1, source_target_pairs={{0,7},{1,0},{2,1},{3,2},{4,3},{5,4},{6,5},{7,6},{8,15},{9,8},{10,9... | collective-permute-start | bytes 1179656 | tf_op jit(solution)/shard_map/ppermute | solution.py:117
  72.7 4.1 %collective-permute-start.3 = (bf16[192,512]{1,0:T(8,128)(2,1)S(1)}, bf16[192,512]{1,0:T(8,128)(2,1)S(1)}, u32[]{:S(2)}, u32[]{:S(2)}) collective-permute-start(bf16[192,512]{1,0:T(8,128)(2,1)S(1)} %bitcast.84), channel_id=1, source_target_pairs={{0,6},{1,7},{2,0},{3,1},{4,2},{5,3},{6,4},{7,5},{8,14},{9,15},{10,... | collective-permute-start | bytes 589832 | tf_op jit(solution)/shard_map/ppermute | solution.py:117
  76.9 2.1 %collective-permute-start.4 = (bf16[192,512]{1,0:T(8,128)(2,1)S(1)}, bf16[192,512]{1,0:T(8,128)(2,1)S(1)}, u32[]{:S(2)}, u32[]{:S(2)}) collective-permute-start(bf16[192,512]{1,0:T(8,128)(2,1)S(1)} %bitcast.83), channel_id=1, source_target_pairs={{0,2},{1,3},{2,4},{3,5},{4,6},{5,7},{6,0},{7,1},{8,10},{9,11},{10,... | collective-permute-start | bytes 589832 | tf_op jit(solution)/shard_map/ppermute | solution.py:117
  79.0 5.6 %collective-permute-done.3.x_2a = bf16[192,512]{1,0:T(8,128)(2,1)S(1)} collective-permute-done((bf16[192,512]{1,0:T(8,128)(2,1)S(1)}, bf16[192,512]{1,0:T(8,128)(2,1)S(1)}, u32[]{:S(2)}, u32[]{:S(2)}) %collective-permute-start.3) | collective-permute-done | bytes 196640 | tf_op jit(solution)/shard_map/ppermute | solution.py:117
  84.6 4.6 %collective-permute-done.4.x_2b = bf16[192,512]{1,0:T(8,128)(2,1)S(1)} collective-permute-done((bf16[192,512]{1,0:T(8,128)(2,1)S(1)}, bf16[192,512]{1,0:T(8,128)(2,1)S(1)}, u32[]{:S(2)}, u32[]{:S(2)}) %collective-permute-start.4) | collective-permute-done | bytes 196640 | tf_op jit(solution)/shard_map/ppermute | solution.py:117
  90.4 8.6 %shard_map.133 = bf16[8,384,256]{2,1,0:T(8,128)(2,1)S(1)} custom-call(s32[1]{0:T(128)} %bitcast.34.index, bf16[384,512]{1,0:T(8,128)(2,1)S(1)} %bitcast.76, bf16[384,512]{1,0:T(8,128)(2,1)S(1)} %collective-permute-done.1.x_1, bf16[384,512]{1,0:T(8,128)(2,1)S(1)} %collective-permute-done.2.x_3, bf16[192,512]{1,0:T(8,128)(2,1)S(1)} %collective-permute-done.3.x_2a, ...), custom_call_target="tpu_custom_call" | custom-call | flops 3000000000 | bytes 10000000 | tf_op jit(solution)/shard_map/pallas_call | solution.py:202
  99.0 35.7 %all_to_all.15.pieces = bf16[8,384,256]{2,1,0:T(8,128)(2,1)S(1)} all-to-all(bf16[8,384,256]{2,1,0:T(8,128)(2,1)S(1)} %shard_map.133), channel_id=1, replica_groups=mesh['grp'=2,'z'=16,'core'=2,'tp'=8] {'tp'}, dimensions={0} | all-to-all | bytes 3145728 | tf_op jit(solution)/shard_map/all_to_all | solution.py:216
  135.7 19.5 %all-to-all-start.2 = ((bf16[16,24,256]{2,1,0:T(8,128)(2,1)}), bf16[16,24,256]{2,1,0:T(8,128)(2,1)S(1)}, u32[]{:S(2)}, u32[]{:S(2)}) async-start(bf16[16,24,256]{2,1,0:T(8,128)(2,1)} %bitcast.40), calls=%async_computation.2 | async-start | bytes 393216 | tf_op jit(solution)/shard_map/all_to_all | solution.py:227
  155.2 3.7 %collective-permute-start.10 = (bf16[512,128]{1,0:T(8,128)(2,1)S(1)}, bf16[512,128]{1,0:T(8,128)(2,1)S(1)}, u32[]{:S(2)}, u32[]{:S(2)}) collective-permute-start(bf16[512,128]{1,0:T(8,128)(2,1)S(1)} %fusion.1.refs_0_), channel_id=1, source_target_pairs={{0,3},{1,4},{2,5},{3,6},{4,7},{5,0},{6,1},{7,2},{8,11},{9,12},{10,... | collective-permute-start | bytes 393224 | tf_op jit(solution)/shard_map/ppermute | solution.py:117
  159.0 2.0 %collective-permute-start.8 = (bf16[512,128]{1,0:T(8,128)(2,1)S(1)}, bf16[512,128]{1,0:T(8,128)(2,1)S(1)}, u32[]{:S(2)}, u32[]{:S(2)}) collective-permute-start(bf16[512,128]{1,0:T(8,128)(2,1)S(1)} %fusion.1.refs_0_), channel_id=1, source_target_pairs={{0,1},{1,2},{2,3},{3,4},{4,5},{5,6},{6,7},{7,0},{8,9},{9,10},{10,1... | collective-permute-start | bytes 393224 | tf_op jit(solution)/shard_map/ppermute | solution.py:117
  160.9 4.6 %collective-permute-start.9 = (bf16[512,128]{1,0:T(8,128)(2,1)S(1)}, bf16[512,128]{1,0:T(8,128)(2,1)S(1)}, u32[]{:S(2)}, u32[]{:S(2)}) collective-permute-start(bf16[512,128]{1,0:T(8,128)(2,1)S(1)} %fusion.1.refs_0_), channel_id=1, source_target_pairs={{0,2},{1,3},{2,4},{3,5},{4,6},{5,7},{6,0},{7,1},{8,10},{9,11},{10,... | collective-permute-start | bytes 393224 | tf_op jit(solution)/shard_map/ppermute | solution.py:117
  165.5 3.2 %collective-permute-start.11 = (bf16[512,128]{1,0:T(8,128)(2,1)S(1)}, bf16[512,128]{1,0:T(8,128)(2,1)S(1)}, u32[]{:S(2)}, u32[]{:S(2)}) collective-permute-start(bf16[512,128]{1,0:T(8,128)(2,1)S(1)} %fusion.1.refs_0_), channel_id=1, source_target_pairs={{0,4},{1,5},{2,6},{3,7},{4,0},{5,1},{6,2},{7,3},{8,12},{9,13},{10,... | collective-permute-start | bytes 393224 | tf_op jit(solution)/shard_map/ppermute | solution.py:117
  168.8 4.8 %collective-permute-start.12 = (bf16[512,128]{1,0:T(8,128)(2,1)S(1)}, bf16[512,128]{1,0:T(8,128)(2,1)S(1)}, u32[]{:S(2)}, u32[]{:S(2)}) collective-permute-start(bf16[512,128]{1,0:T(8,128)(2,1)S(1)} %fusion.1.refs_0_), channel_id=1, source_target_pairs={{0,5},{1,6},{2,7},{3,0},{4,1},{5,2},{6,3},{7,4},{8,13},{9,14},{10,... | collective-permute-start | bytes 393224 | tf_op jit(solution)/shard_map/ppermute | solution.py:117
  173.6 3.1 %collective-permute-start.13 = (bf16[512,128]{1,0:T(8,128)(2,1)S(1)}, bf16[512,128]{1,0:T(8,128)(2,1)S(1)}, u32[]{:S(2)}, u32[]{:S(2)}) collective-permute-start(bf16[512,128]{1,0:T(8,128)(2,1)S(1)} %fusion.1.refs_0_), channel_id=1, source_target_pairs={{0,6},{1,7},{2,0},{3,1},{4,2},{5,3},{6,4},{7,5},{8,14},{9,15},{10,... | collective-permute-start | bytes 393224 | tf_op jit(solution)/shard_map/ppermute | solution.py:117
  176.8 3.1 %collective-permute-start.14 = (bf16[512,128]{1,0:T(8,128)(2,1)S(1)}, bf16[512,128]{1,0:T(8,128)(2,1)S(1)}, u32[]{:S(2)}, u32[]{:S(2)}) collective-permute-start(bf16[512,128]{1,0:T(8,128)(2,1)S(1)} %fusion.1.refs_0_), channel_id=1, source_target_pairs={{0,7},{1,0},{2,1},{3,2},{4,3},{5,4},{6,5},{7,6},{8,15},{9,8},{10,9... | collective-permute-start | bytes 393224 | tf_op jit(solution)/shard_map/ppermute | solution.py:117
  181.1 7.7 %collective-permute-done.13.refs_6_ = bf16[512,128]{1,0:T(8,128)(2,1)S(1)} collective-permute-done((bf16[512,128]{1,0:T(8,128)(2,1)S(1)}, bf16[512,128]{1,0:T(8,128)(2,1)S(1)}, u32[]{:S(2)}, u32[]{:S(2)}) %collective-permute-start.13) | collective-permute-done | bytes 131104 | tf_op jit(solution)/shard_map/ppermute | solution.py:117
  188.8 4.4 %collective-permute-done.14.refs_7_ = bf16[512,128]{1,0:T(8,128)(2,1)S(1)} collective-permute-done((bf16[512,128]{1,0:T(8,128)(2,1)S(1)}, bf16[512,128]{1,0:T(8,128)(2,1)S(1)}, u32[]{:S(2)}, u32[]{:S(2)}) %collective-permute-start.14) | collective-permute-done | bytes 131104 | tf_op jit(solution)/shard_map/ppermute | solution.py:117
  (40 shorter events, 9.0 us)
Async XLA Ops:
  0.6 51.9 %copy-start.1 = (bf16[1,2048,256]{2,1,0:T(8,128)(2,1)S(1)}, bf16[1,2048,256]{2,1,0:T(8,128)(2,1)}, u32[]{:S(2)}) copy-start(bf16[1,2048,256]{2,1,0:T(8,128)(2,1)} %gate_0.1) | copy-start | bytes 3145732
  0.6 53.8 %copy-start.2 = (bf16[1,2048,256]{2,1,0:T(8,128)(2,1)S(1)}, bf16[1,2048,256]{2,1,0:T(8,128)(2,1)}, u32[]{:S(2)}) copy-start(bf16[1,2048,256]{2,1,0:T(8,128)(2,1)} %up_0.1) | copy-start | bytes 3145732
  0.7 58.2 %copy-start.7 = (f32[31,128]{1,0:T(8,128)S(1)}, f32[31,128]{1,0:T(8,128)}, u32[]{:S(2)}) copy-start(f32[31,128]{1,0:T(8,128)} %param.14) | copy-start | bytes 47620
  3.1 62.2 %all-to-all-start = ((bf16[16,24,512]{2,1,0:T(8,128)(2,1)}), bf16[16,24,512]{2,1,0:T(8,128)(2,1)S(1)}, u32[]{:S(2)}, u32[]{:S(2)}) async-start(bf16[16,24,512]{2,1,0:T(8,128)(2,1)} %bitcast.82), calls=%async_computation | async-start | bytes 786432 | tf_op jit(solution)/shard_map/all_to_all | solution.py:170
  48.3 10.6 %collective-permute-start = (bf16[32,128]{1,0:T(8,128)(2,1)S(1)}, bf16[32,128]{1,0:T(8,128)(2,1)S(1)}, u32[]{:S(2)}, u32[]{:S(2)}) collective-permute-start(bf16[32,128]{1,0:T(8,128)(2,1)S(1)} %slice.268), channel_id=1, source_target_pairs={{0,8},{8,16},{16,24},{24,32},{32,40},{40,48},{48,56},{56,64},{64,7... | collective-permute-start | bytes 24584 | tf_op jit(solution)/shard_map/ppermute | solution.py:179
  52.5 20.2 %collective-permute-start.5 = (bf16[1,2048,256]{2,1,0:T(8,128)(2,1)S(1)}, bf16[1,2048,256]{2,1,0:T(8,128)(2,1)}, u32[]{:S(2)}, u32[]{:S(2)}) collective-permute-start(bf16[1,2048,256]{2,1,0:T(8,128)(2,1)S(1)} %copy-done.1), channel_id=1, source_target_pairs={{0,8},{8,0},{1,9},{9,1},{2,10},{10,2},{3,11},{11,3},{4,12},{12,4},... | collective-permute-start | bytes 3145736 | tf_op jit(solution)/shard_map/ppermute | solution.py:121
  54.5 22.4 %collective-permute-start.6 = (bf16[1,2048,256]{2,1,0:T(8,128)(2,1)S(1)}, bf16[1,2048,256]{2,1,0:T(8,128)(2,1)}, u32[]{:S(2)}, u32[]{:S(2)}) collective-permute-start(bf16[1,2048,256]{2,1,0:T(8,128)(2,1)S(1)} %copy-done.2), channel_id=1, source_target_pairs={{0,8},{8,0},{1,9},{9,1},{2,10},{10,2},{3,11},{11,3},{4,12},{12,4},... | collective-permute-start | bytes 3145736 | tf_op jit(solution)/shard_map/ppermute | solution.py:121
  56.9 22.1 %collective-permute-start.7 = (bf16[1,256,2048]{2,1,0:T(8,128)(2,1)}, bf16[1,256,2048]{2,1,0:T(8,128)(2,1)}, u32[]{:S(2)}, u32[]{:S(2)}) collective-permute-start(bf16[1,256,2048]{2,1,0:T(8,128)(2,1)} %down_0.1), channel_id=1, source_target_pairs={{0,8},{8,0},{1,9},{9,1},{2,10},{10,2},{3,11},{11,3},{4,12},{12,4},... | collective-permute-start | bytes 3145736 | tf_op jit(solution)/shard_map/ppermute | solution.py:121
  65.3 23.9 %collective-permute-start.1 = (bf16[384,512]{1,0:T(8,128)(2,1)S(1)}, bf16[384,512]{1,0:T(8,128)(2,1)S(1)}, u32[]{:S(2)}, u32[]{:S(2)}) collective-permute-start(bf16[384,512]{1,0:T(8,128)(2,1)S(1)} %bitcast.74), channel_id=1, source_target_pairs={{0,7},{1,0},{2,1},{3,2},{4,3},{5,4},{6,5},{7,6},{8,15},{9,8},{10,9... | collective-permute-start | bytes 1179656 | tf_op jit(solution)/shard_map/ppermute | solution.py:117
  70.7 18.4 %collective-permute-start.2 = (bf16[384,512]{1,0:T(8,128)(2,1)S(1)}, bf16[384,512]{1,0:T(8,128)(2,1)S(1)}, u32[]{:S(2)}, u32[]{:S(2)}) collective-permute-start(bf16[384,512]{1,0:T(8,128)(2,1)S(1)} %bitcast.75), channel_id=1, source_target_pairs={{0,1},{1,2},{2,3},{3,4},{4,5},{5,6},{6,7},{7,0},{8,9},{9,10},{10,1... | collective-permute-start | bytes 1179656 | tf_op jit(solution)/shard_map/ppermute | solution.py:117
  72.7 11.8 %collective-permute-start.3 = (bf16[192,512]{1,0:T(8,128)(2,1)S(1)}, bf16[192,512]{1,0:T(8,128)(2,1)S(1)}, u32[]{:S(2)}, u32[]{:S(2)}) collective-permute-start(bf16[192,512]{1,0:T(8,128)(2,1)S(1)} %bitcast.84), channel_id=1, source_target_pairs={{0,6},{1,7},{2,0},{3,1},{4,2},{5,3},{6,4},{7,5},{8,14},{9,15},{10,... | collective-permute-start | bytes 589832 | tf_op jit(solution)/shard_map/ppermute | solution.py:117
  76.9 12.3 %collective-permute-start.4 = (bf16[192,512]{1,0:T(8,128)(2,1)S(1)}, bf16[192,512]{1,0:T(8,128)(2,1)S(1)}, u32[]{:S(2)}, u32[]{:S(2)}) collective-permute-start(bf16[192,512]{1,0:T(8,128)(2,1)S(1)} %bitcast.83), channel_id=1, source_target_pairs={{0,2},{1,3},{2,4},{3,5},{4,6},{5,7},{6,0},{7,1},{8,10},{9,11},{10,... | collective-permute-start | bytes 589832 | tf_op jit(solution)/shard_map/ppermute | solution.py:117
  134.7 45.2 %copy-start = (s32[128,2]{0,1:T(2,128)S(1)}, s32[128,2]{0,1:T(2,128)}, u32[]{:S(2)}) copy-start(s32[128,2]{0,1:T(2,128)} %param.19) | copy-start | bytes 3076
  134.7 45.2 %copy-start.6 = (f32[128,2]{0,1:T(2,128)S(1)}, f32[128,2]{0,1:T(2,128)}, u32[]{:S(2)}) copy-start(f32[128,2]{0,1:T(2,128)} %param.20) | copy-start | bytes 3076
  134.7 58.5 %copy-start.4 = (bf16[1024,256]{1,0:T(8,128)(2,1)S(1)}, bf16[1024,256]{1,0:T(8,128)(2,1)}, u32[]{:S(2)}) copy-start(bf16[1024,256]{1,0:T(8,128)(2,1)} %refs_9_.1) | copy-start | bytes 1572868
  134.7 58.5 %copy-start.5 = (f32[1024]{0:T(1024)S(1)}, f32[1024]{0:T(1024)}, u32[]{:S(2)}) copy-start(f32[1024]{0:T(1024)} %param.15) | copy-start | bytes 12292
  135.7 44.5 %all-to-all-start.2 = ((bf16[16,24,256]{2,1,0:T(8,128)(2,1)}), bf16[16,24,256]{2,1,0:T(8,128)(2,1)S(1)}, u32[]{:S(2)}, u32[]{:S(2)}) async-start(bf16[16,24,256]{2,1,0:T(8,128)(2,1)} %bitcast.40), calls=%async_computation.2 | async-start | bytes 393216 | tf_op jit(solution)/shard_map/all_to_all | solution.py:227
  155.2 18.4 %collective-permute-start.10 = (bf16[512,128]{1,0:T(8,128)(2,1)S(1)}, bf16[512,128]{1,0:T(8,128)(2,1)S(1)}, u32[]{:S(2)}, u32[]{:S(2)}) collective-permute-start(bf16[512,128]{1,0:T(8,128)(2,1)S(1)} %fusion.1.refs_0_), channel_id=1, source_target_pairs={{0,3},{1,4},{2,5},{3,6},{4,7},{5,0},{6,1},{7,2},{8,11},{9,12},{10,... | collective-permute-start | bytes 393224 | tf_op jit(solution)/shard_map/ppermute | solution.py:117
  159.0 17.8 %collective-permute-start.8 = (bf16[512,128]{1,0:T(8,128)(2,1)S(1)}, bf16[512,128]{1,0:T(8,128)(2,1)S(1)}, u32[]{:S(2)}, u32[]{:S(2)}) collective-permute-start(bf16[512,128]{1,0:T(8,128)(2,1)S(1)} %fusion.1.refs_0_), channel_id=1, source_target_pairs={{0,1},{1,2},{2,3},{3,4},{4,5},{5,6},{6,7},{7,0},{8,9},{9,10},{10,1... | collective-permute-start | bytes 393224 | tf_op jit(solution)/shard_map/ppermute | solution.py:117
  160.9 20.2 %collective-permute-start.9 = (bf16[512,128]{1,0:T(8,128)(2,1)S(1)}, bf16[512,128]{1,0:T(8,128)(2,1)S(1)}, u32[]{:S(2)}, u32[]{:S(2)}) collective-permute-start(bf16[512,128]{1,0:T(8,128)(2,1)S(1)} %fusion.1.refs_0_), channel_id=1, source_target_pairs={{0,2},{1,3},{2,4},{3,5},{4,6},{5,7},{6,0},{7,1},{8,10},{9,11},{10,... | collective-permute-start | bytes 393224 | tf_op jit(solution)/shard_map/ppermute | solution.py:117
  165.5 15.5 %collective-permute-start.11 = (bf16[512,128]{1,0:T(8,128)(2,1)S(1)}, bf16[512,128]{1,0:T(8,128)(2,1)S(1)}, u32[]{:S(2)}, u32[]{:S(2)}) collective-permute-start(bf16[512,128]{1,0:T(8,128)(2,1)S(1)} %fusion.1.refs_0_), channel_id=1, source_target_pairs={{0,4},{1,5},{2,6},{3,7},{4,0},{5,1},{6,2},{7,3},{8,12},{9,13},{10,... | collective-permute-start | bytes 393224 | tf_op jit(solution)/shard_map/ppermute | solution.py:117
  168.8 12.3 %collective-permute-start.12 = (bf16[512,128]{1,0:T(8,128)(2,1)S(1)}, bf16[512,128]{1,0:T(8,128)(2,1)S(1)}, u32[]{:S(2)}, u32[]{:S(2)}) collective-permute-start(bf16[512,128]{1,0:T(8,128)(2,1)S(1)} %fusion.1.refs_0_), channel_id=1, source_target_pairs={{0,5},{1,6},{2,7},{3,0},{4,1},{5,2},{6,3},{7,4},{8,13},{9,14},{10,... | collective-permute-start | bytes 393224 | tf_op jit(solution)/shard_map/ppermute | solution.py:117
  173.6 15.2 %collective-permute-start.13 = (bf16[512,128]{1,0:T(8,128)(2,1)S(1)}, bf16[512,128]{1,0:T(8,128)(2,1)S(1)}, u32[]{:S(2)}, u32[]{:S(2)}) collective-permute-start(bf16[512,128]{1,0:T(8,128)(2,1)S(1)} %fusion.1.refs_0_), channel_id=1, source_target_pairs={{0,6},{1,7},{2,0},{3,1},{4,2},{5,3},{6,4},{7,5},{8,14},{9,15},{10,... | collective-permute-start | bytes 393224 | tf_op jit(solution)/shard_map/ppermute | solution.py:117
  176.8 16.4 %collective-permute-start.14 = (bf16[512,128]{1,0:T(8,128)(2,1)S(1)}, bf16[512,128]{1,0:T(8,128)(2,1)S(1)}, u32[]{:S(2)}, u32[]{:S(2)}) collective-permute-start(bf16[512,128]{1,0:T(8,128)(2,1)S(1)} %fusion.1.refs_0_), channel_id=1, source_target_pairs={{0,7},{1,0},{2,1},{3,2},{4,3},{5,4},{6,5},{7,6},{8,15},{9,8},{10,9... | collective-permute-start | bytes 393224 | tf_op jit(solution)/shard_map/ppermute | solution.py:117
  (1 other events, 1.2 us)

commit v9 on v8

--- a/solution.py
+++ b/solution.py
@@ -60,10 +60,10 @@
 
 
 def experts_kernel(
-    index, x_0, x_1, x_3, x_2a, x_2b, gate_0, up_0, gate_1, up_1, down_1, down_0, out, tall, held_out, sem, out_sems
+    index, x_0, x_1, x_3, x_2a, x_2b, gate_0, up_0, gate_1, up_1, down_0, down_1, out, tall, sem
 ):
     blocks, width = out.shape[0], out.shape[2]
-    load = pltpu.make_async_copy(down_0.at[0], tall, sem)
+    load = pltpu.make_async_copy(down_1.at[0], tall, sem)
     load.start()
     depth = x_0.shape[1]
     parts = gate_0.shape[1] // depth
@@ -79,15 +79,10 @@
         for g, u in ((gate_0, up_0), (gate_1, up_1))
     ]
     load.wait()
-    stores = []
     for b in range(blocks):
         span = slice(b * width, (b + 1) * width)
-        piece = dot(hidden[0], tall[:, span]) + dot(hidden[1], down_1[0, :, span])
-        held_out[b] = piece.astype(bf16)
-        stores.append(pltpu.make_async_copy(held_out.at[b], out.at[b], out_sems.at[b]))
-        stores[-1].start()
-    for store in stores:
-        store.wait()
+        piece = dot(hidden[0], down_0[0, :, span]) + dot(hidden[1], tall[:, span])
+        out[b] = piece.astype(bf16)
 
 
 def sum_kernel(pieces, out):
@@ -185,34 +180,29 @@
         start = halo - taps + 1 + offset
         total = total + conv_taps[offset][None, :] * padded[start : start + length]
     convolved = total.astype(bf16)
-    across = moved(convolved, parts)
-    from_back = [moved(convolved, k) for k in range(1, parts - 1)]
-    from_front = [moved(convolved, -k) for k in range(1, parts - 1)]
-    from_back.append(moved(convolved, parts - 1))
-    from_front.append(moved(convolved, 1 - parts))
+    from_back, from_front = {}, {}
+    for k in range(parts, 0, -1):
+        from_back[k] = moved(convolved, k)
+        if k < parts:
+            from_front[k] = moved(convolved, -k)
 
     rows = n_z * capacity
     arrived, _ = lax.optimization_barrier((arrived, convolved))
     x_0 = arrived.reshape(rows, wide)
     x_2a, x_2b = moved(x_0[: rows // 2], -2), moved(x_0[rows // 2 :], 2)
     x_1, x_3 = moved(x_0, -1), moved(x_0, 1)
-    gate_b, up_b, down_b = (partner(w) for w in (gate_w, up_w, down_w))
-    hbm = pl.BlockSpec(memory_space=pl.ANY)
+    down_b = partner(down_w)
+    gate_b, up_b = partner(gate_w), partner(up_w)
     units = gate_w.shape[2]
     pieces = pl.pallas_call(
         experts_kernel,
         out_shape=jax.ShapeDtypeStruct((n_tp, rows, columns), bf16),
-        in_specs=[smem] + [vmem] * 10 + [pl.BlockSpec(memory_space=pltpu.HBM)],
-        out_specs=hbm,
-        scratch_shapes=[
-            pltpu.VMEM((units, width), bf16),
-            pltpu.VMEM((n_tp, rows, columns), bf16),
-            pltpu.SemaphoreType.DMA,
-            pltpu.SemaphoreType.DMA((n_tp,)),
-        ],
+        in_specs=[smem] + [vmem] * 10 + [pl.BlockSpec(memory_space=pl.ANY)],
+        out_specs=vmem,
+        scratch_shapes=[pltpu.VMEM((units, width), bf16), pltpu.SemaphoreType.DMA],
         compiler_params=params(24),
         cost_estimate=cost(3 * 10**9, 10**7),
-    )(quarter, x_0, x_1, x_3, x_2a, x_2b, gate_w, up_w, gate_b, up_b, down_b, down_w)
+    )(quarter, x_0, x_1, x_3, x_2a, x_2b, gate_w, up_w, gate_b, up_b, down_w, down_b)
     pieces = lax.all_to_all(pieces, "tp", split_axis=0, concat_axis=0, tiled=True)
     step = rows // 2
     sums = pl.pallas_call(
@@ -244,9 +234,9 @@
         compiler_params=params(16),
         cost_estimate=cost(10**8, 10**6),
     )(high, low, results)
-    routed_rows, from_back = lax.optimization_barrier((routed_rows, from_back))
     step = length // 2
-    gathered = [convolved, *from_back, across, *from_front[::-1]]
+    gathered = [convolved] + [from_back[k] for k in range(1, parts + 1)]
+    gathered += [from_front[k] for k in range(parts - 1, 0, -1)]
     mixer_rows = pl.pallas_call(
         mixer_kernel,
         grid=(length // step,),

time: 196 us -> 194 us (0.990)
  Pallas kernels: 14.9 us -> 11.7 us
    pallas_call x1, Pallas kernels: 8.6 us -> 5.36 us  [step_on_device(): pl.pallas_call(experts_kernel, out_shape=jax.ShapeDtypeStruct((n_tp, rows...]
  transfers between devices with their start and end apart: 17 -> 17, of which waited for: 5 -> 6; matrix products, arithmetic and copies ran while one was open for 1% -> 1% of each run, Pallas kernels for 1% -> 1%
where the time goes in v9:
time: 194 us; the launch traced here: 193 us
  starting transfers between devices  112 us (58%)
  blocking collectives  35.7 us (18%)
  waiting for transfers between devices  28.7 us (15%)
  Pallas kernels  11.7 us (6%)
    all_to_all x1, starting transfers between devices, step_on_device(): lax.all_to_all(outgoing.reshape(experts, capacity, wide), 'z', split_axis...  44.2 us
    ppermute x11, starting transfers between devices, moved(): return lax.ppermute(value, 'tp', [(i, (i + by) % n) for i in range(n)])  38.3 us
    all_to_all x1, blocking collectives, step_on_device(): lax.all_to_all(pieces, 'tp', split_axis=0, concat_axis=0, tiled=True)  35.7 us
    ppermute x11, waiting for transfers between devices, moved(): return lax.ppermute(value, 'tp', [(i, (i + by) % n) for i in range(n)])  23.1 us
    all_to_all x1, starting transfers between devices, step_on_device(): lax.all_to_all(sums.reshape(n_z, capacity, columns), 'z', split_axis=0, c...  19.5 us
    ppermute x3, starting transfers between devices, partner(): return lax.ppermute(value, 'core', [(0, 1), (1, 0)])  6.34 us
    all_to_all x1, waiting for transfers between devices, step_on_device(): lax.all_to_all(outgoing.reshape(experts, capacity, wide), 'z', split_axis...  5.59 us
    pallas_call x1, Pallas kernels, step_on_device(): pl.pallas_call(experts_kernel, out_shape=jax.ShapeDtypeStruct((n_tp, rows...  5.36 us
  transfers between devices with their start and end apart: 17, of which 6 were waited for; matrix products, arithmetic and copies ran while one was open for 1% of the time, Pallas kernels for 1%

profile of v9, /device:TPU:65, one launch (start us, length us, event | category | flops | bytes accessed | tf_op | source)
XLA Modules:
  0.0 192.6 jit_solution(1009488320459685817)
XLA Ops:
  0.7 2.4 %shard_map.133 = bf16[384,512]{1,0:T(8,128)(2,1)} custom-call(s32[1]{0:T(128)} %bitcast.35.index, s32[2,128]{1,0:T(2,128)} %bitcast.78, bf16[128,2048]{1,0:T(8,128)(2,1)} %rows.1, f32[1,2048]{1,0:T(1,128)} %bitcast.85), custom_call_target="tpu_custom_call" | custom-call | flops 100000000 | bytes 1000000 | tf_op jit(solution)/shard_map/pallas_call | solution.py:156
  3.1 44.2 %all-to-all-start = ((bf16[16,24,512]{2,1,0:T(8,128)(2,1)}), bf16[16,24,512]{2,1,0:T(8,128)(2,1)S(1)}, u32[]{:S(2)}, u32[]{:S(2)}) async-start(bf16[16,24,512]{2,1,0:T(8,128)(2,1)} %bitcast.82), calls=%async_computation | async-start | bytes 786432 | tf_op jit(solution)/shard_map/all_to_all | solution.py:165
  48.3 4.2 %collective-permute-start = (bf16[32,128]{1,0:T(8,128)(2,1)S(1)}, bf16[32,128]{1,0:T(8,128)(2,1)S(1)}, u32[]{:S(2)}, u32[]{:S(2)}) collective-permute-start(bf16[32,128]{1,0:T(8,128)(2,1)S(1)} %slice.268), channel_id=1, source_target_pairs={{0,8},{8,16},{16,24},{24,32},{32,40},{40,48},{48,56},{56,64},{64,7... | collective-permute-start | bytes 24584 | tf_op jit(solution)/shard_map/ppermute | solution.py:174
  54.5 2.4 %collective-permute-start.13 = (bf16[1,2048,256]{2,1,0:T(8,128)(2,1)S(1)}, bf16[1,2048,256]{2,1,0:T(8,128)(2,1)}, u32[]{:S(2)}, u32[]{:S(2)}) collective-permute-start(bf16[1,2048,256]{2,1,0:T(8,128)(2,1)S(1)} %copy-done.2), channel_id=1, source_target_pairs={{0,8},{8,0},{1,9},{9,1},{2,10},{10,2},{3,11},{11,3},{4,12},{12,4},... | collective-permute-start | bytes 3145736 | tf_op jit(solution)/shard_map/ppermute | solution.py:116
  56.9 2.0 %collective-permute-start.14 = (bf16[1,256,2048]{2,1,0:T(8,128)(2,1)}, bf16[1,256,2048]{2,1,0:T(8,128)(2,1)}, u32[]{:S(2)}, u32[]{:S(2)}) collective-permute-start(bf16[1,256,2048]{2,1,0:T(8,128)(2,1)} %down_0.1), channel_id=1, source_target_pairs={{0,8},{8,0},{1,9},{9,1},{2,10},{10,2},{3,11},{11,3},{4,12},{12,4},... | collective-permute-start | bytes 3145736 | tf_op jit(solution)/shard_map/ppermute | solution.py:116
  59.7 5.6 %all-to-all-done = bf16[16,24,512]{2,1,0:T(8,128)(2,1)S(1)} async-done(((bf16[16,24,512]{2,1,0:T(8,128)(2,1)}), bf16[16,24,512]{2,1,0:T(8,128)(2,1)S(1)}, u32[]{:S(2)}, u32[]{:S(2)}) %all-to-all-start) | async-done | bytes 393248 | tf_op jit(solution)/shard_map/all_to_all | solution.py:165
  65.3 5.5 %collective-permute-start.8 = (bf16[384,512]{1,0:T(8,128)(2,1)S(1)}, bf16[384,512]{1,0:T(8,128)(2,1)S(1)}, u32[]{:S(2)}, u32[]{:S(2)}) collective-permute-start(bf16[384,512]{1,0:T(8,128)(2,1)S(1)} %bitcast.74), channel_id=1, source_target_pairs={{0,7},{1,0},{2,1},{3,2},{4,3},{5,4},{6,5},{7,6},{8,15},{9,8},{10,9... | collective-permute-start | bytes 1179656 | tf_op jit(solution)/shard_map/ppermute | solution.py:112
  72.7 4.1 %collective-permute-start.10 = (bf16[192,512]{1,0:T(8,128)(2,1)S(1)}, bf16[192,512]{1,0:T(8,128)(2,1)S(1)}, u32[]{:S(2)}, u32[]{:S(2)}) collective-permute-start(bf16[192,512]{1,0:T(8,128)(2,1)S(1)} %bitcast.84), channel_id=1, source_target_pairs={{0,6},{1,7},{2,0},{3,1},{4,2},{5,3},{6,4},{7,5},{8,14},{9,15},{10,... | collective-permute-start | bytes 589832 | tf_op jit(solution)/shard_map/ppermute | solution.py:112
  76.9 2.1 %collective-permute-start.11 = (bf16[192,512]{1,0:T(8,128)(2,1)S(1)}, bf16[192,512]{1,0:T(8,128)(2,1)S(1)}, u32[]{:S(2)}, u32[]{:S(2)}) collective-permute-start(bf16[192,512]{1,0:T(8,128)(2,1)S(1)} %bitcast.83), channel_id=1, source_target_pairs={{0,2},{1,3},{2,4},{3,5},{4,6},{5,7},{6,0},{7,1},{8,10},{9,11},{10,... | collective-permute-start | bytes 589832 | tf_op jit(solution)/shard_map/ppermute | solution.py:112
  79.0 5.6 %collective-permute-done.10.x_2a = bf16[192,512]{1,0:T(8,128)(2,1)S(1)} collective-permute-done((bf16[192,512]{1,0:T(8,128)(2,1)S(1)}, bf16[192,512]{1,0:T(8,128)(2,1)S(1)}, u32[]{:S(2)}, u32[]{:S(2)}) %collective-permute-start.10) | collective-permute-done | bytes 196640 | tf_op jit(solution)/shard_map/ppermute | solution.py:112
  84.6 4.6 %collective-permute-done.11.x_2b = bf16[192,512]{1,0:T(8,128)(2,1)S(1)} collective-permute-done((bf16[192,512]{1,0:T(8,128)(2,1)S(1)}, bf16[192,512]{1,0:T(8,128)(2,1)S(1)}, u32[]{:S(2)}, u32[]{:S(2)}) %collective-permute-start.11) | collective-permute-done | bytes 196640 | tf_op jit(solution)/shard_map/ppermute | solution.py:112
  90.4 5.4 %shard_map.134 = bf16[8,384,256]{2,1,0:T(8,128)(2,1)S(1)} custom-call(s32[1]{0:T(128)} %bitcast.35.index, bf16[384,512]{1,0:T(8,128)(2,1)S(1)} %bitcast.76, bf16[384,512]{1,0:T(8,128)(2,1)S(1)} %collective-permute-done.8.x_1, bf16[384,512]{1,0:T(8,128)(2,1)S(1)} %collective-permute-done.9.x_3, bf16[192,512]{1,0:T(8,128)(2,1)S(1)} %collective-permute-done.10.x_2a, ...), custom_call_target="tpu_custom_call" | custom-call | flops 3000000000 | bytes 10000000 | tf_op jit(solution)/shard_map/pallas_call | solution.py:197
  95.8 35.7 %all_to_all.15.pieces = bf16[8,384,256]{2,1,0:T(8,128)(2,1)S(1)} all-to-all(bf16[8,384,256]{2,1,0:T(8,128)(2,1)S(1)} %shard_map.134), channel_id=1, replica_groups=mesh['grp'=2,'z'=16,'core'=2,'tp'=8] {'tp'}, dimensions={0} | all-to-all | bytes 3145728 | tf_op jit(solution)/shard_map/all_to_all | solution.py:206
  132.5 19.5 %all-to-all-start.2 = ((bf16[16,24,256]{2,1,0:T(8,128)(2,1)}), bf16[16,24,256]{2,1,0:T(8,128)(2,1)S(1)}, u32[]{:S(2)}, u32[]{:S(2)}) async-start(bf16[16,24,256]{2,1,0:T(8,128)(2,1)} %bitcast.41), calls=%async_computation.2 | async-start | bytes 393216 | tf_op jit(solution)/shard_map/all_to_all | solution.py:217
  152.0 2.3 %collective-permute-start.1 = (bf16[512,128]{1,0:T(8,128)(2,1)S(1)}, bf16[512,128]{1,0:T(8,128)(2,1)S(1)}, u32[]{:S(2)}, u32[]{:S(2)}) collective-permute-start(bf16[512,128]{1,0:T(8,128)(2,1)S(1)} %fusion.1.refs_0_), channel_id=1, source_target_pairs={{0,1},{1,2},{2,3},{3,4},{4,5},{5,6},{6,7},{7,0},{8,9},{9,10},{10,1... | collective-permute-start | bytes 393224 | tf_op jit(solution)/shard_map/ppermute | solution.py:112
  154.3 3.7 %collective-permute-start.2 = (bf16[512,128]{1,0:T(8,128)(2,1)S(1)}, bf16[512,128]{1,0:T(8,128)(2,1)S(1)}, u32[]{:S(2)}, u32[]{:S(2)}) collective-permute-start(bf16[512,128]{1,0:T(8,128)(2,1)S(1)} %fusion.1.refs_0_), channel_id=1, source_target_pairs={{0,2},{1,3},{2,4},{3,5},{4,6},{5,7},{6,0},{7,1},{8,10},{9,11},{10,... | collective-permute-start | bytes 393224 | tf_op jit(solution)/shard_map/ppermute | solution.py:112
  157.9 4.3 %collective-permute-start.3 = (bf16[512,128]{1,0:T(8,128)(2,1)S(1)}, bf16[512,128]{1,0:T(8,128)(2,1)S(1)}, u32[]{:S(2)}, u32[]{:S(2)}) collective-permute-start(bf16[512,128]{1,0:T(8,128)(2,1)S(1)} %fusion.1.refs_0_), channel_id=1, source_target_pairs={{0,3},{1,4},{2,5},{3,6},{4,7},{5,0},{6,1},{7,2},{8,11},{9,12},{10,... | collective-permute-start | bytes 393224 | tf_op jit(solution)/shard_map/ppermute | solution.py:112
  162.3 3.2 %collective-permute-start.4 = (bf16[512,128]{1,0:T(8,128)(2,1)S(1)}, bf16[512,128]{1,0:T(8,128)(2,1)S(1)}, u32[]{:S(2)}, u32[]{:S(2)}) collective-permute-start(bf16[512,128]{1,0:T(8,128)(2,1)S(1)} %fusion.1.refs_0_), channel_id=1, source_target_pairs={{0,4},{1,5},{2,6},{3,7},{4,0},{5,1},{6,2},{7,3},{8,12},{9,13},{10,... | collective-permute-start | bytes 393224 | tf_op jit(solution)/shard_map/ppermute | solution.py:112
  165.5 4.8 %collective-permute-start.5 = (bf16[512,128]{1,0:T(8,128)(2,1)S(1)}, bf16[512,128]{1,0:T(8,128)(2,1)S(1)}, u32[]{:S(2)}, u32[]{:S(2)}) collective-permute-start(bf16[512,128]{1,0:T(8,128)(2,1)S(1)} %fusion.1.refs_0_), channel_id=1, source_target_pairs={{0,5},{1,6},{2,7},{3,0},{4,1},{5,2},{6,3},{7,4},{8,13},{9,14},{10,... | collective-permute-start | bytes 393224 | tf_op jit(solution)/shard_map/ppermute | solution.py:112
  170.4 3.1 %collective-permute-start.6 = (bf16[512,128]{1,0:T(8,128)(2,1)S(1)}, bf16[512,128]{1,0:T(8,128)(2,1)S(1)}, u32[]{:S(2)}, u32[]{:S(2)}) collective-permute-start(bf16[512,128]{1,0:T(8,128)(2,1)S(1)} %fusion.1.refs_0_), channel_id=1, source_target_pairs={{0,6},{1,7},{2,0},{3,1},{4,2},{5,3},{6,4},{7,5},{8,14},{9,15},{10,... | collective-permute-start | bytes 393224 | tf_op jit(solution)/shard_map/ppermute | solution.py:112
  173.5 3.1 %collective-permute-start.7 = (bf16[512,128]{1,0:T(8,128)(2,1)S(1)}, bf16[512,128]{1,0:T(8,128)(2,1)S(1)}, u32[]{:S(2)}, u32[]{:S(2)}) collective-permute-start(bf16[512,128]{1,0:T(8,128)(2,1)S(1)} %fusion.1.refs_0_), channel_id=1, source_target_pairs={{0,7},{1,0},{2,1},{3,2},{4,3},{5,4},{6,5},{7,6},{8,15},{9,8},{10,9... | collective-permute-start | bytes 393224 | tf_op jit(solution)/shard_map/ppermute | solution.py:112
  177.0 2.1 %collective-permute-done.4.refs_4_ = bf16[512,128]{1,0:T(8,128)(2,1)S(1)} collective-permute-done((bf16[512,128]{1,0:T(8,128)(2,1)S(1)}, bf16[512,128]{1,0:T(8,128)(2,1)S(1)}, u32[]{:S(2)}, u32[]{:S(2)}) %collective-permute-start.4) | collective-permute-done | bytes 131104 | tf_op jit(solution)/shard_map/ppermute | solution.py:112
  179.0 6.5 %collective-permute-done.6.refs_6_ = bf16[512,128]{1,0:T(8,128)(2,1)S(1)} collective-permute-done((bf16[512,128]{1,0:T(8,128)(2,1)S(1)}, bf16[512,128]{1,0:T(8,128)(2,1)S(1)}, u32[]{:S(2)}, u32[]{:S(2)}) %collective-permute-start.6) | collective-permute-done | bytes 131104 | tf_op jit(solution)/shard_map/ppermute | solution.py:112
  185.6 4.4 %collective-permute-done.7.refs_7_ = bf16[512,128]{1,0:T(8,128)(2,1)S(1)} collective-permute-done((bf16[512,128]{1,0:T(8,128)(2,1)S(1)}, bf16[512,128]{1,0:T(8,128)(2,1)S(1)}, u32[]{:S(2)}, u32[]{:S(2)}) %collective-permute-start.7) | collective-permute-done | bytes 131104 | tf_op jit(solution)/shard_map/ppermute | solution.py:112
  (40 shorter events, 11.0 us)
Async XLA Ops:
  0.6 51.9 %copy-start.1 = (bf16[1,2048,256]{2,1,0:T(8,128)(2,1)S(1)}, bf16[1,2048,256]{2,1,0:T(8,128)(2,1)}, u32[]{:S(2)}) copy-start(bf16[1,2048,256]{2,1,0:T(8,128)(2,1)} %gate_0.1) | copy-start | bytes 3145732
  0.6 53.8 %copy-start.2 = (bf16[1,2048,256]{2,1,0:T(8,128)(2,1)S(1)}, bf16[1,2048,256]{2,1,0:T(8,128)(2,1)}, u32[]{:S(2)}) copy-start(bf16[1,2048,256]{2,1,0:T(8,128)(2,1)} %up_0.1) | copy-start | bytes 3145732
  0.7 58.2 %copy-start.7 = (f32[31,128]{1,0:T(8,128)S(1)}, f32[31,128]{1,0:T(8,128)}, u32[]{:S(2)}) copy-start(f32[31,128]{1,0:T(8,128)} %param.14) | copy-start | bytes 47620
  3.1 62.2 %all-to-all-start = ((bf16[16,24,512]{2,1,0:T(8,128)(2,1)}), bf16[16,24,512]{2,1,0:T(8,128)(2,1)S(1)}, u32[]{:S(2)}, u32[]{:S(2)}) async-start(bf16[16,24,512]{2,1,0:T(8,128)(2,1)} %bitcast.82), calls=%async_computation | async-start | bytes 786432 | tf_op jit(solution)/shard_map/all_to_all | solution.py:165
  48.3 10.6 %collective-permute-start = (bf16[32,128]{1,0:T(8,128)(2,1)S(1)}, bf16[32,128]{1,0:T(8,128)(2,1)S(1)}, u32[]{:S(2)}, u32[]{:S(2)}) collective-permute-start(bf16[32,128]{1,0:T(8,128)(2,1)S(1)} %slice.268), channel_id=1, source_target_pairs={{0,8},{8,16},{16,24},{24,32},{32,40},{40,48},{48,56},{56,64},{64,7... | collective-permute-start | bytes 24584 | tf_op jit(solution)/shard_map/ppermute | solution.py:174
  52.5 20.2 %collective-permute-start.12 = (bf16[1,2048,256]{2,1,0:T(8,128)(2,1)S(1)}, bf16[1,2048,256]{2,1,0:T(8,128)(2,1)}, u32[]{:S(2)}, u32[]{:S(2)}) collective-permute-start(bf16[1,2048,256]{2,1,0:T(8,128)(2,1)S(1)} %copy-done.1), channel_id=1, source_target_pairs={{0,8},{8,0},{1,9},{9,1},{2,10},{10,2},{3,11},{11,3},{4,12},{12,4},... | collective-permute-start | bytes 3145736 | tf_op jit(solution)/shard_map/ppermute | solution.py:116
  54.5 22.4 %collective-permute-start.13 = (bf16[1,2048,256]{2,1,0:T(8,128)(2,1)S(1)}, bf16[1,2048,256]{2,1,0:T(8,128)(2,1)}, u32[]{:S(2)}, u32[]{:S(2)}) collective-permute-start(bf16[1,2048,256]{2,1,0:T(8,128)(2,1)S(1)} %copy-done.2), channel_id=1, source_target_pairs={{0,8},{8,0},{1,9},{9,1},{2,10},{10,2},{3,11},{11,3},{4,12},{12,4},... | collective-permute-start | bytes 3145736 | tf_op jit(solution)/shard_map/ppermute | solution.py:116
  56.9 22.1 %collective-permute-start.14 = (bf16[1,256,2048]{2,1,0:T(8,128)(2,1)}, bf16[1,256,2048]{2,1,0:T(8,128)(2,1)}, u32[]{:S(2)}, u32[]{:S(2)}) collective-permute-start(bf16[1,256,2048]{2,1,0:T(8,128)(2,1)} %down_0.1), channel_id=1, source_target_pairs={{0,8},{8,0},{1,9},{9,1},{2,10},{10,2},{3,11},{11,3},{4,12},{12,4},... | collective-permute-start | bytes 3145736 | tf_op jit(solution)/shard_map/ppermute | solution.py:116
  65.3 23.9 %collective-permute-start.8 = (bf16[384,512]{1,0:T(8,128)(2,1)S(1)}, bf16[384,512]{1,0:T(8,128)(2,1)S(1)}, u32[]{:S(2)}, u32[]{:S(2)}) collective-permute-start(bf16[384,512]{1,0:T(8,128)(2,1)S(1)} %bitcast.74), channel_id=1, source_target_pairs={{0,7},{1,0},{2,1},{3,2},{4,3},{5,4},{6,5},{7,6},{8,15},{9,8},{10,9... | collective-permute-start | bytes 1179656 | tf_op jit(solution)/shard_map/ppermute | solution.py:112
  70.7 18.4 %collective-permute-start.9 = (bf16[384,512]{1,0:T(8,128)(2,1)S(1)}, bf16[384,512]{1,0:T(8,128)(2,1)S(1)}, u32[]{:S(2)}, u32[]{:S(2)}) collective-permute-start(bf16[384,512]{1,0:T(8,128)(2,1)S(1)} %bitcast.75), channel_id=1, source_target_pairs={{0,1},{1,2},{2,3},{3,4},{4,5},{5,6},{6,7},{7,0},{8,9},{9,10},{10,1... | collective-permute-start | bytes 1179656 | tf_op jit(solution)/shard_map/ppermute | solution.py:112
  72.7 11.8 %collective-permute-start.10 = (bf16[192,512]{1,0:T(8,128)(2,1)S(1)}, bf16[192,512]{1,0:T(8,128)(2,1)S(1)}, u32[]{:S(2)}, u32[]{:S(2)}) collective-permute-start(bf16[192,512]{1,0:T(8,128)(2,1)S(1)} %bitcast.84), channel_id=1, source_target_pairs={{0,6},{1,7},{2,0},{3,1},{4,2},{5,3},{6,4},{7,5},{8,14},{9,15},{10,... | collective-permute-start | bytes 589832 | tf_op jit(solution)/shard_map/ppermute | solution.py:112
  76.9 12.3 %collective-permute-start.11 = (bf16[192,512]{1,0:T(8,128)(2,1)S(1)}, bf16[192,512]{1,0:T(8,128)(2,1)S(1)}, u32[]{:S(2)}, u32[]{:S(2)}) collective-permute-start(bf16[192,512]{1,0:T(8,128)(2,1)S(1)} %bitcast.83), channel_id=1, source_target_pairs={{0,2},{1,3},{2,4},{3,5},{4,6},{5,7},{6,0},{7,1},{8,10},{9,11},{10,... | collective-permute-start | bytes 589832 | tf_op jit(solution)/shard_map/ppermute | solution.py:112
  131.5 45.2 %copy-start = (s32[128,2]{0,1:T(2,128)S(1)}, s32[128,2]{0,1:T(2,128)}, u32[]{:S(2)}) copy-start(s32[128,2]{0,1:T(2,128)} %param.19) | copy-start | bytes 3076
  131.5 45.2 %copy-start.6 = (f32[128,2]{0,1:T(2,128)S(1)}, f32[128,2]{0,1:T(2,128)}, u32[]{:S(2)}) copy-start(f32[128,2]{0,1:T(2,128)} %param.20) | copy-start | bytes 3076
  131.5 58.5 %copy-start.4 = (bf16[1024,256]{1,0:T(8,128)(2,1)S(1)}, bf16[1024,256]{1,0:T(8,128)(2,1)}, u32[]{:S(2)}) copy-start(bf16[1024,256]{1,0:T(8,128)(2,1)} %refs_9_.1) | copy-start | bytes 1572868
  131.5 58.5 %copy-start.5 = (f32[1024]{0:T(1024)S(1)}, f32[1024]{0:T(1024)}, u32[]{:S(2)}) copy-start(f32[1024]{0:T(1024)} %param.15) | copy-start | bytes 12292
  132.5 59.3 %all-to-all-start.2 = ((bf16[16,24,256]{2,1,0:T(8,128)(2,1)}), bf16[16,24,256]{2,1,0:T(8,128)(2,1)S(1)}, u32[]{:S(2)}, u32[]{:S(2)}) async-start(bf16[16,24,256]{2,1,0:T(8,128)(2,1)} %bitcast.41), calls=%async_computation.2 | async-start | bytes 393216 | tf_op jit(solution)/shard_map/all_to_all | solution.py:217
  152.0 18.4 %collective-permute-start.1 = (bf16[512,128]{1,0:T(8,128)(2,1)S(1)}, bf16[512,128]{1,0:T(8,128)(2,1)S(1)}, u32[]{:S(2)}, u32[]{:S(2)}) collective-permute-start(bf16[512,128]{1,0:T(8,128)(2,1)S(1)} %fusion.1.refs_0_), channel_id=1, source_target_pairs={{0,1},{1,2},{2,3},{3,4},{4,5},{5,6},{6,7},{7,0},{8,9},{9,10},{10,1... | collective-permute-start | bytes 393224 | tf_op jit(solution)/shard_map/ppermute | solution.py:112
  154.3 19.2 %collective-permute-start.2 = (bf16[512,128]{1,0:T(8,128)(2,1)S(1)}, bf16[512,128]{1,0:T(8,128)(2,1)S(1)}, u32[]{:S(2)}, u32[]{:S(2)}) collective-permute-start(bf16[512,128]{1,0:T(8,128)(2,1)S(1)} %fusion.1.refs_0_), channel_id=1, source_target_pairs={{0,2},{1,3},{2,4},{3,5},{4,6},{5,7},{6,0},{7,1},{8,10},{9,11},{10,... | collective-permute-start | bytes 393224 | tf_op jit(solution)/shard_map/ppermute | solution.py:112
  157.9 19.0 %collective-permute-start.3 = (bf16[512,128]{1,0:T(8,128)(2,1)S(1)}, bf16[512,128]{1,0:T(8,128)(2,1)S(1)}, u32[]{:S(2)}, u32[]{:S(2)}) collective-permute-start(bf16[512,128]{1,0:T(8,128)(2,1)S(1)} %fusion.1.refs_0_), channel_id=1, source_target_pairs={{0,3},{1,4},{2,5},{3,6},{4,7},{5,0},{6,1},{7,2},{8,11},{9,12},{10,... | collective-permute-start | bytes 393224 | tf_op jit(solution)/shard_map/ppermute | solution.py:112
  162.3 16.7 %collective-permute-start.4 = (bf16[512,128]{1,0:T(8,128)(2,1)S(1)}, bf16[512,128]{1,0:T(8,128)(2,1)S(1)}, u32[]{:S(2)}, u32[]{:S(2)}) collective-permute-start(bf16[512,128]{1,0:T(8,128)(2,1)S(1)} %fusion.1.refs_0_), channel_id=1, source_target_pairs={{0,4},{1,5},{2,6},{3,7},{4,0},{5,1},{6,2},{7,3},{8,12},{9,13},{10,... | collective-permute-start | bytes 393224 | tf_op jit(solution)/shard_map/ppermute | solution.py:112
  165.5 13.5 %collective-permute-start.5 = (bf16[512,128]{1,0:T(8,128)(2,1)S(1)}, bf16[512,128]{1,0:T(8,128)(2,1)S(1)}, u32[]{:S(2)}, u32[]{:S(2)}) collective-permute-start(bf16[512,128]{1,0:T(8,128)(2,1)S(1)} %fusion.1.refs_0_), channel_id=1, source_target_pairs={{0,5},{1,6},{2,7},{3,0},{4,1},{5,2},{6,3},{7,4},{8,13},{9,14},{10,... | collective-permute-start | bytes 393224 | tf_op jit(solution)/shard_map/ppermute | solution.py:112
  170.4 15.2 %collective-permute-start.6 = (bf16[512,128]{1,0:T(8,128)(2,1)S(1)}, bf16[512,128]{1,0:T(8,128)(2,1)S(1)}, u32[]{:S(2)}, u32[]{:S(2)}) collective-permute-start(bf16[512,128]{1,0:T(8,128)(2,1)S(1)} %fusion.1.refs_0_), channel_id=1, source_target_pairs={{0,6},{1,7},{2,0},{3,1},{4,2},{5,3},{6,4},{7,5},{8,14},{9,15},{10,... | collective-permute-start | bytes 393224 | tf_op jit(solution)/shard_map/ppermute | solution.py:112
  173.5 16.4 %collective-permute-start.7 = (bf16[512,128]{1,0:T(8,128)(2,1)S(1)}, bf16[512,128]{1,0:T(8,128)(2,1)S(1)}, u32[]{:S(2)}, u32[]{:S(2)}) collective-permute-start(bf16[512,128]{1,0:T(8,128)(2,1)S(1)} %fusion.1.refs_0_), channel_id=1, source_target_pairs={{0,7},{1,0},{2,1},{3,2},{4,3},{5,4},{6,5},{7,6},{8,15},{9,8},{10,9... | collective-permute-start | bytes 393224 | tf_op jit(solution)/shard_map/ppermute | solution.py:112
  (1 other events, 1.2 us)

commit v10 on v9

--- a/solution.py
+++ b/solution.py
@@ -60,9 +60,8 @@
 
 
 def experts_kernel(
-    index, x_0, x_1, x_3, x_2a, x_2b, gate_0, up_0, gate_1, up_1, down_0, down_1, out, tall, sem
+    index, x_0, x_1, x_3, x_2a, x_2b, gate_0, up_0, gate_1, up_1, down_0, down_1, me, out, top, bottom, tall, sem
 ):
-    blocks, width = out.shape[0], out.shape[2]
     load = pltpu.make_async_copy(down_1.at[0], tall, sem)
     load.start()
     depth = x_0.shape[1]
@@ -79,17 +78,39 @@
         for g, u in ((gate_0, up_0), (gate_1, up_1))
     ]
     load.wait()
-    for b in range(blocks):
-        span = slice(b * width, (b + 1) * width)
-        piece = dot(hidden[0], down_0[0, :, span]) + dot(hidden[1], tall[:, span])
-        out[b] = piece.astype(bf16)
-
-
-def sum_kernel(pieces, out):
-    total = pieces[0].astype(f32)
-    for b in range(1, pieces.shape[0]):
-        total = total + pieces[b].astype(f32)
-    out[...] = total.astype(bf16)
+    half, width = top.shape
+    n = tall.shape[1] // width
+    span = block_of(me, n // 2, n, width)
+    piece = dot(hidden[0], down_0[0, :, span]) + dot(hidden[1], tall[:, span])
+    top[...] = piece[:half].astype(bf16)
+    bottom[...] = piece[half:].astype(bf16)
+    units = hidden[0].shape[1]
+    out[:, :units] = hidden[0]
+    out[:, units:] = hidden[1]
+
+
+def block_of(me, by, n, width):
+    return pl.ds(pl.multiple_of(lax.rem(me[0] + by + n, n) * width, width), width)
+
+
+def pieces_kernel(far, me, hidden, down_0, down_1, top, bottom, *outs):
+    half, width = top.shape
+    n, units = down_1.shape[1] // width, down_1.shape[0]
+    order = [0] + [sign * k for k in range(1, far + 1) for sign in (1, -1)]
+    for by, out in zip(order, outs):
+        span = block_of(me, by, n, width)
+        piece = dot(hidden[:, :units], down_0[0, :, span])
+        piece = piece + dot(hidden[:, units:], down_1[:, span])
+        if by == far:
+            piece = jnp.concatenate([piece[:half] + top[...].astype(f32), piece[half:]], axis=0)
+        if by == -far:
+            piece = jnp.concatenate([piece[:half], piece[half:] + bottom[...].astype(f32)], axis=0)
+        out[...] = piece.astype(bf16)
+
+
+def sum_kernel(*refs):
+    *pieces, out = refs
+    out[...] = functools.reduce(jnp.add, [p[...].astype(f32) for p in pieces]).astype(bf16)
 
 
 def mixer_kernel(index, *refs):
@@ -194,26 +215,43 @@
     down_b = partner(down_w)
     gate_b, up_b = partner(gate_w), partner(up_w)
     units = gate_w.shape[2]
-    pieces = pl.pallas_call(
+    me_ref = me.astype(jnp.int32).reshape(1)
+    shape = lambda *dims: jax.ShapeDtypeStruct(dims, bf16)
+    hidden, top, bottom, down_b = pl.pallas_call(
         experts_kernel,
-        out_shape=jax.ShapeDtypeStruct((n_tp, rows, columns), bf16),
-        in_specs=[smem] + [vmem] * 10 + [pl.BlockSpec(memory_space=pl.ANY)],
-        out_specs=vmem,
-        scratch_shapes=[pltpu.VMEM((units, width), bf16), pltpu.SemaphoreType.DMA],
+        out_shape=[
+            shape(rows, 2 * units),
+            shape(rows // 2, columns),
+            shape(rows // 2, columns),
+            shape(units, width),
+        ],
+        in_specs=[smem] + [vmem] * 10 + [pl.BlockSpec(memory_space=pl.ANY), smem],
+        out_specs=[vmem] * 4,
+        scratch_shapes=[pltpu.SemaphoreType.DMA],
         compiler_params=params(24),
-        cost_estimate=cost(3 * 10**9, 10**7),
-    )(quarter, x_0, x_1, x_3, x_2a, x_2b, gate_w, up_w, gate_b, up_b, down_w, down_b)
-    pieces = lax.all_to_all(pieces, "tp", split_axis=0, concat_axis=0, tiled=True)
-    step = rows // 2
+        cost_estimate=cost(2 * 10**9, 10**7),
+    )(quarter, x_0, x_1, x_3, x_2a, x_2b, gate_w, up_w, gate_b, up_b, down_w, down_b, me_ref)
+    top, bottom = moved(top, 1), moved(bottom, -1)
+    far = parts - 1
+    own, *sent = pl.pallas_call(
+        functools.partial(pieces_kernel, far),
+        out_shape=[shape(rows, columns)] * (2 * far + 1),
+        in_specs=[smem] + [vmem] * 5,
+        out_specs=[vmem] * (2 * far + 1),
+        compiler_params=params(16),
+        cost_estimate=cost(10**9, 10**6),
+    )(me_ref, hidden, down_w, down_b, top, bottom)
+    pieces = [own]
+    for k in range(far, 0, -1):
+        pieces += [moved(sent[2 * k - 2], k), moved(sent[2 * k - 1], -k)]
     sums = pl.pallas_call(
         sum_kernel,
-        grid=(rows // step,),
-        out_shape=jax.ShapeDtypeStruct((rows, columns), bf16),
-        in_specs=[pl.BlockSpec((n_tp, step, columns), lambda i: (0, i, 0))],
-        out_specs=pl.BlockSpec((step, columns), lambda i: (i, 0)),
+        out_shape=shape(rows, columns),
+        in_specs=[vmem] * len(pieces),
+        out_specs=vmem,
         compiler_params=params(16),
         cost_estimate=cost(10**8, 2 * 10**6),
-    )(pieces)
+    )(*pieces)
     results = lax.all_to_all(
         sums.reshape(n_z, capacity, columns), "z", split_axis=0, concat_axis=0, tiled=True
     ).reshape(slots, columns)

time: 194 us -> 195 us (level)
  blocking collectives: 35.7 us -> 0 us
  starting transfers between devices: 112 us -> 139 us
  waiting for transfers between devices: 28.7 us -> 39.3 us
    all_to_all x1 -> x0, blocking collectives: 35.7 us -> none  [step_on_device(): lax.all_to_all(pieces, 'tp', split_axis=0, concat_axis=0, tiled=True)]
    ppermute x11 -> x19, starting transfers between devices: 38.3 us -> 68.5 us  [moved(): return lax.ppermute(value, 'tp', [(i, (i + by) % n) for i in range(n)])]
    ppermute x11 -> x19, waiting for transfers between devices: 23.1 us -> 34.4 us  [moved(): return lax.ppermute(value, 'tp', [(i, (i + by) % n) for i in range(n)])]
    all_to_all x1, starting transfers between devices: 19.5 us -> 16.2 us  [step_on_device(): lax.all_to_all(sums.reshape(n_z, capacity, columns), 'z', split_axis=0, c...]
    pallas_call x2 -> x3, Pallas kernels: 6.36 us -> 5.58 us  [the longest x1 3.84 us: step_on_device(): pl.pallas_call(experts_kernel, out_shape=[shape(rows, 2 * units), shape(r...]
  transfers between devices with their start and end apart: 17 -> 25, of which waited for: 6 -> 10; matrix products, arithmetic and copies ran while one was open for 1% -> 1% of each run, Pallas kernels for 1% -> 1%
where the time goes in v10:
time: 195 us; the launch traced here: 193 us
  starting transfers between devices  139 us (71%)
  waiting for transfers between devices  39.3 us (20%)
  Pallas kernels  10.9 us (6%)
  other arithmetic  2.43 us (1%)
    ppermute x19, starting transfers between devices, moved(): return lax.ppermute(value, 'tp', [(i, (i + by) % n) for i in range(n)])  68.5 us
    all_to_all x1, starting transfers between devices, step_on_device(): lax.all_to_all(outgoing.reshape(experts, capacity, wide), 'z', split_axis...  44.2 us
    ppermute x19, waiting for transfers between devices, moved(): return lax.ppermute(value, 'tp', [(i, (i + by) % n) for i in range(n)])  34.4 us
    all_to_all x1, starting transfers between devices, step_on_device(): lax.all_to_all(sums.reshape(n_z, capacity, columns), 'z', split_axis=0, c...  16.2 us
    ppermute x3, starting transfers between devices, partner(): return lax.ppermute(value, 'core', [(0, 1), (1, 0)])  6.34 us
    all_to_all x1, waiting for transfers between devices, step_on_device(): lax.all_to_all(outgoing.reshape(experts, capacity, wide), 'z', split_axis...  4.91 us
    ppermute x1, starting transfers between devices, step_on_device(): lax.ppermute(glu[length - halo:], ('z', 'core'), [(i, i + 1) for i in ran...  4.15 us
  transfers between devices with their start and end apart: 25, of which 10 were waited for; matrix products, arithmetic and copies ran while one was open for 1% of the time, Pallas kernels for 1%

profile of v10, /device:TPU:65, one launch (start us, length us, event | category | flops | bytes accessed | tf_op | source)
XLA Modules:
  0.0 193.3 jit_solution(16656814699203618815)
XLA Ops:
  3.0 44.2 %all-to-all-start = ((bf16[16,24,512]{2,1,0:T(8,128)(2,1)}), bf16[16,24,512]{2,1,0:T(8,128)(2,1)S(1)}, u32[]{:S(2)}, u32[]{:S(2)}) async-start(bf16[16,24,512]{2,1,0:T(8,128)(2,1)} %bitcast.82), calls=%async_computation | async-start | bytes 786432 | tf_op jit(solution)/shard_map/all_to_all | solution.py:186
  48.4 4.2 %collective-permute-start = (bf16[32,128]{1,0:T(8,128)(2,1)S(1)}, bf16[32,128]{1,0:T(8,128)(2,1)S(1)}, u32[]{:S(2)}, u32[]{:S(2)}) collective-permute-start(bf16[32,128]{1,0:T(8,128)(2,1)S(1)} %slice.268), channel_id=1, source_target_pairs={{0,8},{8,16},{16,24},{24,32},{32,40},{40,48},{48,56},{56,64},{64,7... | collective-permute-start | bytes 24584 | tf_op jit(solution)/shard_map/ppermute | solution.py:195
  60.4 4.9 %all-to-all-done = bf16[16,24,512]{2,1,0:T(8,128)(2,1)S(1)} async-done(((bf16[16,24,512]{2,1,0:T(8,128)(2,1)}), bf16[16,24,512]{2,1,0:T(8,128)(2,1)S(1)}, u32[]{:S(2)}, u32[]{:S(2)}) %all-to-all-start) | async-done | bytes 393248 | tf_op jit(solution)/shard_map/all_to_all | solution.py:186
  65.3 5.4 %collective-permute-start.8 = (bf16[384,512]{1,0:T(8,128)(2,1)S(1)}, bf16[384,512]{1,0:T(8,128)(2,1)S(1)}, u32[]{:S(2)}, u32[]{:S(2)}) collective-permute-start(bf16[384,512]{1,0:T(8,128)(2,1)S(1)} %bitcast.74), channel_id=1, source_target_pairs={{0,7},{1,0},{2,1},{3,2},{4,3},{5,4},{6,5},{7,6},{8,15},{9,8},{10,9... | collective-permute-start | bytes 1179656 | tf_op jit(solution)/shard_map/ppermute | solution.py:133
  72.7 4.1 %collective-permute-start.10 = (bf16[192,512]{1,0:T(8,128)(2,1)S(1)}, bf16[192,512]{1,0:T(8,128)(2,1)S(1)}, u32[]{:S(2)}, u32[]{:S(2)}) collective-permute-start(bf16[192,512]{1,0:T(8,128)(2,1)S(1)} %bitcast.84), channel_id=1, source_target_pairs={{0,6},{1,7},{2,0},{3,1},{4,2},{5,3},{6,4},{7,5},{8,14},{9,15},{10,... | collective-permute-start | bytes 589832 | tf_op jit(solution)/shard_map/ppermute | solution.py:133
  79.0 5.6 %collective-permute-done.10.x_2a = bf16[192,512]{1,0:T(8,128)(2,1)S(1)} collective-permute-done((bf16[192,512]{1,0:T(8,128)(2,1)S(1)}, bf16[192,512]{1,0:T(8,128)(2,1)S(1)}, u32[]{:S(2)}, u32[]{:S(2)}) %collective-permute-start.10) | collective-permute-done | bytes 196640 | tf_op jit(solution)/shard_map/ppermute | solution.py:133
  84.6 4.6 %collective-permute-done.11.x_2b = bf16[192,512]{1,0:T(8,128)(2,1)S(1)} collective-permute-done((bf16[192,512]{1,0:T(8,128)(2,1)S(1)}, bf16[192,512]{1,0:T(8,128)(2,1)S(1)}, u32[]{:S(2)}, u32[]{:S(2)}) %collective-permute-start.11) | collective-permute-done | bytes 196640 | tf_op jit(solution)/shard_map/ppermute | solution.py:133
  89.2 3.8 %shard_map.134 = (bf16[384,512]{1,0:T(8,128)(2,1)S(1)}, bf16[192,256]{1,0:T(8,128)(2,1)S(1)}, bf16[192,256]{1,0:T(8,128)(2,1)S(1)}, bf16[256,2048]{1,0:T(8,128)(2,1)S(1)}) custom-call(s32[1]{0:T(128)} %bitcast.35.index, bf16[384,512]{1,0:T(8,128)(2,1)S(1)} %bitcast.76, bf16[384,512]{1,0:T(8,128)(2,1)S(1)} %collective-permute-done.8.x_1, ...), custom_call_target="tpu_custom_call" | custom-call | flops 2000000000 | bytes 10000000 | tf_op jit(solution)/shard_map/pallas_call | solution.py:220
  93.0 4.0 %collective-permute-start.15 = (bf16[192,256]{1,0:T(8,128)(2,1)S(1)}, bf16[192,256]{1,0:T(8,128)(2,1)S(1)}, u32[]{:S(2)}, u32[]{:S(2)}) collective-permute-start(bf16[192,256]{1,0:T(8,128)(2,1)S(1)} %get-tuple-element.21), channel_id=1, source_target_pairs={{0,1},{1,2},{2,3},{3,4},{4,5},{5,6},{6,7},{7,0},{8,9},{9,10},{10,1... | collective-permute-start | bytes 294920 | tf_op jit(solution)/shard_map/ppermute | solution.py:133
  99.6 2.8 %collective-permute-done.16.bottom = bf16[192,256]{1,0:T(8,128)(2,1)S(1)} collective-permute-done((bf16[192,256]{1,0:T(8,128)(2,1)S(1)}, bf16[192,256]{1,0:T(8,128)(2,1)S(1)}, u32[]{:S(2)}, u32[]{:S(2)}) %collective-permute-start.16) | collective-permute-done | bytes 98336 | tf_op jit(solution)/shard_map/ppermute | solution.py:133
  106.0 5.6 %collective-permute-start.18 = (bf16[384,256]{1,0:T(8,128)(2,1)S(1)}, bf16[384,256]{1,0:T(8,128)(2,1)S(1)}, u32[]{:S(2)}, u32[]{:S(2)}) collective-permute-start(bf16[384,256]{1,0:T(8,128)(2,1)S(1)} %get-tuple-element.25), channel_id=1, source_target_pairs={{0,5},{1,6},{2,7},{3,0},{4,1},{5,2},{6,3},{7,4},{8,13},{9,14},{10,... | collective-permute-start | bytes 589832 | tf_op jit(solution)/shard_map/ppermute | solution.py:133
  113.6 5.5 %collective-permute-start.20 = (bf16[384,256]{1,0:T(8,128)(2,1)S(1)}, bf16[384,256]{1,0:T(8,128)(2,1)S(1)}, u32[]{:S(2)}, u32[]{:S(2)}) collective-permute-start(bf16[384,256]{1,0:T(8,128)(2,1)S(1)} %get-tuple-element.27), channel_id=1, source_target_pairs={{0,6},{1,7},{2,0},{3,1},{4,2},{5,3},{6,4},{7,5},{8,14},{9,15},{10,... | collective-permute-start | bytes 589832 | tf_op jit(solution)/shard_map/ppermute | solution.py:133
  121.1 4.6 %collective-permute-start.22 = (bf16[384,256]{1,0:T(8,128)(2,1)S(1)}, bf16[384,256]{1,0:T(8,128)(2,1)S(1)}, u32[]{:S(2)}, u32[]{:S(2)}) collective-permute-start(bf16[384,256]{1,0:T(8,128)(2,1)S(1)} %get-tuple-element.29), channel_id=1, source_target_pairs={{0,7},{1,0},{2,1},{3,2},{4,3},{5,4},{6,5},{7,6},{8,15},{9,8},{10,9... | collective-permute-start | bytes 589832 | tf_op jit(solution)/shard_map/ppermute | solution.py:133
  125.7 3.2 %collective-permute-done.19.refs_3_ = bf16[384,256]{1,0:T(8,128)(2,1)S(1)} collective-permute-done((bf16[384,256]{1,0:T(8,128)(2,1)S(1)}, bf16[384,256]{1,0:T(8,128)(2,1)S(1)}, u32[]{:S(2)}, u32[]{:S(2)}) %collective-permute-start.19) | collective-permute-done | bytes 196640 | tf_op jit(solution)/shard_map/ppermute | solution.py:133
  128.9 4.1 %collective-permute-done.21.refs_5_ = bf16[384,256]{1,0:T(8,128)(2,1)S(1)} collective-permute-done((bf16[384,256]{1,0:T(8,128)(2,1)S(1)}, bf16[384,256]{1,0:T(8,128)(2,1)S(1)}, u32[]{:S(2)}, u32[]{:S(2)}) %collective-permute-start.21) | collective-permute-done | bytes 196640 | tf_op jit(solution)/shard_map/ppermute | solution.py:133
  136.0 16.2 %all-to-all-start.1 = ((bf16[16,24,256]{2,1,0:T(8,128)(2,1)}), bf16[16,24,256]{2,1,0:T(8,128)(2,1)S(1)}, u32[]{:S(2)}, u32[]{:S(2)}) async-start(bf16[16,24,256]{2,1,0:T(8,128)(2,1)} %bitcast.41), calls=%async_computation.1 | async-start | bytes 393216 | tf_op jit(solution)/shard_map/all_to_all | solution.py:255
  154.2 4.4 %collective-permute-start.2 = (bf16[512,128]{1,0:T(8,128)(2,1)S(1)}, bf16[512,128]{1,0:T(8,128)(2,1)S(1)}, u32[]{:S(2)}, u32[]{:S(2)}) collective-permute-start(bf16[512,128]{1,0:T(8,128)(2,1)S(1)} %copy-done.3), channel_id=1, source_target_pairs={{0,2},{1,3},{2,4},{3,5},{4,6},{5,7},{6,0},{7,1},{8,10},{9,11},{10,... | collective-permute-start | bytes 393224 | tf_op jit(solution)/shard_map/ppermute | solution.py:133
  158.6 3.6 %collective-permute-start.3 = (bf16[512,128]{1,0:T(8,128)(2,1)S(1)}, bf16[512,128]{1,0:T(8,128)(2,1)S(1)}, u32[]{:S(2)}, u32[]{:S(2)}) collective-permute-start(bf16[512,128]{1,0:T(8,128)(2,1)S(1)} %copy-done.3), channel_id=1, source_target_pairs={{0,3},{1,4},{2,5},{3,6},{4,7},{5,0},{6,1},{7,2},{8,11},{9,12},{10,... | collective-permute-start | bytes 393224 | tf_op jit(solution)/shard_map/ppermute | solution.py:133
  162.2 3.6 %collective-permute-start.4 = (bf16[512,128]{1,0:T(8,128)(2,1)S(1)}, bf16[512,128]{1,0:T(8,128)(2,1)S(1)}, u32[]{:S(2)}, u32[]{:S(2)}) collective-permute-start(bf16[512,128]{1,0:T(8,128)(2,1)S(1)} %copy-done.3), channel_id=1, source_target_pairs={{0,4},{1,5},{2,6},{3,7},{4,0},{5,1},{6,2},{7,3},{8,12},{9,13},{10,... | collective-permute-start | bytes 393224 | tf_op jit(solution)/shard_map/ppermute | solution.py:133
  165.8 6.0 %collective-permute-start.5 = (bf16[512,128]{1,0:T(8,128)(2,1)S(1)}, bf16[512,128]{1,0:T(8,128)(2,1)S(1)}, u32[]{:S(2)}, u32[]{:S(2)}) collective-permute-start(bf16[512,128]{1,0:T(8,128)(2,1)S(1)} %copy-done.3), channel_id=1, source_target_pairs={{0,5},{1,6},{2,7},{3,0},{4,1},{5,2},{6,3},{7,4},{8,13},{9,14},{10,... | collective-permute-start | bytes 393224 | tf_op jit(solution)/shard_map/ppermute | solution.py:133
  171.8 3.0 %collective-permute-start.6 = (bf16[512,128]{1,0:T(8,128)(2,1)S(1)}, bf16[512,128]{1,0:T(8,128)(2,1)S(1)}, u32[]{:S(2)}, u32[]{:S(2)}) collective-permute-start(bf16[512,128]{1,0:T(8,128)(2,1)S(1)} %copy-done.3), channel_id=1, source_target_pairs={{0,6},{1,7},{2,0},{3,1},{4,2},{5,3},{6,4},{7,5},{8,14},{9,15},{10,... | collective-permute-start | bytes 393224 | tf_op jit(solution)/shard_map/ppermute | solution.py:133
  174.8 3.4 %collective-permute-start.7 = (bf16[512,128]{1,0:T(8,128)(2,1)S(1)}, bf16[512,128]{1,0:T(8,128)(2,1)S(1)}, u32[]{:S(2)}, u32[]{:S(2)}) collective-permute-start(bf16[512,128]{1,0:T(8,128)(2,1)S(1)} %copy-done.3), channel_id=1, source_target_pairs={{0,7},{1,0},{2,1},{3,2},{4,3},{5,4},{6,5},{7,6},{8,15},{9,8},{10,9... | collective-permute-start | bytes 393224 | tf_op jit(solution)/shard_map/ppermute | solution.py:133
  178.6 4.3 %collective-permute-done.5.refs_5_ = bf16[512,128]{1,0:T(8,128)(2,1)S(1)} collective-permute-done((bf16[512,128]{1,0:T(8,128)(2,1)S(1)}, bf16[512,128]{1,0:T(8,128)(2,1)S(1)}, u32[]{:S(2)}, u32[]{:S(2)}) %collective-permute-start.5) | collective-permute-done | bytes 131104 | tf_op jit(solution)/shard_map/ppermute | solution.py:133
  182.9 7.0 %collective-permute-done.6.refs_6_ = bf16[512,128]{1,0:T(8,128)(2,1)S(1)} collective-permute-done((bf16[512,128]{1,0:T(8,128)(2,1)S(1)}, bf16[512,128]{1,0:T(8,128)(2,1)S(1)}, u32[]{:S(2)}, u32[]{:S(2)}) %collective-permute-start.6) | collective-permute-done | bytes 131104 | tf_op jit(solution)/shard_map/ppermute | solution.py:133
  (58 shorter events, 34.0 us)
Async XLA Ops:
  3.0 62.2 %all-to-all-start = ((bf16[16,24,512]{2,1,0:T(8,128)(2,1)}), bf16[16,24,512]{2,1,0:T(8,128)(2,1)S(1)}, u32[]{:S(2)}, u32[]{:S(2)}) async-start(bf16[16,24,512]{2,1,0:T(8,128)(2,1)} %bitcast.82), calls=%async_computation | async-start | bytes 786432 | tf_op jit(solution)/shard_map/all_to_all | solution.py:186
  48.4 10.6 %collective-permute-start = (bf16[32,128]{1,0:T(8,128)(2,1)S(1)}, bf16[32,128]{1,0:T(8,128)(2,1)S(1)}, u32[]{:S(2)}, u32[]{:S(2)}) collective-permute-start(bf16[32,128]{1,0:T(8,128)(2,1)S(1)} %slice.268), channel_id=1, source_target_pairs={{0,8},{8,16},{16,24},{24,32},{32,40},{40,48},{48,56},{56,64},{64,7... | collective-permute-start | bytes 24584 | tf_op jit(solution)/shard_map/ppermute | solution.py:195
  52.5 20.2 %collective-permute-start.12 = (bf16[1,2048,256]{2,1,0:T(8,128)(2,1)S(1)}, bf16[1,2048,256]{2,1,0:T(8,128)(2,1)}, u32[]{:S(2)}, u32[]{:S(2)}) collective-permute-start(bf16[1,2048,256]{2,1,0:T(8,128)(2,1)S(1)} %copy-done), channel_id=1, source_target_pairs={{0,8},{8,0},{1,9},{9,1},{2,10},{10,2},{3,11},{11,3},{4,12},{12,4},... | collective-permute-start | bytes 3145736 | tf_op jit(solution)/shard_map/ppermute | solution.py:137
  54.5 22.4 %collective-permute-start.13 = (bf16[1,2048,256]{2,1,0:T(8,128)(2,1)S(1)}, bf16[1,2048,256]{2,1,0:T(8,128)(2,1)}, u32[]{:S(2)}, u32[]{:S(2)}) collective-permute-start(bf16[1,2048,256]{2,1,0:T(8,128)(2,1)S(1)} %copy-done.1), channel_id=1, source_target_pairs={{0,8},{8,0},{1,9},{9,1},{2,10},{10,2},{3,11},{11,3},{4,12},{12,4},... | collective-permute-start | bytes 3145736 | tf_op jit(solution)/shard_map/ppermute | solution.py:137
  56.9 22.1 %collective-permute-start.14 = (bf16[1,256,2048]{2,1,0:T(8,128)(2,1)}, bf16[1,256,2048]{2,1,0:T(8,128)(2,1)}, u32[]{:S(2)}, u32[]{:S(2)}) collective-permute-start(bf16[1,256,2048]{2,1,0:T(8,128)(2,1)} %down_0.3), channel_id=1, source_target_pairs={{0,8},{8,0},{1,9},{9,1},{2,10},{10,2},{3,11},{11,3},{4,12},{12,4},... | collective-permute-start | bytes 3145736 | tf_op jit(solution)/shard_map/ppermute | solution.py:137
  65.3 23.9 %collective-permute-start.8 = (bf16[384,512]{1,0:T(8,128)(2,1)S(1)}, bf16[384,512]{1,0:T(8,128)(2,1)S(1)}, u32[]{:S(2)}, u32[]{:S(2)}) collective-permute-start(bf16[384,512]{1,0:T(8,128)(2,1)S(1)} %bitcast.74), channel_id=1, source_target_pairs={{0,7},{1,0},{2,1},{3,2},{4,3},{5,4},{6,5},{7,6},{8,15},{9,8},{10,9... | collective-permute-start | bytes 1179656 | tf_op jit(solution)/shard_map/ppermute | solution.py:133
  70.7 18.4 %collective-permute-start.9 = (bf16[384,512]{1,0:T(8,128)(2,1)S(1)}, bf16[384,512]{1,0:T(8,128)(2,1)S(1)}, u32[]{:S(2)}, u32[]{:S(2)}) collective-permute-start(bf16[384,512]{1,0:T(8,128)(2,1)S(1)} %bitcast.75), channel_id=1, source_target_pairs={{0,1},{1,2},{2,3},{3,4},{4,5},{5,6},{6,7},{7,0},{8,9},{9,10},{10,1... | collective-permute-start | bytes 1179656 | tf_op jit(solution)/shard_map/ppermute | solution.py:133
  72.7 11.8 %collective-permute-start.10 = (bf16[192,512]{1,0:T(8,128)(2,1)S(1)}, bf16[192,512]{1,0:T(8,128)(2,1)S(1)}, u32[]{:S(2)}, u32[]{:S(2)}) collective-permute-start(bf16[192,512]{1,0:T(8,128)(2,1)S(1)} %bitcast.84), channel_id=1, source_target_pairs={{0,6},{1,7},{2,0},{3,1},{4,2},{5,3},{6,4},{7,5},{8,14},{9,15},{10,... | collective-permute-start | bytes 589832 | tf_op jit(solution)/shard_map/ppermute | solution.py:133
  76.9 12.3 %collective-permute-start.11 = (bf16[192,512]{1,0:T(8,128)(2,1)S(1)}, bf16[192,512]{1,0:T(8,128)(2,1)S(1)}, u32[]{:S(2)}, u32[]{:S(2)}) collective-permute-start(bf16[192,512]{1,0:T(8,128)(2,1)S(1)} %bitcast.83), channel_id=1, source_target_pairs={{0,2},{1,3},{2,4},{3,5},{4,6},{5,7},{6,0},{7,1},{8,10},{9,11},{10,... | collective-permute-start | bytes 589832 | tf_op jit(solution)/shard_map/ppermute | solution.py:133
  93.0 6.6 %collective-permute-start.15 = (bf16[192,256]{1,0:T(8,128)(2,1)S(1)}, bf16[192,256]{1,0:T(8,128)(2,1)S(1)}, u32[]{:S(2)}, u32[]{:S(2)}) collective-permute-start(bf16[192,256]{1,0:T(8,128)(2,1)S(1)} %get-tuple-element.21), channel_id=1, source_target_pairs={{0,1},{1,2},{2,3},{3,4},{4,5},{5,6},{6,7},{7,0},{8,9},{9,10},{10,1... | collective-permute-start | bytes 294920 | tf_op jit(solution)/shard_map/ppermute | solution.py:133
  103.3 17.8 %collective-permute-start.17 = (bf16[384,256]{1,0:T(8,128)(2,1)S(1)}, bf16[384,256]{1,0:T(8,128)(2,1)S(1)}, u32[]{:S(2)}, u32[]{:S(2)}) collective-permute-start(bf16[384,256]{1,0:T(8,128)(2,1)S(1)} %get-tuple-element.24), channel_id=1, source_target_pairs={{0,3},{1,4},{2,5},{3,6},{4,7},{5,0},{6,1},{7,2},{8,11},{9,12},{10,... | collective-permute-start | bytes 589832 | tf_op jit(solution)/shard_map/ppermute | solution.py:133
  106.0 19.7 %collective-permute-start.18 = (bf16[384,256]{1,0:T(8,128)(2,1)S(1)}, bf16[384,256]{1,0:T(8,128)(2,1)S(1)}, u32[]{:S(2)}, u32[]{:S(2)}) collective-permute-start(bf16[384,256]{1,0:T(8,128)(2,1)S(1)} %get-tuple-element.25), channel_id=1, source_target_pairs={{0,5},{1,6},{2,7},{3,0},{4,1},{5,2},{6,3},{7,4},{8,13},{9,14},{10,... | collective-permute-start | bytes 589832 | tf_op jit(solution)/shard_map/ppermute | solution.py:133
  111.7 17.2 %collective-permute-start.19 = (bf16[384,256]{1,0:T(8,128)(2,1)S(1)}, bf16[384,256]{1,0:T(8,128)(2,1)S(1)}, u32[]{:S(2)}, u32[]{:S(2)}) collective-permute-start(bf16[384,256]{1,0:T(8,128)(2,1)S(1)} %get-tuple-element.26), channel_id=1, source_target_pairs={{0,2},{1,3},{2,4},{3,5},{4,6},{5,7},{6,0},{7,1},{8,10},{9,11},{10,... | collective-permute-start | bytes 589832 | tf_op jit(solution)/shard_map/ppermute | solution.py:133
  113.6 15.3 %collective-permute-start.20 = (bf16[384,256]{1,0:T(8,128)(2,1)S(1)}, bf16[384,256]{1,0:T(8,128)(2,1)S(1)}, u32[]{:S(2)}, u32[]{:S(2)}) collective-permute-start(bf16[384,256]{1,0:T(8,128)(2,1)S(1)} %get-tuple-element.27), channel_id=1, source_target_pairs={{0,6},{1,7},{2,0},{3,1},{4,2},{5,3},{6,4},{7,5},{8,14},{9,15},{10,... | collective-permute-start | bytes 589832 | tf_op jit(solution)/shard_map/ppermute | solution.py:133
  119.2 13.9 %collective-permute-start.21 = (bf16[384,256]{1,0:T(8,128)(2,1)S(1)}, bf16[384,256]{1,0:T(8,128)(2,1)S(1)}, u32[]{:S(2)}, u32[]{:S(2)}) collective-permute-start(bf16[384,256]{1,0:T(8,128)(2,1)S(1)} %get-tuple-element.28), channel_id=1, source_target_pairs={{0,1},{1,2},{2,3},{3,4},{4,5},{5,6},{6,7},{7,0},{8,9},{9,10},{10,1... | collective-permute-start | bytes 589832 | tf_op jit(solution)/shard_map/ppermute | solution.py:133
  121.1 14.0 %collective-permute-start.22 = (bf16[384,256]{1,0:T(8,128)(2,1)S(1)}, bf16[384,256]{1,0:T(8,128)(2,1)S(1)}, u32[]{:S(2)}, u32[]{:S(2)}) collective-permute-start(bf16[384,256]{1,0:T(8,128)(2,1)S(1)} %get-tuple-element.29), channel_id=1, source_target_pairs={{0,7},{1,0},{2,1},{3,2},{4,3},{5,4},{6,5},{7,6},{8,15},{9,8},{10,9... | collective-permute-start | bytes 589832 | tf_op jit(solution)/shard_map/ppermute | solution.py:133
  136.0 56.5 %all-to-all-start.1 = ((bf16[16,24,256]{2,1,0:T(8,128)(2,1)}), bf16[16,24,256]{2,1,0:T(8,128)(2,1)S(1)}, u32[]{:S(2)}, u32[]{:S(2)}) async-start(bf16[16,24,256]{2,1,0:T(8,128)(2,1)} %bitcast.41), calls=%async_computation.1 | async-start | bytes 393216 | tf_op jit(solution)/shard_map/all_to_all | solution.py:255
  152.2 19.6 %collective-permute-start.1 = (bf16[512,128]{1,0:T(8,128)(2,1)S(1)}, bf16[512,128]{1,0:T(8,128)(2,1)S(1)}, u32[]{:S(2)}, u32[]{:S(2)}) collective-permute-start(bf16[512,128]{1,0:T(8,128)(2,1)S(1)} %copy-done.3), channel_id=1, source_target_pairs={{0,1},{1,2},{2,3},{3,4},{4,5},{5,6},{6,7},{7,0},{8,9},{9,10},{10,1... | collective-permute-start | bytes 393224 | tf_op jit(solution)/shard_map/ppermute | solution.py:133
  154.2 20.7 %collective-permute-start.2 = (bf16[512,128]{1,0:T(8,128)(2,1)S(1)}, bf16[512,128]{1,0:T(8,128)(2,1)S(1)}, u32[]{:S(2)}, u32[]{:S(2)}) collective-permute-start(bf16[512,128]{1,0:T(8,128)(2,1)S(1)} %copy-done.3), channel_id=1, source_target_pairs={{0,2},{1,3},{2,4},{3,5},{4,6},{5,7},{6,0},{7,1},{8,10},{9,11},{10,... | collective-permute-start | bytes 393224 | tf_op jit(solution)/shard_map/ppermute | solution.py:133
  158.6 19.9 %collective-permute-start.3 = (bf16[512,128]{1,0:T(8,128)(2,1)S(1)}, bf16[512,128]{1,0:T(8,128)(2,1)S(1)}, u32[]{:S(2)}, u32[]{:S(2)}) collective-permute-start(bf16[512,128]{1,0:T(8,128)(2,1)S(1)} %copy-done.3), channel_id=1, source_target_pairs={{0,3},{1,4},{2,5},{3,6},{4,7},{5,0},{6,1},{7,2},{8,11},{9,12},{10,... | collective-permute-start | bytes 393224 | tf_op jit(solution)/shard_map/ppermute | solution.py:133
  162.2 16.4 %collective-permute-start.4 = (bf16[512,128]{1,0:T(8,128)(2,1)S(1)}, bf16[512,128]{1,0:T(8,128)(2,1)S(1)}, u32[]{:S(2)}, u32[]{:S(2)}) collective-permute-start(bf16[512,128]{1,0:T(8,128)(2,1)S(1)} %copy-done.3), channel_id=1, source_target_pairs={{0,4},{1,5},{2,6},{3,7},{4,0},{5,1},{6,2},{7,3},{8,12},{9,13},{10,... | collective-permute-start | bytes 393224 | tf_op jit(solution)/shard_map/ppermute | solution.py:133
  165.8 17.1 %collective-permute-start.5 = (bf16[512,128]{1,0:T(8,128)(2,1)S(1)}, bf16[512,128]{1,0:T(8,128)(2,1)S(1)}, u32[]{:S(2)}, u32[]{:S(2)}) collective-permute-start(bf16[512,128]{1,0:T(8,128)(2,1)S(1)} %copy-done.3), channel_id=1, source_target_pairs={{0,5},{1,6},{2,7},{3,0},{4,1},{5,2},{6,3},{7,4},{8,13},{9,14},{10,... | collective-permute-start | bytes 393224 | tf_op jit(solution)/shard_map/ppermute | solution.py:133
  171.8 18.1 %collective-permute-start.6 = (bf16[512,128]{1,0:T(8,128)(2,1)S(1)}, bf16[512,128]{1,0:T(8,128)(2,1)S(1)}, u32[]{:S(2)}, u32[]{:S(2)}) collective-permute-start(bf16[512,128]{1,0:T(8,128)(2,1)S(1)} %copy-done.3), channel_id=1, source_target_pairs={{0,6},{1,7},{2,0},{3,1},{4,2},{5,3},{6,4},{7,5},{8,14},{9,15},{10,... | collective-permute-start | bytes 393224 | tf_op jit(solution)/shard_map/ppermute | solution.py:133
  174.8 15.7 %collective-permute-start.7 = (bf16[512,128]{1,0:T(8,128)(2,1)S(1)}, bf16[512,128]{1,0:T(8,128)(2,1)S(1)}, u32[]{:S(2)}, u32[]{:S(2)}) collective-permute-start(bf16[512,128]{1,0:T(8,128)(2,1)S(1)} %copy-done.3), channel_id=1, source_target_pairs={{0,7},{1,0},{2,1},{3,2},{4,3},{5,4},{6,5},{7,6},{8,15},{9,8},{10,9... | collective-permute-start | bytes 393224 | tf_op jit(solution)/shard_map/ppermute | solution.py:133
  (10 other events, 304.2 us)

commit v11 on v10

--- a/solution.py
+++ b/solution.py
@@ -60,8 +60,9 @@
 
 
 def experts_kernel(
-    index, x_0, x_1, x_3, x_2a, x_2b, gate_0, up_0, gate_1, up_1, down_0, down_1, me, out, top, bottom, tall, sem
+    index, x_0, x_1, x_3, x_2a, x_2b, gate_0, up_0, gate_1, up_1, down_0, down_1, me, out, top, bottom, tall, *rest
 ):
+    *outs, sem = rest
     load = pltpu.make_async_copy(down_1.at[0], tall, sem)
     load.start()
     depth = x_0.shape[1]
@@ -84,6 +85,10 @@
     piece = dot(hidden[0], down_0[0, :, span]) + dot(hidden[1], tall[:, span])
     top[...] = piece[:half].astype(bf16)
     bottom[...] = piece[half:].astype(bf16)
+    for by, block in zip(offsets(n // 2 - 2), outs):
+        span = block_of(me, by, n, width)
+        piece = dot(hidden[0], down_0[0, :, span]) + dot(hidden[1], tall[:, span])
+        block[...] = piece.astype(bf16)
     units = hidden[0].shape[1]
     out[:, :units] = hidden[0]
     out[:, units:] = hidden[1]
@@ -93,19 +98,23 @@
     return pl.ds(pl.multiple_of(lax.rem(me[0] + by + n, n) * width, width), width)
 
 
-def pieces_kernel(far, me, hidden, down_0, down_1, top, bottom, *outs):
+def offsets(reach):
+    return [0] + [sign * k for k in range(1, reach + 1) for sign in (1, -1)]
+
+
+def far_kernel(far, me, hidden, down_0, down_1, top, bottom, ahead, behind):
     half, width = top.shape
     n, units = down_1.shape[1] // width, down_1.shape[0]
-    order = [0] + [sign * k for k in range(1, far + 1) for sign in (1, -1)]
-    for by, out in zip(order, outs):
+
+    def piece(by):
         span = block_of(me, by, n, width)
-        piece = dot(hidden[:, :units], down_0[0, :, span])
-        piece = piece + dot(hidden[:, units:], down_1[:, span])
-        if by == far:
-            piece = jnp.concatenate([piece[:half] + top[...].astype(f32), piece[half:]], axis=0)
-        if by == -far:
-            piece = jnp.concatenate([piece[:half], piece[half:] + bottom[...].astype(f32)], axis=0)
-        out[...] = piece.astype(bf16)
+        return dot(hidden[:, :units], down_0[0, :, span]) + dot(hidden[:, units:], down_1[:, span])
+
+    front, back = piece(far), piece(-far)
+    ahead[:half] = (front[:half] + top[...].astype(f32)).astype(bf16)
+    ahead[half:] = front[half:].astype(bf16)
+    behind[:half] = back[:half].astype(bf16)
+    behind[half:] = (back[half:] + bottom[...].astype(f32)).astype(bf16)
 
 
 def sum_kernel(*refs):
@@ -204,8 +213,9 @@
     from_back, from_front = {}, {}
     for k in range(parts, 0, -1):
         from_back[k] = moved(convolved, k)
-        if k < parts:
+        if 1 < k < parts:
             from_front[k] = moved(convolved, -k)
+    from_front[1] = moved(convolved, -1)
 
     rows = n_z * capacity
     arrived, _ = lax.optimization_barrier((arrived, convolved))
@@ -217,27 +227,29 @@
     units = gate_w.shape[2]
     me_ref = me.astype(jnp.int32).reshape(1)
     shape = lambda *dims: jax.ShapeDtypeStruct(dims, bf16)
-    hidden, top, bottom, down_b = pl.pallas_call(
+    far = parts - 1
+    near = [shape(rows, columns)] * (2 * far - 1)
+    hidden, top, bottom, down_b, own, *sent = pl.pallas_call(
         experts_kernel,
         out_shape=[
             shape(rows, 2 * units),
             shape(rows // 2, columns),
             shape(rows // 2, columns),
             shape(units, width),
-        ],
+        ]
+        + near,
         in_specs=[smem] + [vmem] * 10 + [pl.BlockSpec(memory_space=pl.ANY), smem],
-        out_specs=[vmem] * 4,
+        out_specs=[vmem] * (4 + len(near)),
         scratch_shapes=[pltpu.SemaphoreType.DMA],
         compiler_params=params(24),
         cost_estimate=cost(2 * 10**9, 10**7),
     )(quarter, x_0, x_1, x_3, x_2a, x_2b, gate_w, up_w, gate_b, up_b, down_w, down_b, me_ref)
     top, bottom = moved(top, 1), moved(bottom, -1)
-    far = parts - 1
-    own, *sent = pl.pallas_call(
-        functools.partial(pieces_kernel, far),
-        out_shape=[shape(rows, columns)] * (2 * far + 1),
+    sent += pl.pallas_call(
+        functools.partial(far_kernel, far),
+        out_shape=[shape(rows, columns)] * 2,
         in_specs=[smem] + [vmem] * 5,
-        out_specs=[vmem] * (2 * far + 1),
+        out_specs=[vmem] * 2,
         compiler_params=params(16),
         cost_estimate=cost(10**9, 10**6),
     )(me_ref, hidden, down_w, down_b, top, bottom)

time: 195 us -> 196 us (level)
  starting transfers between devices: 139 us -> 143 us
  waiting for transfers between devices: 39.3 us -> 35.7 us
    ppermute x19, waiting for transfers between devices: 34.4 us -> 30.8 us  [moved(): return lax.ppermute(value, 'tp', [(i, (i + by) % n) for i in range(n)])]
  transfers between devices with their start and end apart: 25 -> 25, of which waited for: 10 -> 8; matrix products, arithmetic and copies ran while one was open for 1% -> 1% of each run, Pallas kernels for 1% -> 1%
where the time goes in v11:
time: 196 us; the launch traced here: 194 us
  starting transfers between devices  143 us (73%)
  waiting for transfers between devices  35.7 us (18%)
  Pallas kernels  11.7 us (6%)
  other arithmetic  2.43 us (1%)
    ppermute x19, starting transfers between devices, moved(): return lax.ppermute(value, 'tp', [(i, (i + by) % n) for i in range(n)])  70.1 us
    all_to_all x1, starting transfers between devices, step_on_device(): lax.all_to_all(outgoing.reshape(experts, capacity, wide), 'z', split_axis...  44.2 us
    ppermute x19, waiting for transfers between devices, moved(): return lax.ppermute(value, 'tp', [(i, (i + by) % n) for i in range(n)])  30.8 us
    all_to_all x1, starting transfers between devices, step_on_device(): lax.all_to_all(sums.reshape(n_z, capacity, columns), 'z', split_axis=0, c...  17.7 us
    ppermute x3, starting transfers between devices, partner(): return lax.ppermute(value, 'core', [(0, 1), (1, 0)])  6.34 us
    pallas_call x1, Pallas kernels, step_on_device(): pl.pallas_call(experts_kernel, out_shape=[shape(rows, 2 * units), shape(r...  5.11 us
    all_to_all x1, waiting for transfers between devices, step_on_device(): lax.all_to_all(outgoing.reshape(experts, capacity, wide), 'z', split_axis...  4.91 us
    ppermute x1, starting transfers between devices, step_on_device(): lax.ppermute(glu[length - halo:], ('z', 'core'), [(i, i + 1) for i in ran...  4.15 us
  transfers between devices with their start and end apart: 25, of which 8 were waited for; matrix products, arithmetic and copies ran while one was open for 1% of the time, Pallas kernels for 1%

profile of v11, /device:TPU:65, one launch (start us, length us, event | category | flops | bytes accessed | tf_op | source)
XLA Modules:
  0.0 193.5 jit_solution(1744957620171611286)
XLA Ops:
  3.0 44.2 %all-to-all-start = ((bf16[16,24,512]{2,1,0:T(8,128)(2,1)}), bf16[16,24,512]{2,1,0:T(8,128)(2,1)S(1)}, u32[]{:S(2)}, u32[]{:S(2)}) async-start(bf16[16,24,512]{2,1,0:T(8,128)(2,1)} %bitcast.82), calls=%async_computation | async-start | bytes 786432 | tf_op jit(solution)/shard_map/all_to_all | solution.py:195
  48.4 4.2 %collective-permute-start = (bf16[32,128]{1,0:T(8,128)(2,1)S(1)}, bf16[32,128]{1,0:T(8,128)(2,1)S(1)}, u32[]{:S(2)}, u32[]{:S(2)}) collective-permute-start(bf16[32,128]{1,0:T(8,128)(2,1)S(1)} %slice.268), channel_id=1, source_target_pairs={{0,8},{8,16},{16,24},{24,32},{32,40},{40,48},{48,56},{56,64},{64,7... | collective-permute-start | bytes 24584 | tf_op jit(solution)/shard_map/ppermute | solution.py:204
  60.4 4.9 %all-to-all-done = bf16[16,24,512]{2,1,0:T(8,128)(2,1)S(1)} async-done(((bf16[16,24,512]{2,1,0:T(8,128)(2,1)}), bf16[16,24,512]{2,1,0:T(8,128)(2,1)S(1)}, u32[]{:S(2)}, u32[]{:S(2)}) %all-to-all-start) | async-done | bytes 393248 | tf_op jit(solution)/shard_map/all_to_all | solution.py:195
  65.3 5.4 %collective-permute-start.8 = (bf16[384,512]{1,0:T(8,128)(2,1)S(1)}, bf16[384,512]{1,0:T(8,128)(2,1)S(1)}, u32[]{:S(2)}, u32[]{:S(2)}) collective-permute-start(bf16[384,512]{1,0:T(8,128)(2,1)S(1)} %bitcast.74), channel_id=1, source_target_pairs={{0,7},{1,0},{2,1},{3,2},{4,3},{5,4},{6,5},{7,6},{8,15},{9,8},{10,9... | collective-permute-start | bytes 1179656 | tf_op jit(solution)/shard_map/ppermute | solution.py:142
  72.7 4.1 %collective-permute-start.10 = (bf16[192,512]{1,0:T(8,128)(2,1)S(1)}, bf16[192,512]{1,0:T(8,128)(2,1)S(1)}, u32[]{:S(2)}, u32[]{:S(2)}) collective-permute-start(bf16[192,512]{1,0:T(8,128)(2,1)S(1)} %bitcast.84), channel_id=1, source_target_pairs={{0,6},{1,7},{2,0},{3,1},{4,2},{5,3},{6,4},{7,5},{8,14},{9,15},{10,... | collective-permute-start | bytes 589832 | tf_op jit(solution)/shard_map/ppermute | solution.py:142
  79.0 5.6 %collective-permute-done.10.x_2a = bf16[192,512]{1,0:T(8,128)(2,1)S(1)} collective-permute-done((bf16[192,512]{1,0:T(8,128)(2,1)S(1)}, bf16[192,512]{1,0:T(8,128)(2,1)S(1)}, u32[]{:S(2)}, u32[]{:S(2)}) %collective-permute-start.10) | collective-permute-done | bytes 196640 | tf_op jit(solution)/shard_map/ppermute | solution.py:142
  84.6 4.6 %collective-permute-done.11.x_2b = bf16[192,512]{1,0:T(8,128)(2,1)S(1)} collective-permute-done((bf16[192,512]{1,0:T(8,128)(2,1)S(1)}, bf16[192,512]{1,0:T(8,128)(2,1)S(1)}, u32[]{:S(2)}, u32[]{:S(2)}) %collective-permute-start.11) | collective-permute-done | bytes 196640 | tf_op jit(solution)/shard_map/ppermute | solution.py:142
  89.2 5.1 %shard_map.134 = (bf16[384,512]{1,0:T(8,128)(2,1)S(1)}, bf16[192,256]{1,0:T(8,128)(2,1)S(1)}, bf16[192,256]{1,0:T(8,128)(2,1)S(1)}, bf16[256,2048]{1,0:T(8,128)(...) custom-call(s32[1]{0:T(128)} %bitcast.35.index, ...), custom_call_target="tpu_custom_call" | custom-call | flops 2000000000 | bytes 10000000 | tf_op jit(solution)/shard_map/pallas_call | solution.py:232
  96.2 4.0 %collective-permute-start.15 = (bf16[192,256]{1,0:T(8,128)(2,1)S(1)}, bf16[192,256]{1,0:T(8,128)(2,1)S(1)}, u32[]{:S(2)}, u32[]{:S(2)}) collective-permute-start(bf16[192,256]{1,0:T(8,128)(2,1)S(1)} %get-tuple-element.22), channel_id=1, source_target_pairs={{0,1},{1,2},{2,3},{3,4},{4,5},{5,6},{6,7},{7,0},{8,9},{9,10},{10,1... | collective-permute-start | bytes 294920 | tf_op jit(solution)/shard_map/ppermute | solution.py:142
  100.2 4.3 %collective-permute-start.16 = (bf16[192,256]{1,0:T(8,128)(2,1)S(1)}, bf16[192,256]{1,0:T(8,128)(2,1)S(1)}, u32[]{:S(2)}, u32[]{:S(2)}) collective-permute-start(bf16[192,256]{1,0:T(8,128)(2,1)S(1)} %get-tuple-element.23), channel_id=1, source_target_pairs={{0,7},{1,0},{2,1},{3,2},{4,3},{5,4},{6,5},{7,6},{8,15},{9,8},{10,9... | collective-permute-start | bytes 294920 | tf_op jit(solution)/shard_map/ppermute | solution.py:142
  104.6 3.1 %collective-permute-start.20 = (bf16[384,256]{1,0:T(8,128)(2,1)S(1)}, bf16[384,256]{1,0:T(8,128)(2,1)S(1)}, u32[]{:S(2)}, u32[]{:S(2)}) collective-permute-start(bf16[384,256]{1,0:T(8,128)(2,1)S(1)} %get-tuple-element.27), channel_id=1, source_target_pairs={{0,6},{1,7},{2,0},{3,1},{4,2},{5,3},{6,4},{7,5},{8,14},{9,15},{10,... | collective-permute-start | bytes 589832 | tf_op jit(solution)/shard_map/ppermute | solution.py:142
  107.7 3.4 %collective-permute-start.21 = (bf16[384,256]{1,0:T(8,128)(2,1)S(1)}, bf16[384,256]{1,0:T(8,128)(2,1)S(1)}, u32[]{:S(2)}, u32[]{:S(2)}) collective-permute-start(bf16[384,256]{1,0:T(8,128)(2,1)S(1)} %get-tuple-element.28), channel_id=1, source_target_pairs={{0,1},{1,2},{2,3},{3,4},{4,5},{5,6},{6,7},{7,0},{8,9},{9,10},{10,1... | collective-permute-start | bytes 589832 | tf_op jit(solution)/shard_map/ppermute | solution.py:142
  111.1 3.2 %collective-permute-start.22 = (bf16[384,256]{1,0:T(8,128)(2,1)S(1)}, bf16[384,256]{1,0:T(8,128)(2,1)S(1)}, u32[]{:S(2)}, u32[]{:S(2)}) collective-permute-start(bf16[384,256]{1,0:T(8,128)(2,1)S(1)} %get-tuple-element.29), channel_id=1, source_target_pairs={{0,7},{1,0},{2,1},{3,2},{4,3},{5,4},{6,5},{7,6},{8,15},{9,8},{10,9... | collective-permute-start | bytes 589832 | tf_op jit(solution)/shard_map/ppermute | solution.py:142
  116.7 6.4 %collective-permute-start.18 = (bf16[384,256]{1,0:T(8,128)(2,1)S(1)}, bf16[384,256]{1,0:T(8,128)(2,1)S(1)}, u32[]{:S(2)}, u32[]{:S(2)}) collective-permute-start(bf16[384,256]{1,0:T(8,128)(2,1)S(1)} %get-tuple-element.25), channel_id=1, source_target_pairs={{0,5},{1,6},{2,7},{3,0},{4,1},{5,2},{6,3},{7,4},{8,13},{9,14},{10,... | collective-permute-start | bytes 589832 | tf_op jit(solution)/shard_map/ppermute | solution.py:142
  123.1 5.9 %collective-permute-done.17.refs_1_ = bf16[384,256]{1,0:T(8,128)(2,1)S(1)} collective-permute-done((bf16[384,256]{1,0:T(8,128)(2,1)S(1)}, bf16[384,256]{1,0:T(8,128)(2,1)S(1)}, u32[]{:S(2)}, u32[]{:S(2)}) %collective-permute-start.17) | collective-permute-done | bytes 196640 | tf_op jit(solution)/shard_map/ppermute | solution.py:142
  129.0 2.8 %collective-permute-done.18.refs_2_ = bf16[384,256]{1,0:T(8,128)(2,1)S(1)} collective-permute-done((bf16[384,256]{1,0:T(8,128)(2,1)S(1)}, bf16[384,256]{1,0:T(8,128)(2,1)S(1)}, u32[]{:S(2)}, u32[]{:S(2)}) %collective-permute-start.18) | collective-permute-done | bytes 196640 | tf_op jit(solution)/shard_map/ppermute | solution.py:142
  132.7 17.7 %all-to-all-start.1 = ((bf16[16,24,256]{2,1,0:T(8,128)(2,1)}), bf16[16,24,256]{2,1,0:T(8,128)(2,1)S(1)}, u32[]{:S(2)}, u32[]{:S(2)}) async-start(bf16[16,24,256]{2,1,0:T(8,128)(2,1)} %bitcast.41), calls=%async_computation.1 | async-start | bytes 393216 | tf_op jit(solution)/shard_map/all_to_all | solution.py:267
  152.3 4.6 %collective-permute-start.2 = (bf16[512,128]{1,0:T(8,128)(2,1)S(1)}, bf16[512,128]{1,0:T(8,128)(2,1)S(1)}, u32[]{:S(2)}, u32[]{:S(2)}) collective-permute-start(bf16[512,128]{1,0:T(8,128)(2,1)S(1)} %copy-done.3), channel_id=1, source_target_pairs={{0,2},{1,3},{2,4},{3,5},{4,6},{5,7},{6,0},{7,1},{8,10},{9,11},{10,... | collective-permute-start | bytes 393224 | tf_op jit(solution)/shard_map/ppermute | solution.py:142
  156.9 5.8 %collective-permute-start.3 = (bf16[512,128]{1,0:T(8,128)(2,1)S(1)}, bf16[512,128]{1,0:T(8,128)(2,1)S(1)}, u32[]{:S(2)}, u32[]{:S(2)}) collective-permute-start(bf16[512,128]{1,0:T(8,128)(2,1)S(1)} %copy-done.3), channel_id=1, source_target_pairs={{0,3},{1,4},{2,5},{3,6},{4,7},{5,0},{6,1},{7,2},{8,11},{9,12},{10,... | collective-permute-start | bytes 393224 | tf_op jit(solution)/shard_map/ppermute | solution.py:142
  162.8 3.7 %collective-permute-start.4 = (bf16[512,128]{1,0:T(8,128)(2,1)S(1)}, bf16[512,128]{1,0:T(8,128)(2,1)S(1)}, u32[]{:S(2)}, u32[]{:S(2)}) collective-permute-start(bf16[512,128]{1,0:T(8,128)(2,1)S(1)} %copy-done.3), channel_id=1, source_target_pairs={{0,4},{1,5},{2,6},{3,7},{4,0},{5,1},{6,2},{7,3},{8,12},{9,13},{10,... | collective-permute-start | bytes 393224 | tf_op jit(solution)/shard_map/ppermute | solution.py:142
  166.5 4.7 %collective-permute-start.5 = (bf16[512,128]{1,0:T(8,128)(2,1)S(1)}, bf16[512,128]{1,0:T(8,128)(2,1)S(1)}, u32[]{:S(2)}, u32[]{:S(2)}) collective-permute-start(bf16[512,128]{1,0:T(8,128)(2,1)S(1)} %copy-done.3), channel_id=1, source_target_pairs={{0,5},{1,6},{2,7},{3,0},{4,1},{5,2},{6,3},{7,4},{8,13},{9,14},{10,... | collective-permute-start | bytes 393224 | tf_op jit(solution)/shard_map/ppermute | solution.py:142
  171.1 5.5 %collective-permute-start.6 = (bf16[512,128]{1,0:T(8,128)(2,1)S(1)}, bf16[512,128]{1,0:T(8,128)(2,1)S(1)}, u32[]{:S(2)}, u32[]{:S(2)}) collective-permute-start(bf16[512,128]{1,0:T(8,128)(2,1)S(1)} %copy-done.3), channel_id=1, source_target_pairs={{0,6},{1,7},{2,0},{3,1},{4,2},{5,3},{6,4},{7,5},{8,14},{9,15},{10,... | collective-permute-start | bytes 393224 | tf_op jit(solution)/shard_map/ppermute | solution.py:142
  179.0 3.9 %collective-permute-done.5.refs_5_ = bf16[512,128]{1,0:T(8,128)(2,1)S(1)} collective-permute-done((bf16[512,128]{1,0:T(8,128)(2,1)S(1)}, bf16[512,128]{1,0:T(8,128)(2,1)S(1)}, u32[]{:S(2)}, u32[]{:S(2)}) %collective-permute-start.5) | collective-permute-done | bytes 131104 | tf_op jit(solution)/shard_map/ppermute | solution.py:142
  182.9 5.9 %collective-permute-done.6.refs_6_ = bf16[512,128]{1,0:T(8,128)(2,1)S(1)} collective-permute-done((bf16[512,128]{1,0:T(8,128)(2,1)S(1)}, bf16[512,128]{1,0:T(8,128)(2,1)S(1)}, u32[]{:S(2)}, u32[]{:S(2)}) %collective-permute-start.6) | collective-permute-done | bytes 131104 | tf_op jit(solution)/shard_map/ppermute | solution.py:142
  (58 shorter events, 29.5 us)
Async XLA Ops:
  3.0 62.2 %all-to-all-start = ((bf16[16,24,512]{2,1,0:T(8,128)(2,1)}), bf16[16,24,512]{2,1,0:T(8,128)(2,1)S(1)}, u32[]{:S(2)}, u32[]{:S(2)}) async-start(bf16[16,24,512]{2,1,0:T(8,128)(2,1)} %bitcast.82), calls=%async_computation | async-start | bytes 786432 | tf_op jit(solution)/shard_map/all_to_all | solution.py:195
  52.5 20.2 %collective-permute-start.12 = (bf16[1,2048,256]{2,1,0:T(8,128)(2,1)S(1)}, bf16[1,2048,256]{2,1,0:T(8,128)(2,1)}, u32[]{:S(2)}, u32[]{:S(2)}) collective-permute-start(bf16[1,2048,256]{2,1,0:T(8,128)(2,1)S(1)} %copy-done), channel_id=1, source_target_pairs={{0,8},{8,0},{1,9},{9,1},{2,10},{10,2},{3,11},{11,3},{4,12},{12,4},... | collective-permute-start | bytes 3145736 | tf_op jit(solution)/shard_map/ppermute | solution.py:146
  54.5 22.4 %collective-permute-start.13 = (bf16[1,2048,256]{2,1,0:T(8,128)(2,1)S(1)}, bf16[1,2048,256]{2,1,0:T(8,128)(2,1)}, u32[]{:S(2)}, u32[]{:S(2)}) collective-permute-start(bf16[1,2048,256]{2,1,0:T(8,128)(2,1)S(1)} %copy-done.1), channel_id=1, source_target_pairs={{0,8},{8,0},{1,9},{9,1},{2,10},{10,2},{3,11},{11,3},{4,12},{12,4},... | collective-permute-start | bytes 3145736 | tf_op jit(solution)/shard_map/ppermute | solution.py:146
  56.9 22.1 %collective-permute-start.14 = (bf16[1,256,2048]{2,1,0:T(8,128)(2,1)}, bf16[1,256,2048]{2,1,0:T(8,128)(2,1)}, u32[]{:S(2)}, u32[]{:S(2)}) collective-permute-start(bf16[1,256,2048]{2,1,0:T(8,128)(2,1)} %down_0.3), channel_id=1, source_target_pairs={{0,8},{8,0},{1,9},{9,1},{2,10},{10,2},{3,11},{11,3},{4,12},{12,4},... | collective-permute-start | bytes 3145736 | tf_op jit(solution)/shard_map/ppermute | solution.py:146
  65.3 23.9 %collective-permute-start.8 = (bf16[384,512]{1,0:T(8,128)(2,1)S(1)}, bf16[384,512]{1,0:T(8,128)(2,1)S(1)}, u32[]{:S(2)}, u32[]{:S(2)}) collective-permute-start(bf16[384,512]{1,0:T(8,128)(2,1)S(1)} %bitcast.74), channel_id=1, source_target_pairs={{0,7},{1,0},{2,1},{3,2},{4,3},{5,4},{6,5},{7,6},{8,15},{9,8},{10,9... | collective-permute-start | bytes 1179656 | tf_op jit(solution)/shard_map/ppermute | solution.py:142
  70.7 18.4 %collective-permute-start.9 = (bf16[384,512]{1,0:T(8,128)(2,1)S(1)}, bf16[384,512]{1,0:T(8,128)(2,1)S(1)}, u32[]{:S(2)}, u32[]{:S(2)}) collective-permute-start(bf16[384,512]{1,0:T(8,128)(2,1)S(1)} %bitcast.75), channel_id=1, source_target_pairs={{0,1},{1,2},{2,3},{3,4},{4,5},{5,6},{6,7},{7,0},{8,9},{9,10},{10,1... | collective-permute-start | bytes 1179656 | tf_op jit(solution)/shard_map/ppermute | solution.py:142
  72.7 11.8 %collective-permute-start.10 = (bf16[192,512]{1,0:T(8,128)(2,1)S(1)}, bf16[192,512]{1,0:T(8,128)(2,1)S(1)}, u32[]{:S(2)}, u32[]{:S(2)}) collective-permute-start(bf16[192,512]{1,0:T(8,128)(2,1)S(1)} %bitcast.84), channel_id=1, source_target_pairs={{0,6},{1,7},{2,0},{3,1},{4,2},{5,3},{6,4},{7,5},{8,14},{9,15},{10,... | collective-permute-start | bytes 589832 | tf_op jit(solution)/shard_map/ppermute | solution.py:142
  76.9 12.3 %collective-permute-start.11 = (bf16[192,512]{1,0:T(8,128)(2,1)S(1)}, bf16[192,512]{1,0:T(8,128)(2,1)S(1)}, u32[]{:S(2)}, u32[]{:S(2)}) collective-permute-start(bf16[192,512]{1,0:T(8,128)(2,1)S(1)} %bitcast.83), channel_id=1, source_target_pairs={{0,2},{1,3},{2,4},{3,5},{4,6},{5,7},{6,0},{7,1},{8,10},{9,11},{10,... | collective-permute-start | bytes 589832 | tf_op jit(solution)/shard_map/ppermute | solution.py:142
  94.3 22.4 %collective-permute-start.19 = (bf16[384,256]{1,0:T(8,128)(2,1)S(1)}, bf16[384,256]{1,0:T(8,128)(2,1)S(1)}, u32[]{:S(2)}, u32[]{:S(2)}) collective-permute-start(bf16[384,256]{1,0:T(8,128)(2,1)S(1)} %get-tuple-element.26), channel_id=1, source_target_pairs={{0,2},{1,3},{2,4},{3,5},{4,6},{5,7},{6,0},{7,1},{8,10},{9,11},{10,... | collective-permute-start | bytes 589832 | tf_op jit(solution)/shard_map/ppermute | solution.py:142
  96.2 14.9 %collective-permute-start.15 = (bf16[192,256]{1,0:T(8,128)(2,1)S(1)}, bf16[192,256]{1,0:T(8,128)(2,1)S(1)}, u32[]{:S(2)}, u32[]{:S(2)}) collective-permute-start(bf16[192,256]{1,0:T(8,128)(2,1)S(1)} %get-tuple-element.22), channel_id=1, source_target_pairs={{0,1},{1,2},{2,3},{3,4},{4,5},{5,6},{6,7},{7,0},{8,9},{9,10},{10,1... | collective-permute-start | bytes 294920 | tf_op jit(solution)/shard_map/ppermute | solution.py:142
  100.2 14.1 %collective-permute-start.16 = (bf16[192,256]{1,0:T(8,128)(2,1)S(1)}, bf16[192,256]{1,0:T(8,128)(2,1)S(1)}, u32[]{:S(2)}, u32[]{:S(2)}) collective-permute-start(bf16[192,256]{1,0:T(8,128)(2,1)S(1)} %get-tuple-element.23), channel_id=1, source_target_pairs={{0,7},{1,0},{2,1},{3,2},{4,3},{5,4},{6,5},{7,6},{8,15},{9,8},{10,9... | collective-permute-start | bytes 294920 | tf_op jit(solution)/shard_map/ppermute | solution.py:142
  104.6 18.5 %collective-permute-start.20 = (bf16[384,256]{1,0:T(8,128)(2,1)S(1)}, bf16[384,256]{1,0:T(8,128)(2,1)S(1)}, u32[]{:S(2)}, u32[]{:S(2)}) collective-permute-start(bf16[384,256]{1,0:T(8,128)(2,1)S(1)} %get-tuple-element.27), channel_id=1, source_target_pairs={{0,6},{1,7},{2,0},{3,1},{4,2},{5,3},{6,4},{7,5},{8,14},{9,15},{10,... | collective-permute-start | bytes 589832 | tf_op jit(solution)/shard_map/ppermute | solution.py:142
  107.7 15.4 %collective-permute-start.21 = (bf16[384,256]{1,0:T(8,128)(2,1)S(1)}, bf16[384,256]{1,0:T(8,128)(2,1)S(1)}, u32[]{:S(2)}, u32[]{:S(2)}) collective-permute-start(bf16[384,256]{1,0:T(8,128)(2,1)S(1)} %get-tuple-element.28), channel_id=1, source_target_pairs={{0,1},{1,2},{2,3},{3,4},{4,5},{5,6},{6,7},{7,0},{8,9},{9,10},{10,1... | collective-permute-start | bytes 589832 | tf_op jit(solution)/shard_map/ppermute | solution.py:142
  111.1 12.0 %collective-permute-start.22 = (bf16[384,256]{1,0:T(8,128)(2,1)S(1)}, bf16[384,256]{1,0:T(8,128)(2,1)S(1)}, u32[]{:S(2)}, u32[]{:S(2)}) collective-permute-start(bf16[384,256]{1,0:T(8,128)(2,1)S(1)} %get-tuple-element.29), channel_id=1, source_target_pairs={{0,7},{1,0},{2,1},{3,2},{4,3},{5,4},{6,5},{7,6},{8,15},{9,8},{10,9... | collective-permute-start | bytes 589832 | tf_op jit(solution)/shard_map/ppermute | solution.py:142
  114.7 14.3 %collective-permute-start.17 = (bf16[384,256]{1,0:T(8,128)(2,1)S(1)}, bf16[384,256]{1,0:T(8,128)(2,1)S(1)}, u32[]{:S(2)}, u32[]{:S(2)}) collective-permute-start(bf16[384,256]{1,0:T(8,128)(2,1)S(1)} %get-tuple-element.24), channel_id=1, source_target_pairs={{0,3},{1,4},{2,5},{3,6},{4,7},{5,0},{6,1},{7,2},{8,11},{9,12},{10,... | collective-permute-start | bytes 589832 | tf_op jit(solution)/shard_map/ppermute | solution.py:142
  116.7 15.2 %collective-permute-start.18 = (bf16[384,256]{1,0:T(8,128)(2,1)S(1)}, bf16[384,256]{1,0:T(8,128)(2,1)S(1)}, u32[]{:S(2)}, u32[]{:S(2)}) collective-permute-start(bf16[384,256]{1,0:T(8,128)(2,1)S(1)} %get-tuple-element.25), channel_id=1, source_target_pairs={{0,5},{1,6},{2,7},{3,0},{4,1},{5,2},{6,3},{7,4},{8,13},{9,14},{10,... | collective-permute-start | bytes 589832 | tf_op jit(solution)/shard_map/ppermute | solution.py:142
  132.7 60.0 %all-to-all-start.1 = ((bf16[16,24,256]{2,1,0:T(8,128)(2,1)}), bf16[16,24,256]{2,1,0:T(8,128)(2,1)S(1)}, u32[]{:S(2)}, u32[]{:S(2)}) async-start(bf16[16,24,256]{2,1,0:T(8,128)(2,1)} %bitcast.41), calls=%async_computation.1 | async-start | bytes 393216 | tf_op jit(solution)/shard_map/all_to_all | solution.py:267
  150.4 20.8 %collective-permute-start.1 = (bf16[512,128]{1,0:T(8,128)(2,1)S(1)}, bf16[512,128]{1,0:T(8,128)(2,1)S(1)}, u32[]{:S(2)}, u32[]{:S(2)}) collective-permute-start(bf16[512,128]{1,0:T(8,128)(2,1)S(1)} %copy-done.3), channel_id=1, source_target_pairs={{0,1},{1,2},{2,3},{3,4},{4,5},{5,6},{6,7},{7,0},{8,9},{9,10},{10,1... | collective-permute-start | bytes 393224 | tf_op jit(solution)/shard_map/ppermute | solution.py:142
  152.3 24.3 %collective-permute-start.2 = (bf16[512,128]{1,0:T(8,128)(2,1)S(1)}, bf16[512,128]{1,0:T(8,128)(2,1)S(1)}, u32[]{:S(2)}, u32[]{:S(2)}) collective-permute-start(bf16[512,128]{1,0:T(8,128)(2,1)S(1)} %copy-done.3), channel_id=1, source_target_pairs={{0,2},{1,3},{2,4},{3,5},{4,6},{5,7},{6,0},{7,1},{8,10},{9,11},{10,... | collective-permute-start | bytes 393224 | tf_op jit(solution)/shard_map/ppermute | solution.py:142
  156.9 22.0 %collective-permute-start.3 = (bf16[512,128]{1,0:T(8,128)(2,1)S(1)}, bf16[512,128]{1,0:T(8,128)(2,1)S(1)}, u32[]{:S(2)}, u32[]{:S(2)}) collective-permute-start(bf16[512,128]{1,0:T(8,128)(2,1)S(1)} %copy-done.3), channel_id=1, source_target_pairs={{0,3},{1,4},{2,5},{3,6},{4,7},{5,0},{6,1},{7,2},{8,11},{9,12},{10,... | collective-permute-start | bytes 393224 | tf_op jit(solution)/shard_map/ppermute | solution.py:142
  162.8 16.2 %collective-permute-start.4 = (bf16[512,128]{1,0:T(8,128)(2,1)S(1)}, bf16[512,128]{1,0:T(8,128)(2,1)S(1)}, u32[]{:S(2)}, u32[]{:S(2)}) collective-permute-start(bf16[512,128]{1,0:T(8,128)(2,1)S(1)} %copy-done.3), channel_id=1, source_target_pairs={{0,4},{1,5},{2,6},{3,7},{4,0},{5,1},{6,2},{7,3},{8,12},{9,13},{10,... | collective-permute-start | bytes 393224 | tf_op jit(solution)/shard_map/ppermute | solution.py:142
  166.5 16.4 %collective-permute-start.5 = (bf16[512,128]{1,0:T(8,128)(2,1)S(1)}, bf16[512,128]{1,0:T(8,128)(2,1)S(1)}, u32[]{:S(2)}, u32[]{:S(2)}) collective-permute-start(bf16[512,128]{1,0:T(8,128)(2,1)S(1)} %copy-done.3), channel_id=1, source_target_pairs={{0,5},{1,6},{2,7},{3,0},{4,1},{5,2},{6,3},{7,4},{8,13},{9,14},{10,... | collective-permute-start | bytes 393224 | tf_op jit(solution)/shard_map/ppermute | solution.py:142
  171.1 17.6 %collective-permute-start.6 = (bf16[512,128]{1,0:T(8,128)(2,1)S(1)}, bf16[512,128]{1,0:T(8,128)(2,1)S(1)}, u32[]{:S(2)}, u32[]{:S(2)}) collective-permute-start(bf16[512,128]{1,0:T(8,128)(2,1)S(1)} %copy-done.3), channel_id=1, source_target_pairs={{0,6},{1,7},{2,0},{3,1},{4,2},{5,3},{6,4},{7,5},{8,14},{9,15},{10,... | collective-permute-start | bytes 393224 | tf_op jit(solution)/shard_map/ppermute | solution.py:142
  176.7 14.2 %collective-permute-start.7 = (bf16[512,128]{1,0:T(8,128)(2,1)S(1)}, bf16[512,128]{1,0:T(8,128)(2,1)S(1)}, u32[]{:S(2)}, u32[]{:S(2)}) collective-permute-start(bf16[512,128]{1,0:T(8,128)(2,1)S(1)} %copy-done.3), channel_id=1, source_target_pairs={{0,7},{1,0},{2,1},{3,2},{4,3},{5,4},{6,5},{7,6},{8,15},{9,8},{10,9... | collective-permute-start | bytes 393224 | tf_op jit(solution)/shard_map/ppermute | solution.py:142
  (10 other events, 320.2 us)
